TPU v7x, 32 devices: a whole 2x2x4 slice. The times are simulated.
32 devices in a mesh: grp: 2 (over y), sp: 4 (over z), tp: 4 (over x, core).
Axes of the slice: x: 2, y: 2, z: 4, core: 2. Of those that a mesh axis runs over, the one named last changes fastest.
Arguments:
- latents: bfloat16 [3072, 4096], P(('grp', 'sp', 'tp')), parts along dimension 0, may hold values from -3 to 3
- conditions: float32 [4, 4096], P('grp', 'sp'), parts along dimension 0, may hold values from -6 to 6
- context: bfloat16 [1024, 4096], P(('grp', 'sp')), parts along dimension 0, may hold values from -6 to 6
- w_shift: bfloat16 [4096, 4096], P('sp', 'tp'), may hold values from -0.09375 to 0.09375
- w_scale: bfloat16 [4096, 4096], P('sp', 'tp'), may hold values from -0.09375 to 0.09375
- w_gate: bfloat16 [4096, 4096], P('sp', 'tp'), may hold values from -0.09375 to 0.09375
- w_qdown: bfloat16 [4096, 1024], P(None, 'tp'), may hold values from -2 to 2
- w_kvdown: bfloat16 [4096, 512], P(None, 'tp'), may hold values from -2 to 2
- w_rope: bfloat16 [4096, 32], replicated, may hold values from -0.09375 to 0.09375
- q_gain: float32 [1024], replicated, may hold values from 1 to 24
- latent_norm_gain: float32 [512], replicated, may hold values from 0.1 to 1.9
- query_up_weight: bfloat16 [1024, 3072], P(None, 'tp'), may hold values from -0.1875 to 0.1875
- key_up_weight: bfloat16 [512, 2048], P(None, 'tp'), may hold values from -0.25 to 0.25
- value_up_weight: bfloat16 [512, 2048], P(None, 'tp'), may hold values from -0.25 to 0.25
- context_bias: float32 [32], P('tp'), may hold values from 0.5 to 2
- w_out: bfloat16 [2048, 4096], P(None, 'tp'), may hold values from -0.5 to 0.5
Outputs:
- mixed: bfloat16 [3072, 4096], P(('grp', 'sp', 'tp')), parts along dimension 0
There are 2 independent parts, one for each index of `grp`. A program takes and returns all parts, laid end to end along the dimension named above; an argument that names none is the same for every part. Nothing has to cross between parts.
All inputs are finite; a program needn't handle non-finite values.
Results may differ from a plain program's by a relative error of at most 0.01345.
The roundings to bfloat16 on the way count: a program that leaves them out, or rounds other values in their place, can miss the bound.
Values may be sent and summed in bfloat16 or wider, within the bound.
No kernel may reach another device: no remote copies, remote signals or barrier semaphores. Data moves between devices by JAX's collectives and lax.ppermute only.
A program may use at most 64 MiB of HBM per device.

v0:
```python
import functools

import jax
import jax.numpy as jnp
from jax import lax
from jax.experimental import pallas as pl
from jax.experimental.pallas import tpu as pltpu
from jax.sharding import PartitionSpec as P


PLAIN_QK_DIM = 64
ROTARY_DIM = 32
VALUE_DIM = 64
GRID_W = 64
LANES = 128
LOG2E = 1.4426950408889634

EPSILON = 1e-06


VMEM = pltpu.VMEM
SMEM = pltpu.SMEM


def in_vmem():
    return pl.BlockSpec(memory_space=VMEM)


def in_smem():
    return pl.BlockSpec(memory_space=SMEM)


def f32_dot(a, b):
    return jnp.dot(a, b, preferred_element_type=jnp.float32)


def swap(value, axis, bit):
    count = lax.axis_size(axis)
    return lax.ppermute(value, axis, [(i, i ^ bit) for i in range(count)])


def is_small(count):
    return count <= 4


def tp_bits(count):
    bits = []
    bit = 2
    while bit < count:
        bits.append(bit)
        bit *= 2
    if count > 1:
        bits.append(1)
    return bits


def spread(value, axis="tp"):
    if not is_small(lax.axis_size(axis)):
        return list(lax.all_gather(value, axis))
    got = {0: value}
    for bit in tp_bits(lax.axis_size(axis)):
        for member in list(got):
            got[member ^ bit] = swap(got[member], axis, bit)
    return [got[member] for member in range(len(got))]


def add_up(value, axis):
    count = lax.axis_size(axis)
    if not is_small(count):
        return lax.psum(value, axis)
    bit = 1
    while bit < count:
        value = value + swap(value, axis, bit)
        bit *= 2
    return value


def place(pieces, ids, axis):
    width = pieces[0].shape[axis]
    shape = list(pieces[0].shape)
    shape[axis] = width * len(pieces)
    whole = jnp.zeros(shape, pieces[0].dtype)
    for member, piece in enumerate(pieces):
        whole = lax.dynamic_update_slice_in_dim(whole, piece, ids[member] * width, axis)
    return whole


def turn_tables(positions, lanes):
    freq_count = ROTARY_DIM // 4
    inverse = 10000.0 ** (-jnp.arange(freq_count, dtype=jnp.float32) / freq_count)
    grid_row = (positions // GRID_W).astype(jnp.float32)
    grid_col = (positions % GRID_W).astype(jnp.float32)
    cosines, sines = [], []
    for coordinate in (grid_row, grid_col):
        angles = coordinate[:, None] * inverse[None, :]
        cosine, sine_of = jnp.cos(angles), jnp.sin(angles)
        cosines += [cosine, cosine]
        sines += [-sine_of, sine_of]
    cosine = jnp.concatenate(cosines, axis=1)
    sine_of = jnp.concatenate(sines, axis=1)
    repeat = lanes // ROTARY_DIM
    return jnp.tile(cosine, (1, repeat)), jnp.tile(sine_of, (1, repeat))


def turn(values, cosine, sine_of):
    freq_count = ROTARY_DIM // 4
    lanes = values.shape[1]
    lane = lax.broadcasted_iota(jnp.int32, values.shape, 1)
    first = (lane % (2 * freq_count)) < freq_count
    partner = jnp.where(
        first, pltpu.roll(values, lanes - freq_count, 1), pltpu.roll(values, freq_count, 1)
    )
    return values * cosine + partner * sine_of


def gather_rows(scratch, ids, pieces):
    width = pieces[0].shape[1]
    for number, piece in enumerate(pieces):
        scratch[:, pl.ds(pl.multiple_of(ids[number] * width, LANES), width)] = piece[...]


def normalize(values):
    center = values - jnp.mean(values, axis=-1, keepdims=True)
    spread_of = jnp.mean(center * center, axis=-1, keepdims=True)
    return center * lax.rsqrt(spread_of + EPSILON)


def weights_kernel(wq_hbm, wk_ref, rope_ref, wq_ref, wkr_ref, sem):
    copy = pltpu.make_async_copy(wq_hbm, wq_ref, sem)
    copy.start()
    wkr_ref[:, LANES:] = wk_ref[...]
    copies = (
        lax.broadcasted_iota(jnp.int32, (ROTARY_DIM, LANES), 0)
        == lax.broadcasted_iota(jnp.int32, (ROTARY_DIM, LANES), 1) % ROTARY_DIM
    ).astype(jnp.bfloat16)
    wkr_ref[:, :LANES] = lax.dot_general(
        rope_ref[...], copies, (((0,), (0,)), ((), ())), preferred_element_type=jnp.float32
    ).astype(jnp.bfloat16)
    copy.wait()


def early_kernel(count, *refs):
    for source, out_ref in zip(refs[:count], refs[count:]):
        for row in range(0, source.shape[0], 16):
            values = source[row : row + 16, :].astype(jnp.float32)
            out_ref[row : row + 16, :] = normalize(values)


def fetch_kernel(wq_ref, wk_hbm, wv_ref, wo_hbm, wqt_ref, wk_ref, wvt_ref, wo_ref, sems):
    copies = [
        pltpu.make_async_copy(wk_hbm, wk_ref, sems.at[0]),
        pltpu.make_async_copy(wo_hbm, wo_ref, sems.at[1]),
    ]
    for copy in copies:
        copy.start()
    wqt_ref[...] = wq_ref[...].astype(jnp.float32).T.astype(jnp.bfloat16)
    wvt_ref[...] = wv_ref[...].astype(jnp.float32).T.astype(jnp.bfloat16)
    for copy in copies:
        copy.wait()


def down_kernel(early_rows, late_rows, mod_count, tok_count, merged, *refs):
    ids, offsets = refs[:2]
    refs = refs[2:]
    early, refs = refs[: len(early_rows)], refs[len(early_rows) :]
    late, refs = refs[: len(late_rows)], refs[len(late_rows) :]
    pieces, refs = refs[:mod_count], refs[mod_count:]
    ctx_ref, wq_ref, wkr_ref, cos_ref, sin_ref = refs[:5]
    cq_ref, kv_ref, kr_ref, ha_ref, hb_ref, mod_ref, both_ref = refs[5:]
    step = 16
    gather_rows(mod_ref, ids, pieces)

    def modulate(source, target, base, rows, is_ctx, is_normed):
        shift_by = mod_ref[is_ctx : is_ctx + 1, :]
        scale_by = 1.0 + mod_ref[2 + is_ctx : 3 + is_ctx, :]
        for row in range(0, rows, step):
            values = source[row : row + step, :]
            if not is_normed:
                values = normalize(values.astype(jnp.float32))
            target[base + row : base + row + step, :] = (values * scale_by + shift_by).astype(
                jnp.bfloat16
            )

    def multiply(source, rows_of, first, with_ctx):
        cq = f32_dot(source[...], wq_ref[...])
        both = f32_dot(source[...], wkr_ref[...])
        base = 0
        for number, rows in enumerate(rows_of):
            start = pl.multiple_of(offsets[first + number] * rows, 16)
            cq_ref[pl.ds(start, rows), :] = cq[base : base + rows].astype(jnp.bfloat16)
            both_ref[pl.ds(start, rows), :] = both[base : base + rows]
            base += rows
        if with_ctx:
            both_ref[tok_count:, :] = both[base:]

    base = 0
    for source, rows in zip(early, early_rows):
        modulate(source, ha_ref, base, rows, 0, True)
        base += rows
    modulate(ctx_ref, ha_ref, base, ctx_ref.shape[0], 1, True)
    multiply(ha_ref, early_rows, 0, True)
    base = 0
    for source, rows in zip(late, late_rows):
        modulate(source, hb_ref, base, rows, 0, False)
        base += rows
    multiply(hb_ref, late_rows, len(early_rows), False)
    seg = both_ref.shape[0]
    kv_ref[:seg, :] = both_ref[:, LANES:].astype(jnp.bfloat16)
    turned = turn(both_ref[:, :LANES], cos_ref[...], sin_ref[...]).astype(jnp.bfloat16)
    if merged:
        both_ref[:, :LANES] = turned.astype(jnp.float32)
        quarter = seg // mod_count
        sub = quarter // (LANES // ROTARY_DIM)
        lane = lax.broadcasted_iota(jnp.int32, (sub, LANES), 1)
        packed = None
        for part in range(LANES // ROTARY_DIM):
            start = pl.multiple_of(ids[0] * quarter + part * sub, 8)
            rows = both_ref[pl.ds(start, sub), :LANES]
            rows = jnp.where(lane // ROTARY_DIM == part, rows, 0.0)
            packed = rows if packed is None else packed + rows
        kv_ref[seg:, :] = packed.astype(jnp.bfloat16)
        kr_ref[...] = jnp.zeros_like(kr_ref)
    else:
        kr_ref[...] = turned


def normed_into(scratch, ids, pieces, gain_ref):
    width = pieces[0].shape[1]
    rows = scratch.shape[0]
    total = width * len(pieces)
    squares = None
    for piece in pieces:
        values = piece[:rows, :].astype(jnp.float32)
        part = jnp.sum(values * values, axis=-1, keepdims=True)
        squares = part if squares is None else squares + part
    factor = lax.rsqrt(squares / total + EPSILON)
    for number, piece in enumerate(pieces):
        if len(pieces) == 1:
            where = slice(None)
        else:
            where = pl.ds(pl.multiple_of(ids[number] * width, LANES), width)
        gained = piece[:rows, :].astype(jnp.float32) * factor * gain_ref[:, where]
        scratch[:, where] = gained.astype(jnp.bfloat16)


def query_kernel(count, *refs):
    ids = refs[0]
    pieces = refs[1 : 1 + count]
    gain_ref, w_ref, table_ref, q_ref, scratch = refs[1 + count :]
    normed_into(scratch, ids, pieces, gain_ref)
    rows = scratch.shape[0]
    raw = lax.dot_general(
        w_ref[...], scratch[...], (((1,), (1,)), ((), ())), preferred_element_type=jnp.float32
    )
    freq_count = ROTARY_DIM // 4
    tables = [table_ref[i * freq_count : (i + 1) * freq_count, :] for i in range(4)]
    span = PLAIN_QK_DIM + ROTARY_DIM
    q_ref[...] = jnp.zeros_like(q_ref)
    for head in range(2 * q_ref.shape[0]):
        half = head % 2
        lanes = slice(half * rows, (half + 1) * rows)
        start = head * span
        q_ref[head // 2, half * PLAIN_QK_DIM : (half + 1) * PLAIN_QK_DIM, lanes] = raw[
            start : start + PLAIN_QK_DIM
        ].astype(jnp.bfloat16)
        start += PLAIN_QK_DIM
        parts = [raw[start + i * freq_count : start + (i + 1) * freq_count] for i in range(4)]
        turned = []
        for axis in range(2):
            low, high = parts[2 * axis : 2 * axis + 2]
            cosine, sine_of = tables[2 * axis : 2 * axis + 2]
            turned += [low * cosine - high * sine_of, low * sine_of + high * cosine]
        q_ref[head // 2, LANES : LANES + ROTARY_DIM, lanes] = jnp.concatenate(
            turned, axis=0
        ).astype(jnp.bfloat16)


def fold_rows(values):
    return jnp.sum(values.reshape(-1, 8, values.shape[1]), axis=0)


def attend_kernel(counts, tok_keys, seg, merged, first, last, *refs):
    ids, bias_ref, q_ref, gain_ref, wk_ref, wv_ref = refs[:6]
    refs = refs[6:]
    blocks = []
    for count in counts:
        blocks.append(refs[: count + (0 if merged else 1)])
        refs = refs[len(blocks[-1]) :]
    if not first:
        state_in, refs = refs[:3], refs[3:]
    if last:
        out_ref, refs = refs[0], refs[1:]
    else:
        state_out, refs = refs[:3], refs[3:]
    scratch, k_ref, v_ref, r_ref = refs
    pairs, _, lanes = q_ref.shape
    rows = lanes // 2
    for number, block in enumerate(blocks):
        pieces = block if merged else block[:-1]
        base = number * seg
        normed_into(scratch, ids, pieces, gain_ref)
        k_ref[base : base + seg, :] = f32_dot(scratch[...], wk_ref[...]).astype(jnp.bfloat16)
        v_ref[number] = lax.dot_general(
            wv_ref[...], scratch[...], (((1,), (1,)), ((), ())), preferred_element_type=jnp.float32
        ).astype(jnp.bfloat16)
        if merged:
            quarter = seg // len(pieces)
            sub = quarter // (LANES // ROTARY_DIM)
            for member, piece in enumerate(pieces):
                packed = piece[seg:, :].astype(jnp.float32)
                for part in range(LANES // ROTARY_DIM):
                    moved = pltpu.roll(packed, (-part * ROTARY_DIM) % LANES, 1) if part else packed
                    start = pl.multiple_of(base + ids[member] * quarter + part * sub, 16)
                    r_ref[pl.ds(start, sub), :] = moved.astype(jnp.bfloat16)
        else:
            r_ref[base : base + seg, :] = block[-1][...]
    score_scale = (PLAIN_QK_DIM + ROTARY_DIM) ** (-0.5) * LOG2E
    lane = lax.broadcasted_iota(jnp.int32, (1, lanes), 1)
    for pair in range(pairs):
        span = slice(pair * LANES, (pair + 1) * LANES)
        bias = jnp.where(lane < rows, bias_ref[2 * pair], bias_ref[2 * pair + 1]) * LOG2E
        top = total = acc = None
        if not first:
            top = state_in[0][pair, :1, :]
            total, acc = state_in[1][pair], state_in[2][pair]
        for number in range(len(blocks)):
            base = number * seg
            key = jnp.concatenate(
                [k_ref[base : base + seg, span], r_ref[base : base + seg, :]], axis=1
            )
            scores = f32_dot(key, q_ref[pair])
            lat, ctx = scores[:tok_keys], scores[tok_keys:]
            peak = jnp.maximum(
                jnp.max(lat, axis=0, keepdims=True) * score_scale,
                jnp.max(ctx, axis=0, keepdims=True) * score_scale + bias,
            )
            new_top = peak if top is None else jnp.maximum(top, peak)
            e_lat = jnp.exp2(lat * score_scale - new_top)
            e_ctx = jnp.exp2(ctx * score_scale - (new_top - bias))
            part = fold_rows(e_lat) + fold_rows(e_ctx)
            weights = jnp.concatenate([e_lat, e_ctx], axis=0).astype(jnp.bfloat16)
            both = f32_dot(v_ref[number, span, :], weights)
            gathered = jnp.concatenate([both[:VALUE_DIM, :rows], both[VALUE_DIM:, rows:]], axis=0)
            if top is None:
                total, acc = part, gathered
            else:
                rescale = jnp.exp2(top - new_top)
                total = total * rescale + part
                acc = gathered + jnp.concatenate(
                    [acc[:VALUE_DIM] * rescale[:, :rows], acc[VALUE_DIM:] * rescale[:, rows:]],
                    axis=0,
                )
            top = new_top
        if last:
            total = jnp.sum(total, axis=0, keepdims=True)
            done = jnp.concatenate(
                [acc[:VALUE_DIM] / total[:, :rows], acc[VALUE_DIM:] / total[:, rows:]], axis=0
            )
            out_ref[:, span] = done.T.astype(jnp.bfloat16)
        else:
            state_out[0][pair] = jnp.broadcast_to(top, (8, lanes))
            state_out[1][pair] = total
            state_out[2][pair] = acc


def out_kernel(count, parts, *refs):
    ids = refs[0]
    pieces = refs[1 : 1 + count]
    w_ref = refs[1 + count]
    outs = refs[2 + count : 2 + count + parts]
    depth = pieces[0].shape[1]
    total = None
    for number, piece in enumerate(pieces):
        rows = pl.ds(pl.multiple_of(ids[number] * depth, LANES), depth)
        part = f32_dot(piece[...], w_ref[rows, :])
        total = part if total is None else total + part
    if parts == 1:
        outs[0][...] = total.astype(jnp.bfloat16)
        return
    scratch = refs[2 + count + parts]
    scratch[...] = total
    rows = outs[0].shape[0]
    for number, out_ref in enumerate(outs):
        start = pl.multiple_of(ids[number] * rows, 8)
        out_ref[...] = scratch[pl.ds(start, rows), :].astype(jnp.bfloat16)


def final_kernel(count, mod_count, *refs):
    ids = refs[0]
    pieces = refs[1 : 1 + count]
    gates = refs[1 + count : 1 + count + mod_count]
    lat_ref, out_ref = refs[1 + count + mod_count :]
    width = pieces[0].shape[1]
    for number, (piece, gate) in enumerate(zip(pieces, gates)):
        span = pl.ds(pl.multiple_of(ids[number] * width, LANES), width)
        out_ref[:, span] = (
            lat_ref[:, span].astype(jnp.float32)
            + gate[gate.shape[0] - 1 :, :] * piece[...].astype(jnp.float32)
        ).astype(jnp.bfloat16)


def call(kernel, outs, operands, smem=(0,), hbm=(), scratch=(), mib=16):
    specs = []
    for place_of in range(len(operands)):
        if place_of in hbm:
            specs.append(pl.BlockSpec(memory_space=pl.ANY))
        else:
            specs.append(in_smem() if place_of in smem else in_vmem())
    many = isinstance(outs, (list, tuple))
    return pl.pallas_call(
        kernel,
        out_shape=outs,
        in_specs=specs,
        out_specs=[in_vmem() for _ in outs] if many else in_vmem(),
        scratch_shapes=list(scratch),
        compiler_params=pltpu.CompilerParams(vmem_limit_bytes=mib * 1024 * 1024),
    )(*operands)


def on_device(
    latents,
    conditions,
    context,
    w_shift,
    w_scale,
    w_gate,
    w_qdown,
    w_kvdown,
    w_rope,
    q_gain,
    latent_norm_gain,
    query_up_weight,
    key_up_weight,
    value_up_weight,
    context_bias,
    w_out,
):
    tp_count = lax.axis_size("tp")
    sp_count = lax.axis_size("sp")
    tp_index = lax.axis_index("tp")
    sp_index = lax.axis_index("sp")
    own_rows, width = latents.shape
    tok_count = own_rows * tp_count
    ctx_rows = context.shape[0]
    seg_rows = tok_count + ctx_rows
    ids = jnp.arange(tp_count, dtype=jnp.int32)
    if is_small(tp_count):
        ids = jnp.bitwise_xor(tp_index, ids)
    bf16 = jnp.bfloat16

    small = is_small(tp_count)
    shape_of = jax.ShapeDtypeStruct

    lat_blocks = spread(latents)
    cond_act = jax.nn.silu(conditions).astype(bf16)
    partial_mod = jnp.concatenate(
        [f32_dot(cond_act, w_shift), f32_dot(cond_act, w_scale), f32_dot(cond_act[0:1], w_gate)],
        axis=0,
    )
    mod_pieces = spread(add_up(partial_mod, "sp"))

    head_count = query_up_weight.shape[1] // (PLAIN_QK_DIM + ROTARY_DIM)
    pairs = head_count // 2
    q_pos = sp_index * tok_count + jnp.arange(tok_count, dtype=jnp.int32)
    cosine, sine_of = turn_tables(q_pos, LANES)
    k_cosine = jnp.concatenate([cosine, jnp.ones((ctx_rows, LANES), jnp.float32)], axis=0)
    k_sine = jnp.concatenate([sine_of, jnp.zeros((ctx_rows, LANES), jnp.float32)], axis=0)
    freq = ROTARY_DIM // 4
    q_table = jnp.concatenate(
        [
            cosine[:, :freq],
            sine_of[:, freq : 2 * freq],
            cosine[:, 2 * freq : 3 * freq],
            sine_of[:, 3 * freq : 4 * freq],
        ],
        axis=1,
    ).T
    kv_cols = w_kvdown.shape[1]
    q_cols = w_qdown.shape[1]

    w_q, w_kr = call(
        weights_kernel,
        [shape_of(w_qdown.shape, bf16), shape_of((width, LANES + kv_cols), bf16)],
        [w_qdown, w_kvdown, w_rope.T],
        smem=(),
        hbm=(0,),
        scratch=[pltpu.SemaphoreType.DMA],
    )
    block_ids = ids
    if own_rows % 16 or not small:
        lat_blocks = [place(lat_blocks, ids, 0)]
        block_ids = jnp.zeros((1,), jnp.int32)
        order = [0]
    else:
        order = [0, 1] + list(range(2, tp_count)) if tp_count > 1 else [0]
    early_of = [lat_blocks[member] for member in order[:2]] if len(order) > 2 else []
    late_of = [lat_blocks[member] for member in order[len(early_of) :]]
    normed = call(
        functools.partial(early_kernel, len(early_of) + 1),
        [shape_of(value.shape, jnp.float32) for value in [*early_of, context]],
        [*early_of, context],
        smem=(),
        mib=12,
    )
    w_qt, w_k, w_vt, w_o = call(
        fetch_kernel,
        [
            shape_of(query_up_weight.shape[::-1], bf16),
            shape_of(key_up_weight.shape, bf16),
            shape_of(value_up_weight.shape[::-1], bf16),
            shape_of(w_out.shape, bf16),
        ],
        [query_up_weight, key_up_weight, value_up_weight, w_out],
        smem=(),
        hbm=(1, 3),
        scratch=[pltpu.SemaphoreType.DMA((2,))],
    )
    merged = (
        kv_cols % LANES == 0
        and seg_rows % (16 * tp_count * LANES // ROTARY_DIM) == 0
        and small
        and is_small(sp_count)
    )
    extra = seg_rows // tp_count * ROTARY_DIM // LANES if merged else 0
    late_rows = [value.shape[0] for value in late_of]
    early_rows = [value.shape[0] for value in early_of]
    cq_cols, kv_own, kr_own = call(
        functools.partial(down_kernel, early_rows, late_rows, tp_count, tok_count, merged),
        [
            shape_of((tok_count, q_cols), bf16),
            shape_of((seg_rows + extra, kv_cols), bf16),
            shape_of((16 if merged else seg_rows, LANES), bf16),
        ],
        [
            ids,
            block_ids,
            *normed[:-1],
            *late_of,
            *mod_pieces,
            normed[-1],
            w_q,
            w_kr,
            k_cosine,
            k_sine,
        ],
        smem=(0, 1),
        scratch=[
            VMEM((sum(early_rows) + ctx_rows, width), bf16),
            VMEM((sum(late_rows), width), bf16),
            VMEM((5, width), jnp.float32),
            VMEM((seg_rows, LANES + kv_cols), jnp.float32),
        ],
        mib=16,
    )

    def columns(value):
        pieces = spread(value)
        if value.shape[1] % LANES:
            return [place(pieces, ids, 1)]
        return pieces

    if is_small(sp_count):
        blocks = []
        for member in range(sp_count):
            moved = swap(kv_own, "sp", member) if member else kv_own
            block = columns(moved)
            if not merged:
                block.append(swap(kr_own, "sp", member) if member else kr_own)
            blocks.append(block)
    else:
        kr_blocks = lax.all_gather(kr_own, "sp")
        whole_rows = lax.all_gather(kv_own, "tp", axis=1, tiled=True)
        kv_blocks = lax.all_gather(whole_rows, "sp")
        blocks = [[kv, kr] for kv, kr in zip(kv_blocks, kr_blocks)]
    cq_pieces = columns(cq_cols)
    queries = call(
        functools.partial(query_kernel, len(cq_pieces)),
        shape_of((pairs, 2 * LANES, 2 * tok_count), bf16),
        [ids, *cq_pieces, q_gain[None, :], w_qt, q_table],
        scratch=[VMEM((tok_count, q_gain.shape[0]), bf16)],
    )
    held = [
        shape_of((pairs, 8, 2 * tok_count), jnp.float32),
        shape_of((pairs, 8, 2 * tok_count), jnp.float32),
        shape_of((pairs, LANES, tok_count), jnp.float32),
    ]
    state = []
    begin = 0
    while begin < sp_count:
        part = blocks[begin : begin + (1 if begin < 2 else 2)]
        first, last = begin == 0, begin + len(part) >= sp_count
        state = call(
            functools.partial(
                attend_kernel,
                [len(block) - (0 if merged else 1) for block in part],
                tok_count,
                seg_rows,
                merged,
                first,
                last,
            ),
            shape_of((tok_count, head_count * VALUE_DIM), bf16) if last else held,
            [
                ids,
                context_bias,
                queries,
                latent_norm_gain[None, :],
                w_k,
                w_vt,
                *[piece for block in part for piece in block],
                *state,
            ],
            smem=(0, 1),
            scratch=[
                VMEM((seg_rows, latent_norm_gain.shape[0]), bf16),
                VMEM((len(part) * seg_rows, head_count * PLAIN_QK_DIM), bf16),
                VMEM((len(part), head_count * VALUE_DIM, seg_rows), bf16),
                VMEM((len(part) * seg_rows, LANES), bf16),
            ],
            mib=16,
        )
        begin += len(part)
    att_pieces = spread(state)
    out_cols = w_out.shape[1]
    parts = tp_count if small and own_rows % 8 == 0 else 1
    proj = call(
        functools.partial(out_kernel, tp_count, parts),
        [shape_of((tok_count // parts, out_cols), bf16) for _ in range(parts)],
        [ids, *att_pieces, w_o],
        scratch=[VMEM((tok_count, out_cols), jnp.float32)] if parts > 1 else [],
    )
    if parts > 1:
        proj_pieces = [
            swap(value, "tp", member) if member else value
            for member, value in enumerate(proj)
        ]
    else:
        by_owner = proj[0].reshape(tp_count, own_rows, out_cols)
        proj_pieces = list(lax.all_to_all(by_owner, "tp", 0, 0))
        if small:
            proj_pieces = [
                lax.dynamic_index_in_dim(jnp.stack(proj_pieces), ids[member], 0, False)
                for member in range(tp_count)
            ]
    return call(
        functools.partial(final_kernel, tp_count, tp_count),
        shape_of((own_rows, width), bf16),
        [ids, *proj_pieces, *mod_pieces, latents],
    )


def solution(mesh):
    in_specs = (
        P(("grp", "sp", "tp"), None),
        P("grp", "sp"),
        P(("grp", "sp"), None),
        P("sp", "tp"),
        P("sp", "tp"),
        P("sp", "tp"),
        P(None, "tp"),
        P(None, "tp"),
        P(),
        P(),
        P(),
        P(None, "tp"),
        P(None, "tp"),
        P(None, "tp"),
        P("tp"),
        P(None, "tp"),
    )
    out_specs = P(("grp", "sp", "tp"), None)
    return jax.shard_map(
        on_device, mesh=mesh, in_specs=in_specs, out_specs=out_specs, check_vma=False
    )
```

profile of v0, /device:TPU:0, one launch (start us, length us, event | category | flops | bytes accessed | tf_op | source)
XLA Modules:
  0.0 130.6 jit_solution(947208289654266679)
XLA Ops:
  0.5 2.6 %collective-permute-start.1 = (bf16[96,4096]{1,0:T(8,128)(2,1)}, bf16[96,4096]{1,0:T(8,128)(2,1)}, u32[]{:S(2)}, u32[]{:S(2)}) collective-permute-start(bf16[96,4096]{1,0:T(8,128)(2,1)} %refs_9_.1), channel_id=1, source_target_pairs={{0,2},{1,3},{2,0},{3,1},{4,6},{5,7},{6,4},{7,5},{8,10},{9,11},{10,... | collective-permute-start | bytes 2359304 | tf_op jit(solution)/shard_map/ppermute | solution.py:39
  5.8 1.6 %collective-permute-start.3 = (f32[5,1024]{1,0:T(8,128)S(1)}, f32[5,1024]{1,0:T(8,128)S(1)}, u32[]{:S(2)}, u32[]{:S(2)}) collective-permute-start(f32[5,1024]{1,0:T(8,128)S(1)} %pad_maximum_fusion.2), channel_id=1, source_target_pairs={{0,4},{4,0},{8,12},{12,8},{1,5},{5,1},{9,13},{13,9},{2,6},{6,2},{1... | collective-permute-start | bytes 61448 | tf_op jit(solution)/shard_map/ppermute | solution.py:39
  7.5 14.0 %collective-permute-done.1.refs_4_ = bf16[96,4096]{1,0:T(8,128)(2,1)} collective-permute-done((bf16[96,4096]{1,0:T(8,128)(2,1)}, bf16[96,4096]{1,0:T(8,128)(2,1)}, u32[]{:S(2)}, u32[]{:S(2)}) %collective-permute-start.1) | collective-permute-done | bytes 786464 | tf_op jit(solution)/shard_map/ppermute | solution.py:39
  21.7 2.9 %collective-permute-start.4 = (f32[5,1024]{1,0:T(8,128)S(1)}, f32[5,1024]{1,0:T(8,128)S(1)}, u32[]{:S(2)}, u32[]{:S(2)}) collective-permute-start(f32[5,1024]{1,0:T(8,128)S(1)} %fusion.9), channel_id=1, source_target_pairs={{0,8},{4,12},{8,0},{12,4},{1,9},{5,13},{9,1},{13,5},{2,10},{6,14},... | collective-permute-start | bytes 61448 | tf_op jit(solution)/shard_map/ppermute | solution.py:39
  26.7 1.7 %collective-permute-start.6 = (f32[5,1024]{1,0:T(8,128)S(1)}, f32[5,1024]{1,0:T(8,128)S(1)}, u32[]{:S(2)}, u32[]{:S(2)}) collective-permute-start(f32[5,1024]{1,0:T(8,128)S(1)} %add.44.refs_6_.refs_5_), channel_id=1, source_target_pairs={{0,2},{1,3},{2,0},{3,1},{4,6},{5,7},{6,4},{7,5},{8,10},{9,11},{10,... | collective-permute-start | bytes 61448 | tf_op jit(solution)/shard_map/ppermute | solution.py:39
  29.0 1.6 %collective-permute-done.6.refs_8_.refs_7_ = f32[5,1024]{1,0:T(8,128)S(1)} collective-permute-done((f32[5,1024]{1,0:T(8,128)S(1)}, f32[5,1024]{1,0:T(8,128)S(1)}, u32[]{:S(2)}, u32[]{:S(2)}) %collective-permute-start.6) | collective-permute-done | bytes 20512 | tf_op jit(solution)/shard_map/ppermute | solution.py:39
  32.1 1.7 %copy.20 = f32[384,128]{1,0:T(8,128)} copy(f32[384,128]{0,1:T(8,128)} %bitcast.23) | data formatting | bytes 393216
  35.3 1.7 %copy.19 = f32[384,128]{1,0:T(8,128)} copy(f32[384,128]{0,1:T(8,128)} %bitcast.21) | data formatting | bytes 393216
  39.0 1.6 %copy-done.3 = bf16[4096,256]{1,0:T(8,128)(2,1)S(1)} copy-done((bf16[4096,256]{1,0:T(8,128)(2,1)S(1)}, bf16[4096,256]{1,0:T(8,128)(2,1)}, u32[]{:S(2)}) %copy-start.3) | copy-done | bytes 2097176
  41.9 2.7 %shard_map.154 = (f32[96,4096]{1,0:T(8,128)S(1)}, f32[96,4096]{1,0:T(8,128)S(1)}, f32[128,4096]{1,0:T(8,128)S(1)}) custom-call(bf16[96,4096]{1,0:T(8,128)(2,1)S(1)} %copy-done.2, bf16[96,4096]{1,0:T(8,128)(2,1)} %collective-permute-done.refs_1_, bf16[128,4096]{1,0:T(8,128)(2,1)S(1)} %copy-done.6), custom_call_target="tpu_custom_call" | custom-call | tf_op jit(solution)/shard_map/pallas_call | solution.py:410
  44.6 5.2 %shard_map.156 = (bf16[384,256]{1,0:T(8,128)(2,1)S(1)}, bf16[544,128]{1,0:T(8,128)(2,1)S(1)}, bf16[16,128]{1,0:T(8,128)(2,1)}) custom-call(s32[4]{0:T(128)S(1)} %iota_xor_fusion.refs_0_.refs_1_, s32[4]{0:T(128)S(1)} %iota_xor_fusion.refs_0_.refs_1_, f32[96,4096]{1,0:T(8,128)S(1)} %get-tuple-element.26.refs_2_, f32[96,4096]{1,0:T(8,128)S(1)} %get-tuple-element.27.refs_3_, ...), custom_call_target="tpu_custom_call" | custom-call | tf_op jit(solution)/shard_map/pallas_call | solution.py:410
  49.8 1.7 %collective-permute-start.24 = (bf16[544,128]{1,0:T(8,128)(2,1)S(1)}, bf16[544,128]{1,0:T(8,128)(2,1)S(1)}, u32[]{:S(2)}, u32[]{:S(2)}) collective-permute-start(bf16[544,128]{1,0:T(8,128)(2,1)S(1)} %get-tuple-element.35.refs_6_), channel_id=1, source_target_pairs={{0,2},{1,3},{2,0},{3,1},{4,6},{5,7},{6,4},{7,5},{8,10},{9,11},{10,... | collective-permute-start | bytes 417800 | tf_op jit(solution)/shard_map/ppermute | solution.py:39
  51.7 1.6 %collective-permute-start.19 = (bf16[544,128]{1,0:T(8,128)(2,1)S(1)}, bf16[544,128]{1,0:T(8,128)(2,1)S(1)}, u32[]{:S(2)}, u32[]{:S(2)}) collective-permute-start(bf16[544,128]{1,0:T(8,128)(2,1)S(1)} %get-tuple-element.35.refs_6_), channel_id=1, source_target_pairs={{0,4},{4,0},{8,12},{12,8},{1,5},{5,1},{9,13},{13,9},{2,6},{6,2},{1... | collective-permute-start | bytes 417800 | tf_op jit(solution)/shard_map/ppermute | solution.py:39
  53.8 2.1 %collective-permute-done.24.refs_8_ = bf16[544,128]{1,0:T(8,128)(2,1)S(1)} collective-permute-done((bf16[544,128]{1,0:T(8,128)(2,1)S(1)}, bf16[544,128]{1,0:T(8,128)(2,1)S(1)}, u32[]{:S(2)}, u32[]{:S(2)}) %collective-permute-start.24) | collective-permute-done | bytes 139296 | tf_op jit(solution)/shard_map/ppermute | solution.py:39
  56.0 2.7 %collective-permute-start.11 = (bf16[544,128]{1,0:T(8,128)(2,1)S(1)}, bf16[544,128]{1,0:T(8,128)(2,1)S(1)}, u32[]{:S(2)}, u32[]{:S(2)}) collective-permute-start(bf16[544,128]{1,0:T(8,128)(2,1)S(1)} %get-tuple-element.35.refs_6_), channel_id=1, source_target_pairs={{0,8},{4,12},{8,0},{12,4},{1,9},{5,13},{9,1},{13,5},{2,10},{6,14},... | collective-permute-start | bytes 417800 | tf_op jit(solution)/shard_map/ppermute | solution.py:39
  58.7 2.0 %collective-permute-start.15 = (bf16[544,128]{1,0:T(8,128)(2,1)S(1)}, bf16[544,128]{1,0:T(8,128)(2,1)S(1)}, u32[]{:S(2)}, u32[]{:S(2)}) collective-permute-start(bf16[544,128]{1,0:T(8,128)(2,1)S(1)} %get-tuple-element.35.refs_6_), channel_id=1, source_target_pairs={{0,12},{4,8},{8,4},{12,0},{1,13},{5,9},{9,5},{13,1},{2,14},{6,10},... | collective-permute-start | bytes 417800 | tf_op jit(solution)/shard_map/ppermute | solution.py:39
  60.6 8.7 %collective-permute-done.11.refs_6_ = bf16[544,128]{1,0:T(8,128)(2,1)S(1)} collective-permute-done((bf16[544,128]{1,0:T(8,128)(2,1)S(1)}, bf16[544,128]{1,0:T(8,128)(2,1)S(1)}, u32[]{:S(2)}, u32[]{:S(2)}) %collective-permute-start.11) | collective-permute-done | bytes 139296 | tf_op jit(solution)/shard_map/ppermute | solution.py:39
  69.4 1.7 %collective-permute-start.21 = (bf16[544,128]{1,0:T(8,128)(2,1)S(1)}, bf16[544,128]{1,0:T(8,128)(2,1)S(1)}, u32[]{:S(2)}, u32[]{:S(2)}) collective-permute-start(bf16[544,128]{1,0:T(8,128)(2,1)S(1)} %collective-permute-done.19.refs_6_), channel_id=1, source_target_pairs={{0,2},{1,3},{2,0},{3,1},{4,6},{5,7},{6,4},{7,5},{8,10},{9,11},{10,... | collective-permute-start | bytes 417800 | tf_op jit(solution)/shard_map/ppermute | solution.py:39
  71.5 1.7 %collective-permute-start.17 = (bf16[544,128]{1,0:T(8,128)(2,1)S(1)}, bf16[544,128]{1,0:T(8,128)(2,1)S(1)}, u32[]{:S(2)}, u32[]{:S(2)}) collective-permute-start(bf16[544,128]{1,0:T(8,128)(2,1)S(1)} %collective-permute-done.15.refs_10_), channel_id=1, source_target_pairs={{0,2},{1,3},{2,0},{3,1},{4,6},{5,7},{6,4},{7,5},{8,10},{9,11},{10,... | collective-permute-start | bytes 417800 | tf_op jit(solution)/shard_map/ppermute | solution.py:39
  75.7 2.3 %collective-permute-done.13.refs_8_ = bf16[544,128]{1,0:T(8,128)(2,1)S(1)} collective-permute-done((bf16[544,128]{1,0:T(8,128)(2,1)S(1)}, bf16[544,128]{1,0:T(8,128)(2,1)S(1)}, u32[]{:S(2)}, u32[]{:S(2)}) %collective-permute-start.13) | collective-permute-done | bytes 139296 | tf_op jit(solution)/shard_map/ppermute | solution.py:39
  78.0 2.4 %collective-permute-done.17.refs_12_ = bf16[544,128]{1,0:T(8,128)(2,1)S(1)} collective-permute-done((bf16[544,128]{1,0:T(8,128)(2,1)S(1)}, bf16[544,128]{1,0:T(8,128)(2,1)S(1)}, u32[]{:S(2)}, u32[]{:S(2)}) %collective-permute-start.17) | collective-permute-done | bytes 139296 | tf_op jit(solution)/shard_map/ppermute | solution.py:39
  82.9 2.1 %shard_map.158.refs_2_ = bf16[4,256,768]{2,1,0:T(8,128)(2,1)S(1)} custom-call(s32[4]{0:T(128)S(1)} %iota_xor_fusion.refs_0_.refs_1_, bf16[384,256]{1,0:T(8,128)(2,1)S(1)} %get-tuple-element.31.refs_1_, bf16[384,256]{1,0:T(8,128)(2,1)S(1)} %collective-permute-done.8.refs_2_, bf16[384,256]{1,0:T(8,128)(2,1)S(1)} %collective-permute-done.9.refs_3_, ...), custom_call_target="tpu_custom_call" | custom-call | tf_op jit(solution)/shard_map/pallas_call | solution.py:410
  85.0 4.3 %shard_map.159 = (f32[4,8,768]{2,1,0:T(8,128)S(1)}, f32[4,8,768]{2,1,0:T(8,128)S(1)}, f32[4,128,384]{2,1,0:T(8,128)S(1)}) custom-call(s32[4]{0:T(128)S(1)} %iota_xor_fusion.refs_0_.refs_1_, f32[8]{0:T(128)S(1)} %copy-done.11, bf16[4,256,768]{2,1,0:T(8,128)(2,1)S(1)} %shard_map.158.refs_2_, f32[1,512]{1,0:T(1,128)S(1)} %bitcast.17, ...), custom_call_target="tpu_custom_call" | custom-call | tf_op jit(solution)/shard_map/pallas_call | solution.py:410
  89.3 4.8 %shard_map.160 = (f32[4,8,768]{2,1,0:T(8,128)S(1)}, f32[4,8,768]{2,1,0:T(8,128)S(1)}, f32[4,128,384]{2,1,0:T(8,128)S(1)}) custom-call(s32[4]{0:T(128)S(1)} %iota_xor_fusion.refs_0_.refs_1_, f32[8]{0:T(128)S(1)} %copy-done.11, bf16[4,256,768]{2,1,0:T(8,128)(2,1)S(1)} %shard_map.158.refs_2_, f32[1,512]{1,0:T(1,128)S(1)} %bitcast.18, ...), custom_call_target="tpu_custom_call" | custom-call | tf_op jit(solution)/shard_map/pallas_call | solution.py:410
  94.2 8.5 %shard_map.161.refs_1_ = bf16[384,512]{1,0:T(8,128)(2,1)S(1)} custom-call(s32[4]{0:T(128)S(1)} %iota_xor_fusion.refs_0_.refs_1_, f32[8]{0:T(128)S(1)} %copy-done.11, bf16[4,256,768]{2,1,0:T(8,128)(2,1)S(1)} %shard_map.158.refs_2_, f32[1,512]{1,0:T(1,128)S(1)} %bitcast.19, bf16[512,512]{1,0:T(8,128)(2,1)S(1)} %get-tuple-element.33.refs_4_, ...), custom_call_target="tpu_custom_call" | custom-call | tf_op jit(solution)/shard_map/pallas_call | solution.py:410
  102.6 1.6 %collective-permute-start.27 = (bf16[384,512]{1,0:T(8,128)(2,1)S(1)}, bf16[384,512]{1,0:T(8,128)(2,1)S(1)}, u32[]{:S(2)}, u32[]{:S(2)}) collective-permute-start(bf16[384,512]{1,0:T(8,128)(2,1)S(1)} %shard_map.161.refs_1_), channel_id=1, source_target_pairs={{0,2},{1,3},{2,0},{3,1},{4,6},{5,7},{6,4},{7,5},{8,10},{9,11},{10,... | collective-permute-start | bytes 1179656 | tf_op jit(solution)/shard_map/ppermute | solution.py:39
  104.3 9.4 %collective-permute-done.27.refs_3_ = bf16[384,512]{1,0:T(8,128)(2,1)S(1)} collective-permute-done((bf16[384,512]{1,0:T(8,128)(2,1)S(1)}, bf16[384,512]{1,0:T(8,128)(2,1)S(1)}, u32[]{:S(2)}, u32[]{:S(2)}) %collective-permute-start.27) | collective-permute-done | bytes 393248 | tf_op jit(solution)/shard_map/ppermute | solution.py:39
  113.7 1.7 %collective-permute-done.28.refs_4_ = bf16[384,512]{1,0:T(8,128)(2,1)S(1)} collective-permute-done((bf16[384,512]{1,0:T(8,128)(2,1)S(1)}, bf16[384,512]{1,0:T(8,128)(2,1)S(1)}, u32[]{:S(2)}, u32[]{:S(2)}) %collective-permute-start.28) | collective-permute-done | bytes 393248 | tf_op jit(solution)/shard_map/ppermute | solution.py:39
  115.4 2.4 %shard_map.162 = (bf16[96,1024]{1,0:T(8,128)(2,1)S(1)}, bf16[96,1024]{1,0:T(8,128)(2,1)S(1)}, bf16[96,1024]{1,0:T(8,128)(2,1)S(1)}, bf16[96,1024]{1,0:T(8,128)(2,1)S(1)}) custom-call(s32[4]{0:T(128)S(1)} %iota_xor_fusion.refs_0_.refs_1_, bf16[384,512]{1,0:T(8,128)(2,1)S(1)} %shard_map.161.refs_1_, bf16[384,512]{1,0:T(8,128)(2,1)S(1)} %collective-permute-done.26.refs_2_, ...), custom_call_target="tpu_custom_call" | custom-call | tf_op jit(solution)/shard_map/pallas_call | solution.py:410
  119.8 6.0 %collective-permute-done.30.refs_3_ = bf16[96,1024]{1,0:T(8,128)(2,1)S(1)} collective-permute-done((bf16[96,1024]{1,0:T(8,128)(2,1)S(1)}, bf16[96,1024]{1,0:T(8,128)(2,1)S(1)}, u32[]{:S(2)}, u32[]{:S(2)}) %collective-permute-start.30) | collective-permute-done | bytes 196640 | tf_op jit(solution)/shard_map/ppermute | solution.py:39
  125.9 3.0 %collective-permute-done.31.refs_4_ = bf16[96,1024]{1,0:T(8,128)(2,1)S(1)} collective-permute-done((bf16[96,1024]{1,0:T(8,128)(2,1)S(1)}, bf16[96,1024]{1,0:T(8,128)(2,1)S(1)}, u32[]{:S(2)}, u32[]{:S(2)}) %collective-permute-start.31) | collective-permute-done | bytes 196640 | tf_op jit(solution)/shard_map/ppermute | solution.py:39
  128.9 1.7 %shard_map.163 = bf16[96,4096]{1,0:T(8,128)(2,1)} custom-call(s32[4]{0:T(128)S(1)} %iota_xor_fusion.refs_0_.refs_1_, bf16[96,1024]{1,0:T(8,128)(2,1)S(1)} %get-tuple-element.43.refs_1_, bf16[96,1024]{1,0:T(8,128)(2,1)S(1)} %collective-permute-done.29.refs_2_, bf16[96,1024]{1,0:T(8,128)(2,1)S(1)} %collective-permute-done.30.refs_3_, ...), custom_call_target="tpu_custom_call" | custom-call | tf_op jit(solution)/shard_map/pallas_call | solution.py:410
  (94 shorter events, 20.3 us)
Async XLA Ops:
  0.0 41.4 %collective-permute-start = (bf16[96,4096]{1,0:T(8,128)(2,1)}, bf16[96,4096]{1,0:T(8,128)(2,1)}, u32[]{:S(2)}, u32[]{:S(2)}) collective-permute-start(bf16[96,4096]{1,0:T(8,128)(2,1)} %refs_9_.1), channel_id=1, source_target_pairs={{0,1},{1,0},{2,3},{3,2},{4,5},{5,4},{6,7},{7,6},{8,9},{9,8},{10,11... | collective-permute-start | bytes 2359304 | tf_op jit(solution)/shard_map/ppermute | solution.py:39
  0.5 21.0 %collective-permute-start.1 = (bf16[96,4096]{1,0:T(8,128)(2,1)}, bf16[96,4096]{1,0:T(8,128)(2,1)}, u32[]{:S(2)}, u32[]{:S(2)}) collective-permute-start(bf16[96,4096]{1,0:T(8,128)(2,1)} %refs_9_.1), channel_id=1, source_target_pairs={{0,2},{1,3},{2,0},{3,1},{4,6},{5,7},{6,4},{7,5},{8,10},{9,11},{10,... | collective-permute-start | bytes 2359304 | tf_op jit(solution)/shard_map/ppermute | solution.py:39
  5.8 15.9 %collective-permute-start.3 = (f32[5,1024]{1,0:T(8,128)S(1)}, f32[5,1024]{1,0:T(8,128)S(1)}, u32[]{:S(2)}, u32[]{:S(2)}) collective-permute-start(f32[5,1024]{1,0:T(8,128)S(1)} %pad_maximum_fusion.2), channel_id=1, source_target_pairs={{0,4},{4,0},{8,12},{12,8},{1,5},{5,1},{9,13},{13,9},{2,6},{6,2},{1... | collective-permute-start | bytes 61448 | tf_op jit(solution)/shard_map/ppermute | solution.py:39
  21.5 23.1 %collective-permute-start.2 = (bf16[96,4096]{1,0:T(8,128)(2,1)}, bf16[96,4096]{1,0:T(8,128)(2,1)}, u32[]{:S(2)}, u32[]{:S(2)}) collective-permute-start(bf16[96,4096]{1,0:T(8,128)(2,1)} %collective-permute-done.1.refs_4_), channel_id=1, source_target_pairs={{0,1},{1,0},{2,3},{3,2},{4,5},{5,4},{6,7},{7,6},{8,9},{9,8},{10,11... | collective-permute-start | bytes 2359304 | tf_op jit(solution)/shard_map/ppermute | solution.py:39
  21.7 5.0 %collective-permute-start.4 = (f32[5,1024]{1,0:T(8,128)S(1)}, f32[5,1024]{1,0:T(8,128)S(1)}, u32[]{:S(2)}, u32[]{:S(2)}) collective-permute-start(f32[5,1024]{1,0:T(8,128)S(1)} %fusion.9), channel_id=1, source_target_pairs={{0,8},{4,12},{8,0},{12,4},{1,9},{5,13},{9,1},{13,5},{2,10},{6,14},... | collective-permute-start | bytes 61448 | tf_op jit(solution)/shard_map/ppermute | solution.py:39
  26.7 3.9 %collective-permute-start.6 = (f32[5,1024]{1,0:T(8,128)S(1)}, f32[5,1024]{1,0:T(8,128)S(1)}, u32[]{:S(2)}, u32[]{:S(2)}) collective-permute-start(f32[5,1024]{1,0:T(8,128)S(1)} %add.44.refs_6_.refs_5_), channel_id=1, source_target_pairs={{0,2},{1,3},{2,0},{3,1},{4,6},{5,7},{6,4},{7,5},{8,10},{9,11},{10,... | collective-permute-start | bytes 61448 | tf_op jit(solution)/shard_map/ppermute | solution.py:39
  29.0 15.6 %collective-permute-start.5 = (f32[5,1024]{1,0:T(8,128)S(1)}, f32[5,1024]{1,0:T(8,128)S(1)}, u32[]{:S(2)}, u32[]{:S(2)}) collective-permute-start(f32[5,1024]{1,0:T(8,128)S(1)} %add.44.refs_6_.refs_5_), channel_id=1, source_target_pairs={{0,1},{1,0},{2,3},{3,2},{4,5},{5,4},{6,7},{7,6},{8,9},{9,8},{10,11... | collective-permute-start | bytes 61448 | tf_op jit(solution)/shard_map/ppermute | solution.py:39
  30.6 14.0 %collective-permute-start.7 = (f32[5,1024]{1,0:T(8,128)S(1)}, f32[5,1024]{1,0:T(8,128)S(1)}, u32[]{:S(2)}, u32[]{:S(2)}) collective-permute-start(f32[5,1024]{1,0:T(8,128)S(1)} %collective-permute-done.6.refs_8_.refs_7_), channel_id=1, source_target_pairs={{0,1},{1,0},{2,3},{3,2},{4,5},{5,4},{6,7},{7,6},{8,9},{9,8},{10,11... | collective-permute-start | bytes 61448 | tf_op jit(solution)/shard_map/ppermute | solution.py:39
  49.8 6.1 %collective-permute-start.24 = (bf16[544,128]{1,0:T(8,128)(2,1)S(1)}, bf16[544,128]{1,0:T(8,128)(2,1)S(1)}, u32[]{:S(2)}, u32[]{:S(2)}) collective-permute-start(bf16[544,128]{1,0:T(8,128)(2,1)S(1)} %get-tuple-element.35.refs_6_), channel_id=1, source_target_pairs={{0,2},{1,3},{2,0},{3,1},{4,6},{5,7},{6,4},{7,5},{8,10},{9,11},{10,... | collective-permute-start | bytes 417800 | tf_op jit(solution)/shard_map/ppermute | solution.py:39
  51.5 7.2 %collective-permute-start.23 = (bf16[544,128]{1,0:T(8,128)(2,1)S(1)}, bf16[544,128]{1,0:T(8,128)(2,1)S(1)}, u32[]{:S(2)}, u32[]{:S(2)}) collective-permute-start(bf16[544,128]{1,0:T(8,128)(2,1)S(1)} %get-tuple-element.35.refs_6_), channel_id=1, source_target_pairs={{0,1},{1,0},{2,3},{3,2},{4,5},{5,4},{6,7},{7,6},{8,9},{9,8},{10,11... | collective-permute-start | bytes 417800 | tf_op jit(solution)/shard_map/ppermute | solution.py:39
  51.7 8.9 %collective-permute-start.19 = (bf16[544,128]{1,0:T(8,128)(2,1)S(1)}, bf16[544,128]{1,0:T(8,128)(2,1)S(1)}, u32[]{:S(2)}, u32[]{:S(2)}) collective-permute-start(bf16[544,128]{1,0:T(8,128)(2,1)S(1)} %get-tuple-element.35.refs_6_), channel_id=1, source_target_pairs={{0,4},{4,0},{8,12},{12,8},{1,5},{5,1},{9,13},{13,9},{2,6},{6,2},{1... | collective-permute-start | bytes 417800 | tf_op jit(solution)/shard_map/ppermute | solution.py:39
  53.3 17.8 %collective-permute-start.9 = (bf16[384,256]{1,0:T(8,128)(2,1)S(1)}, bf16[384,256]{1,0:T(8,128)(2,1)S(1)}, u32[]{:S(2)}, u32[]{:S(2)}) collective-permute-start(bf16[384,256]{1,0:T(8,128)(2,1)S(1)} %get-tuple-element.31.refs_1_), channel_id=1, source_target_pairs={{0,2},{1,3},{2,0},{3,1},{4,6},{5,7},{6,4},{7,5},{8,10},{9,11},{10,... | collective-permute-start | bytes 589832 | tf_op jit(solution)/shard_map/ppermute | solution.py:39
  53.8 17.6 %collective-permute-start.8 = (bf16[384,256]{1,0:T(8,128)(2,1)S(1)}, bf16[384,256]{1,0:T(8,128)(2,1)S(1)}, u32[]{:S(2)}, u32[]{:S(2)}) collective-permute-start(bf16[384,256]{1,0:T(8,128)(2,1)S(1)} %get-tuple-element.31.refs_1_), channel_id=1, source_target_pairs={{0,1},{1,0},{2,3},{3,2},{4,5},{5,4},{6,7},{7,6},{8,9},{9,8},{10,11... | collective-permute-start | bytes 589832 | tf_op jit(solution)/shard_map/ppermute | solution.py:39
  56.0 13.4 %collective-permute-start.11 = (bf16[544,128]{1,0:T(8,128)(2,1)S(1)}, bf16[544,128]{1,0:T(8,128)(2,1)S(1)}, u32[]{:S(2)}, u32[]{:S(2)}) collective-permute-start(bf16[544,128]{1,0:T(8,128)(2,1)S(1)} %get-tuple-element.35.refs_6_), channel_id=1, source_target_pairs={{0,8},{4,12},{8,0},{12,4},{1,9},{5,13},{9,1},{13,5},{2,10},{6,14},... | collective-permute-start | bytes 417800 | tf_op jit(solution)/shard_map/ppermute | solution.py:39
  58.7 12.4 %collective-permute-start.15 = (bf16[544,128]{1,0:T(8,128)(2,1)S(1)}, bf16[544,128]{1,0:T(8,128)(2,1)S(1)}, u32[]{:S(2)}, u32[]{:S(2)}) collective-permute-start(bf16[544,128]{1,0:T(8,128)(2,1)S(1)} %get-tuple-element.35.refs_6_), channel_id=1, source_target_pairs={{0,12},{4,8},{8,4},{12,0},{1,13},{5,9},{9,5},{13,1},{2,14},{6,10},... | collective-permute-start | bytes 417800 | tf_op jit(solution)/shard_map/ppermute | solution.py:39
  60.6 12.6 %collective-permute-start.25 = (bf16[544,128]{1,0:T(8,128)(2,1)S(1)}, bf16[544,128]{1,0:T(8,128)(2,1)S(1)}, u32[]{:S(2)}, u32[]{:S(2)}) collective-permute-start(bf16[544,128]{1,0:T(8,128)(2,1)S(1)} %collective-permute-done.24.refs_8_), channel_id=1, source_target_pairs={{0,1},{1,0},{2,3},{3,2},{4,5},{5,4},{6,7},{7,6},{8,9},{9,8},{10,11... | collective-permute-start | bytes 417800 | tf_op jit(solution)/shard_map/ppermute | solution.py:39
  69.4 5.8 %collective-permute-start.21 = (bf16[544,128]{1,0:T(8,128)(2,1)S(1)}, bf16[544,128]{1,0:T(8,128)(2,1)S(1)}, u32[]{:S(2)}, u32[]{:S(2)}) collective-permute-start(bf16[544,128]{1,0:T(8,128)(2,1)S(1)} %collective-permute-done.19.refs_6_), channel_id=1, source_target_pairs={{0,2},{1,3},{2,0},{3,1},{4,6},{5,7},{6,4},{7,5},{8,10},{9,11},{10,... | collective-permute-start | bytes 417800 | tf_op jit(solution)/shard_map/ppermute | solution.py:39
  71.1 4.1 %collective-permute-start.20 = (bf16[544,128]{1,0:T(8,128)(2,1)S(1)}, bf16[544,128]{1,0:T(8,128)(2,1)S(1)}, u32[]{:S(2)}, u32[]{:S(2)}) collective-permute-start(bf16[544,128]{1,0:T(8,128)(2,1)S(1)} %collective-permute-done.19.refs_6_), channel_id=1, source_target_pairs={{0,1},{1,0},{2,3},{3,2},{4,5},{5,4},{6,7},{7,6},{8,9},{9,8},{10,11... | collective-permute-start | bytes 417800 | tf_op jit(solution)/shard_map/ppermute | solution.py:39
  71.1 6.9 %collective-permute-start.13 = (bf16[544,128]{1,0:T(8,128)(2,1)S(1)}, bf16[544,128]{1,0:T(8,128)(2,1)S(1)}, u32[]{:S(2)}, u32[]{:S(2)}) collective-permute-start(bf16[544,128]{1,0:T(8,128)(2,1)S(1)} %collective-permute-done.11.refs_6_), channel_id=1, source_target_pairs={{0,2},{1,3},{2,0},{3,1},{4,6},{5,7},{6,4},{7,5},{8,10},{9,11},{10,... | collective-permute-start | bytes 417800 | tf_op jit(solution)/shard_map/ppermute | solution.py:39
  71.5 8.9 %collective-permute-start.17 = (bf16[544,128]{1,0:T(8,128)(2,1)S(1)}, bf16[544,128]{1,0:T(8,128)(2,1)S(1)}, u32[]{:S(2)}, u32[]{:S(2)}) collective-permute-start(bf16[544,128]{1,0:T(8,128)(2,1)S(1)} %collective-permute-done.15.refs_10_), channel_id=1, source_target_pairs={{0,2},{1,3},{2,0},{3,1},{4,6},{5,7},{6,4},{7,5},{8,10},{9,11},{10,... | collective-permute-start | bytes 417800 | tf_op jit(solution)/shard_map/ppermute | solution.py:39
  73.2 7.2 %collective-permute-start.10 = (bf16[384,256]{1,0:T(8,128)(2,1)S(1)}, bf16[384,256]{1,0:T(8,128)(2,1)S(1)}, u32[]{:S(2)}, u32[]{:S(2)}) collective-permute-start(bf16[384,256]{1,0:T(8,128)(2,1)S(1)} %collective-permute-done.9.refs_3_), channel_id=1, source_target_pairs={{0,1},{1,0},{2,3},{3,2},{4,5},{5,4},{6,7},{7,6},{8,9},{9,8},{10,11... | collective-permute-start | bytes 589832 | tf_op jit(solution)/shard_map/ppermute | solution.py:39
  75.2 18.9 %collective-permute-start.12 = (bf16[544,128]{1,0:T(8,128)(2,1)S(1)}, bf16[544,128]{1,0:T(8,128)(2,1)S(1)}, u32[]{:S(2)}, u32[]{:S(2)}) collective-permute-start(bf16[544,128]{1,0:T(8,128)(2,1)S(1)} %collective-permute-done.11.refs_6_), channel_id=1, source_target_pairs={{0,1},{1,0},{2,3},{3,2},{4,5},{5,4},{6,7},{7,6},{8,9},{9,8},{10,11... | collective-permute-start | bytes 417800 | tf_op jit(solution)/shard_map/ppermute | solution.py:39
  75.2 18.9 %collective-permute-start.16 = (bf16[544,128]{1,0:T(8,128)(2,1)S(1)}, bf16[544,128]{1,0:T(8,128)(2,1)S(1)}, u32[]{:S(2)}, u32[]{:S(2)}) collective-permute-start(bf16[544,128]{1,0:T(8,128)(2,1)S(1)} %collective-permute-done.15.refs_10_), channel_id=1, source_target_pairs={{0,1},{1,0},{2,3},{3,2},{4,5},{5,4},{6,7},{7,6},{8,9},{9,8},{10,11... | collective-permute-start | bytes 417800 | tf_op jit(solution)/shard_map/ppermute | solution.py:39
  78.0 11.3 %collective-permute-start.22 = (bf16[544,128]{1,0:T(8,128)(2,1)S(1)}, bf16[544,128]{1,0:T(8,128)(2,1)S(1)}, u32[]{:S(2)}, u32[]{:S(2)}) collective-permute-start(bf16[544,128]{1,0:T(8,128)(2,1)S(1)} %collective-permute-done.21.refs_8_), channel_id=1, source_target_pairs={{0,1},{1,0},{2,3},{3,2},{4,5},{5,4},{6,7},{7,6},{8,9},{9,8},{10,11... | collective-permute-start | bytes 417800 | tf_op jit(solution)/shard_map/ppermute | solution.py:39
  80.4 13.7 %collective-permute-start.14 = (bf16[544,128]{1,0:T(8,128)(2,1)S(1)}, bf16[544,128]{1,0:T(8,128)(2,1)S(1)}, u32[]{:S(2)}, u32[]{:S(2)}) collective-permute-start(bf16[544,128]{1,0:T(8,128)(2,1)S(1)} %collective-permute-done.13.refs_8_), channel_id=1, source_target_pairs={{0,1},{1,0},{2,3},{3,2},{4,5},{5,4},{6,7},{7,6},{8,9},{9,8},{10,11... | collective-permute-start | bytes 417800 | tf_op jit(solution)/shard_map/ppermute | solution.py:39
  80.4 13.7 %collective-permute-start.18 = (bf16[544,128]{1,0:T(8,128)(2,1)S(1)}, bf16[544,128]{1,0:T(8,128)(2,1)S(1)}, u32[]{:S(2)}, u32[]{:S(2)}) collective-permute-start(bf16[544,128]{1,0:T(8,128)(2,1)S(1)} %collective-permute-done.17.refs_12_), channel_id=1, source_target_pairs={{0,1},{1,0},{2,3},{3,2},{4,5},{5,4},{6,7},{7,6},{8,9},{9,8},{10,11... | collective-permute-start | bytes 417800 | tf_op jit(solution)/shard_map/ppermute | solution.py:39
  102.6 11.1 %collective-permute-start.27 = (bf16[384,512]{1,0:T(8,128)(2,1)S(1)}, bf16[384,512]{1,0:T(8,128)(2,1)S(1)}, u32[]{:S(2)}, u32[]{:S(2)}) collective-permute-start(bf16[384,512]{1,0:T(8,128)(2,1)S(1)} %shard_map.161.refs_1_), channel_id=1, source_target_pairs={{0,2},{1,3},{2,0},{3,1},{4,6},{5,7},{6,4},{7,5},{8,10},{9,11},{10,... | collective-permute-start | bytes 1179656 | tf_op jit(solution)/shard_map/ppermute | solution.py:39
  104.3 9.5 %collective-permute-start.26 = (bf16[384,512]{1,0:T(8,128)(2,1)S(1)}, bf16[384,512]{1,0:T(8,128)(2,1)S(1)}, u32[]{:S(2)}, u32[]{:S(2)}) collective-permute-start(bf16[384,512]{1,0:T(8,128)(2,1)S(1)} %shard_map.161.refs_1_), channel_id=1, source_target_pairs={{0,1},{1,0},{2,3},{3,2},{4,5},{5,4},{6,7},{7,6},{8,9},{9,8},{10,11... | collective-permute-start | bytes 1179656 | tf_op jit(solution)/shard_map/ppermute | solution.py:39
  113.7 1.7 %collective-permute-start.28 = (bf16[384,512]{1,0:T(8,128)(2,1)S(1)}, bf16[384,512]{1,0:T(8,128)(2,1)S(1)}, u32[]{:S(2)}, u32[]{:S(2)}) collective-permute-start(bf16[384,512]{1,0:T(8,128)(2,1)S(1)} %collective-permute-done.27.refs_3_), channel_id=1, source_target_pairs={{0,1},{1,0},{2,3},{3,2},{4,5},{5,4},{6,7},{7,6},{8,9},{9,8},{10,11... | collective-permute-start | bytes 1179656 | tf_op jit(solution)/shard_map/ppermute | solution.py:39
  117.9 1.9 %collective-permute-start.29 = (bf16[96,1024]{1,0:T(8,128)(2,1)S(1)}, bf16[96,1024]{1,0:T(8,128)(2,1)S(1)}, u32[]{:S(2)}, u32[]{:S(2)}) collective-permute-start(bf16[96,1024]{1,0:T(8,128)(2,1)S(1)} %get-tuple-element.44), channel_id=1, source_target_pairs={{0,1},{1,0},{2,3},{3,2},{4,5},{5,4},{6,7},{7,6},{8,9},{9,8},{10,11... | collective-permute-start | bytes 589832 | tf_op jit(solution)/shard_map/ppermute | solution.py:39
  118.1 7.8 %collective-permute-start.30 = (bf16[96,1024]{1,0:T(8,128)(2,1)S(1)}, bf16[96,1024]{1,0:T(8,128)(2,1)S(1)}, u32[]{:S(2)}, u32[]{:S(2)}) collective-permute-start(bf16[96,1024]{1,0:T(8,128)(2,1)S(1)} %get-tuple-element.45), channel_id=1, source_target_pairs={{0,2},{1,3},{2,0},{3,1},{4,6},{5,7},{6,4},{7,5},{8,10},{9,11},{10,... | collective-permute-start | bytes 589832 | tf_op jit(solution)/shard_map/ppermute | solution.py:39
  119.7 9.2 %collective-permute-start.31 = (bf16[96,1024]{1,0:T(8,128)(2,1)S(1)}, bf16[96,1024]{1,0:T(8,128)(2,1)S(1)}, u32[]{:S(2)}, u32[]{:S(2)}) collective-permute-start(bf16[96,1024]{1,0:T(8,128)(2,1)S(1)} %get-tuple-element.46), channel_id=1, source_target_pairs={{0,3},{1,2},{2,1},{3,0},{4,7},{5,6},{6,5},{7,4},{8,11},{9,10},{10,... | collective-permute-start | bytes 589832 | tf_op jit(solution)/shard_map/ppermute | solution.py:39
  (15 other events, 237.7 us)
where the time goes:
time: 131 us
  waiting for transfers between devices  54.2 us (41%)
  Pallas kernels  33.5 us (26%)
  starting transfers between devices  26.4 us (20%)
  local copies, waits for them, and re-layouts  12.8 us (10%)
  other arithmetic  2.21 us (2%)
    ppermute x32, waiting for transfers between devices, swap(): return lax.ppermute(value, axis, [(i, i ^ bit) for i in range(count)])  54.2 us
    pallas_call x10, Pallas kernels, call(): pl.pallas_call(kernel, out_shape=outs, in_specs=specs, out_specs=[in_vmem...  33.5 us
    ppermute x32, starting transfers between devices, swap(): return lax.ppermute(value, axis, [(i, i ^ bit) for i in range(count)])  26.4 us
    unnamed x32, local copies, waits for them, and re-layouts  6.36 us
    another operation x2, local copies, waits for them, and re-layouts, turn_tables(): return (jnp.tile(cosine, (1, repeat)), jnp.tile(sine_of, (1, repeat)))  2.97 us
  transfers between devices with their start and end apart: 32, of which 12 were waited for; matrix products, arithmetic and copies ran while one was open for 10% of the time, Pallas kernels for 12%

commit v1 on v0

--- a/solution.py
+++ b/solution.py
@@ -85,21 +85,33 @@
     return whole
 
 
-def turn_tables(positions, lanes):
+def angles(position, frequency, use_column):
     freq_count = ROTARY_DIM // 4
-    inverse = 10000.0 ** (-jnp.arange(freq_count, dtype=jnp.float32) / freq_count)
-    grid_row = (positions // GRID_W).astype(jnp.float32)
-    grid_col = (positions % GRID_W).astype(jnp.float32)
-    cosines, sines = [], []
-    for coordinate in (grid_row, grid_col):
-        angles = coordinate[:, None] * inverse[None, :]
-        cosine, sine_of = jnp.cos(angles), jnp.sin(angles)
-        cosines += [cosine, cosine]
-        sines += [-sine_of, sine_of]
-    cosine = jnp.concatenate(cosines, axis=1)
-    sine_of = jnp.concatenate(sines, axis=1)
-    repeat = lanes // ROTARY_DIM
-    return jnp.tile(cosine, (1, repeat)), jnp.tile(sine_of, (1, repeat))
+    inverse = jnp.zeros(frequency.shape, jnp.float32)
+    for number in range(freq_count):
+        inverse = jnp.where(
+            frequency == number, jnp.float32(10000.0 ** (-number / freq_count)), inverse
+        )
+    coordinate = jnp.where(use_column, position % GRID_W, position // GRID_W)
+    return coordinate.astype(jnp.float32) * inverse
+
+
+def tables_kernel(tok_count, info, cos_ref, sin_ref, table_ref):
+    freq_count = ROTARY_DIM // 4
+    start = info[0] * tok_count
+    shape = cos_ref.shape
+    row = lax.broadcasted_iota(jnp.int32, shape, 0)
+    lane = lax.broadcasted_iota(jnp.int32, shape, 1)
+    angle = angles(start + row, lane % freq_count, (lane // (2 * freq_count)) % 2 == 1)
+    is_lat = row < tok_count
+    cos_ref[...] = jnp.where(is_lat, jnp.cos(angle), 1.0)
+    sine_of = jnp.where((lane // freq_count) % 2 == 0, -jnp.sin(angle), jnp.sin(angle))
+    sin_ref[...] = jnp.where(is_lat, sine_of, 0.0)
+    shape = table_ref.shape
+    row = lax.broadcasted_iota(jnp.int32, shape, 0)
+    lane = lax.broadcasted_iota(jnp.int32, shape, 1)
+    angle = angles(start + lane, row % freq_count, row // (2 * freq_count) == 1)
+    table_ref[...] = jnp.where((row // freq_count) % 2 == 0, jnp.cos(angle), jnp.sin(angle))
 
 
 def turn(values, cosine, sine_of):
@@ -113,10 +125,26 @@
     return values * cosine + partner * sine_of
 
 
+class Members:
+    def __init__(self, info):
+        self.info = info
+
+    def __getitem__(self, member):
+        return self.info[1 + member]
+
+
+def member_ids(info, count):
+    return Members(info) if is_small(count) else list(range(count))
+
+
+def aligned(value, step):
+    return value if isinstance(value, int) else pl.multiple_of(value, step)
+
+
 def gather_rows(scratch, ids, pieces):
     width = pieces[0].shape[1]
     for number, piece in enumerate(pieces):
-        scratch[:, pl.ds(pl.multiple_of(ids[number] * width, LANES), width)] = piece[...]
+        scratch[:, pl.ds(aligned(ids[number] * width, LANES), width)] = piece[...]
 
 
 def normalize(values):
@@ -159,9 +187,9 @@
         copy.wait()
 
 
-def down_kernel(early_rows, late_rows, mod_count, tok_count, merged, *refs):
-    ids, offsets = refs[:2]
-    refs = refs[2:]
+def down_kernel(early_rows, late_rows, mod_count, tok_count, merged, info, *refs):
+    ids = member_ids(info, mod_count)
+    offsets = [0] if len(early_rows) + len(late_rows) == 1 else ids
     early, refs = refs[: len(early_rows)], refs[len(early_rows) :]
     late, refs = refs[: len(late_rows)], refs[len(late_rows) :]
     pieces, refs = refs[:mod_count], refs[mod_count:]
@@ -186,7 +214,7 @@
         both = f32_dot(source[...], wkr_ref[...])
         base = 0
         for number, rows in enumerate(rows_of):
-            start = pl.multiple_of(offsets[first + number] * rows, 16)
+            start = aligned(offsets[first + number] * rows, 16)
             cq_ref[pl.ds(start, rows), :] = cq[base : base + rows].astype(jnp.bfloat16)
             both_ref[pl.ds(start, rows), :] = both[base : base + rows]
             base += rows
@@ -214,7 +242,7 @@
         lane = lax.broadcasted_iota(jnp.int32, (sub, LANES), 1)
         packed = None
         for part in range(LANES // ROTARY_DIM):
-            start = pl.multiple_of(ids[0] * quarter + part * sub, 8)
+            start = aligned(ids[0] * quarter + part * sub, 8)
             rows = both_ref[pl.ds(start, sub), :LANES]
             rows = jnp.where(lane // ROTARY_DIM == part, rows, 0.0)
             packed = rows if packed is None else packed + rows
@@ -238,15 +266,15 @@
         if len(pieces) == 1:
             where = slice(None)
         else:
-            where = pl.ds(pl.multiple_of(ids[number] * width, LANES), width)
+            where = pl.ds(aligned(ids[number] * width, LANES), width)
         gained = piece[:rows, :].astype(jnp.float32) * factor * gain_ref[:, where]
         scratch[:, where] = gained.astype(jnp.bfloat16)
 
 
-def query_kernel(count, *refs):
-    ids = refs[0]
-    pieces = refs[1 : 1 + count]
-    gain_ref, w_ref, table_ref, q_ref, scratch = refs[1 + count :]
+def query_kernel(count, info, *refs):
+    ids = member_ids(info, count)
+    pieces = refs[:count]
+    gain_ref, w_ref, table_ref, q_ref, scratch = refs[count:]
     normed_into(scratch, ids, pieces, gain_ref)
     rows = scratch.shape[0]
     raw = lax.dot_general(
@@ -279,9 +307,10 @@
     return jnp.sum(values.reshape(-1, 8, values.shape[1]), axis=0)
 
 
-def attend_kernel(counts, tok_keys, seg, merged, first, last, *refs):
-    ids, bias_ref, q_ref, gain_ref, wk_ref, wv_ref = refs[:6]
-    refs = refs[6:]
+def attend_kernel(counts, tok_keys, seg, merged, first, last, info, *refs):
+    ids = member_ids(info, counts[0])
+    bias_ref, q_ref, gain_ref, wk_ref, wv_ref = refs[:5]
+    refs = refs[5:]
     blocks = []
     for count in counts:
         blocks.append(refs[: count + (0 if merged else 1)])
@@ -298,10 +327,11 @@
     for number, block in enumerate(blocks):
         pieces = block if merged else block[:-1]
         base = number * seg
-        normed_into(scratch, ids, pieces, gain_ref)
-        k_ref[base : base + seg, :] = f32_dot(scratch[...], wk_ref[...]).astype(jnp.bfloat16)
+        rows_ref = scratch.at[number]
+        normed_into(rows_ref, ids, pieces, gain_ref)
+        k_ref[base : base + seg, :] = f32_dot(rows_ref[...], wk_ref[...]).astype(jnp.bfloat16)
         v_ref[number] = lax.dot_general(
-            wv_ref[...], scratch[...], (((1,), (1,)), ((), ())), preferred_element_type=jnp.float32
+            wv_ref[...], rows_ref[...], (((1,), (1,)), ((), ())), preferred_element_type=jnp.float32
         ).astype(jnp.bfloat16)
         if merged:
             quarter = seg // len(pieces)
@@ -310,7 +340,7 @@
                 packed = piece[seg:, :].astype(jnp.float32)
                 for part in range(LANES // ROTARY_DIM):
                     moved = pltpu.roll(packed, (-part * ROTARY_DIM) % LANES, 1) if part else packed
-                    start = pl.multiple_of(base + ids[member] * quarter + part * sub, 16)
+                    start = aligned(base + ids[member] * quarter + part * sub, 16)
                     r_ref[pl.ds(start, sub), :] = moved.astype(jnp.bfloat16)
         else:
             r_ref[base : base + seg, :] = block[-1][...]
@@ -363,43 +393,43 @@
             state_out[2][pair] = acc
 
 
-def out_kernel(count, parts, *refs):
-    ids = refs[0]
-    pieces = refs[1 : 1 + count]
-    w_ref = refs[1 + count]
-    outs = refs[2 + count : 2 + count + parts]
+def out_kernel(count, parts, info, *refs):
+    ids = member_ids(info, count)
+    pieces = refs[:count]
+    w_ref = refs[count]
+    outs = refs[1 + count : 1 + count + parts]
     depth = pieces[0].shape[1]
     total = None
     for number, piece in enumerate(pieces):
-        rows = pl.ds(pl.multiple_of(ids[number] * depth, LANES), depth)
+        rows = pl.ds(aligned(ids[number] * depth, LANES), depth)
         part = f32_dot(piece[...], w_ref[rows, :])
         total = part if total is None else total + part
     if parts == 1:
         outs[0][...] = total.astype(jnp.bfloat16)
         return
-    scratch = refs[2 + count + parts]
+    scratch = refs[1 + count + parts]
     scratch[...] = total
     rows = outs[0].shape[0]
     for number, out_ref in enumerate(outs):
-        start = pl.multiple_of(ids[number] * rows, 8)
+        start = aligned(ids[number] * rows, 8)
         out_ref[...] = scratch[pl.ds(start, rows), :].astype(jnp.bfloat16)
 
 
-def final_kernel(count, mod_count, *refs):
-    ids = refs[0]
-    pieces = refs[1 : 1 + count]
-    gates = refs[1 + count : 1 + count + mod_count]
-    lat_ref, out_ref = refs[1 + count + mod_count :]
+def final_kernel(count, mod_count, info, *refs):
+    ids = member_ids(info, count)
+    pieces = refs[:count]
+    gates = refs[count : count + mod_count]
+    lat_ref, out_ref = refs[count + mod_count :]
     width = pieces[0].shape[1]
     for number, (piece, gate) in enumerate(zip(pieces, gates)):
-        span = pl.ds(pl.multiple_of(ids[number] * width, LANES), width)
+        span = pl.ds(aligned(ids[number] * width, LANES), width)
         out_ref[:, span] = (
             lat_ref[:, span].astype(jnp.float32)
             + gate[gate.shape[0] - 1 :, :] * piece[...].astype(jnp.float32)
         ).astype(jnp.bfloat16)
 
 
-def call(kernel, outs, operands, smem=(0,), hbm=(), scratch=(), mib=16):
+def call(kernel, outs, operands, smem=(), hbm=(), scratch=(), mib=16):
     specs = []
     for place_of in range(len(operands)):
         if place_of in hbm:
@@ -437,18 +467,19 @@
 ):
     tp_count = lax.axis_size("tp")
     sp_count = lax.axis_size("sp")
-    tp_index = lax.axis_index("tp")
-    sp_index = lax.axis_index("sp")
     own_rows, width = latents.shape
     tok_count = own_rows * tp_count
     ctx_rows = context.shape[0]
     seg_rows = tok_count + ctx_rows
-    ids = jnp.arange(tp_count, dtype=jnp.int32)
-    if is_small(tp_count):
-        ids = jnp.bitwise_xor(tp_index, ids)
+    small = is_small(tp_count)
+    members = jnp.arange(-1, tp_count, dtype=jnp.int32)
+    info = jnp.where(
+        members < 0, lax.axis_index("sp"), jnp.bitwise_xor(lax.axis_index("tp"), members)
+    )
+    info, conditions = lax.optimization_barrier((info, conditions))
+    ids = member_ids(info, tp_count)
     bf16 = jnp.bfloat16
 
-    small = is_small(tp_count)
     shape_of = jax.ShapeDtypeStruct
 
     lat_blocks = spread(latents)
@@ -461,20 +492,16 @@
 
     head_count = query_up_weight.shape[1] // (PLAIN_QK_DIM + ROTARY_DIM)
     pairs = head_count // 2
-    q_pos = sp_index * tok_count + jnp.arange(tok_count, dtype=jnp.int32)
-    cosine, sine_of = turn_tables(q_pos, LANES)
-    k_cosine = jnp.concatenate([cosine, jnp.ones((ctx_rows, LANES), jnp.float32)], axis=0)
-    k_sine = jnp.concatenate([sine_of, jnp.zeros((ctx_rows, LANES), jnp.float32)], axis=0)
-    freq = ROTARY_DIM // 4
-    q_table = jnp.concatenate(
+    k_cosine, k_sine, q_table = call(
+        functools.partial(tables_kernel, tok_count),
         [
-            cosine[:, :freq],
-            sine_of[:, freq : 2 * freq],
-            cosine[:, 2 * freq : 3 * freq],
-            sine_of[:, 3 * freq : 4 * freq],
+            shape_of((seg_rows, LANES), jnp.float32),
+            shape_of((seg_rows, LANES), jnp.float32),
+            shape_of((ROTARY_DIM, tok_count), jnp.float32),
         ],
-        axis=1,
-    ).T
+        [info],
+        smem=(0,),
+    )
     kv_cols = w_kvdown.shape[1]
     q_cols = w_qdown.shape[1]
 
@@ -482,14 +509,11 @@
         weights_kernel,
         [shape_of(w_qdown.shape, bf16), shape_of((width, LANES + kv_cols), bf16)],
         [w_qdown, w_kvdown, w_rope.T],
-        smem=(),
         hbm=(0,),
         scratch=[pltpu.SemaphoreType.DMA],
     )
-    block_ids = ids
     if own_rows % 16 or not small:
         lat_blocks = [place(lat_blocks, ids, 0)]
-        block_ids = jnp.zeros((1,), jnp.int32)
         order = [0]
     else:
         order = [0, 1] + list(range(2, tp_count)) if tp_count > 1 else [0]
@@ -499,7 +523,6 @@
         functools.partial(early_kernel, len(early_of) + 1),
         [shape_of(value.shape, jnp.float32) for value in [*early_of, context]],
         [*early_of, context],
-        smem=(),
         mib=12,
     )
     w_qt, w_k, w_vt, w_o = call(
@@ -511,7 +534,6 @@
             shape_of(w_out.shape, bf16),
         ],
         [query_up_weight, key_up_weight, value_up_weight, w_out],
-        smem=(),
         hbm=(1, 3),
         scratch=[pltpu.SemaphoreType.DMA((2,))],
     )
@@ -532,8 +554,7 @@
             shape_of((16 if merged else seg_rows, LANES), bf16),
         ],
         [
-            ids,
-            block_ids,
+            info,
             *normed[:-1],
             *late_of,
             *mod_pieces,
@@ -543,7 +564,7 @@
             k_cosine,
             k_sine,
         ],
-        smem=(0, 1),
+        smem=(0,),
         scratch=[
             VMEM((sum(early_rows) + ctx_rows, width), bf16),
             VMEM((sum(late_rows), width), bf16),
@@ -576,7 +597,8 @@
     queries = call(
         functools.partial(query_kernel, len(cq_pieces)),
         shape_of((pairs, 2 * LANES, 2 * tok_count), bf16),
-        [ids, *cq_pieces, q_gain[None, :], w_qt, q_table],
+        [info, *cq_pieces, q_gain[None, :], w_qt, q_table],
+        smem=(0,),
         scratch=[VMEM((tok_count, q_gain.shape[0]), bf16)],
     )
     held = [
@@ -601,7 +623,7 @@
             ),
             shape_of((tok_count, head_count * VALUE_DIM), bf16) if last else held,
             [
-                ids,
+                info,
                 context_bias,
                 queries,
                 latent_norm_gain[None, :],
@@ -612,7 +634,7 @@
             ],
             smem=(0, 1),
             scratch=[
-                VMEM((seg_rows, latent_norm_gain.shape[0]), bf16),
+                VMEM((len(part), seg_rows, latent_norm_gain.shape[0]), bf16),
                 VMEM((len(part) * seg_rows, head_count * PLAIN_QK_DIM), bf16),
                 VMEM((len(part), head_count * VALUE_DIM, seg_rows), bf16),
                 VMEM((len(part) * seg_rows, LANES), bf16),
@@ -626,7 +648,8 @@
     proj = call(
         functools.partial(out_kernel, tp_count, parts),
         [shape_of((tok_count // parts, out_cols), bf16) for _ in range(parts)],
-        [ids, *att_pieces, w_o],
+        [info, *att_pieces, w_o],
+        smem=(0,),
         scratch=[VMEM((tok_count, out_cols), jnp.float32)] if parts > 1 else [],
     )
     if parts > 1:
@@ -645,7 +668,8 @@
     return call(
         functools.partial(final_kernel, tp_count, tp_count),
         shape_of((own_rows, width), bf16),
-        [ids, *proj_pieces, *mod_pieces, latents],
+        [info, *proj_pieces, *mod_pieces, latents],
+        smem=(0,),
     )
 
 
@@ -669,6 +693,9 @@
         P(None, "tp"),
     )
     out_specs = P(("grp", "sp", "tp"), None)
-    return jax.shard_map(
+    step = jax.shard_map(
         on_device, mesh=mesh, in_specs=in_specs, out_specs=out_specs, check_vma=False
     )
+    if not (is_small(mesh.shape["tp"]) and is_small(mesh.shape["sp"])):
+        return step
+    return step

time: 131 us -> 126 us (0.962)
  local copies, waits for them, and re-layouts: 12.8 us -> 0.07 us
  waiting for transfers between devices: 54.2 us -> 59.9 us
  matrix products: 1.15 us -> 2.74 us
    unnamed x32 -> x28, local copies, waits for them, and re-layouts: 6.36 us -> 0.07 us
    ppermute x32, waiting for transfers between devices: 54.2 us -> 59.9 us  [swap(): return lax.ppermute(value, axis, [(i, i ^ bit) for i in range(count)])]
    another operation x2 -> x0, local copies, waits for them, and re-layouts: 2.97 us -> none  [turn_tables(): return (jnp.tile(cosine, (1, repeat)), jnp.tile(sine_of, (1, repeat)))]
    concatenate x2 -> x0, local copies, waits for them, and re-layouts: 1.96 us -> none  [the longest x1 1.02 us: on_device(): jnp.concatenate([sine_of, jnp.zeros((ctx_rows, LANES), jnp.float32)], axi...]
    dot_general x3, matrix products: 1.15 us -> 2.74 us  [f32_dot(): return jnp.dot(a, b, preferred_element_type=jnp.float32)]
    slice x2 -> x0, local copies, waits for them, and re-layouts: 1.45 us -> none  [the longest x1 0.73 us: on_device(): sine_of[:, freq:2 * freq]]
    pallas_call x10 -> x11, Pallas kernels: 33.5 us -> 34.2 us  [call(): pl.pallas_call(kernel, out_shape=outs, in_specs=specs, out_specs=[in_vmem...]
  transfers between devices with their start and end apart: 32 -> 32, of which waited for: 12 -> 13; matrix products, arithmetic and copies ran while one was open for 10% -> 3% of each run, Pallas kernels for 12% -> 14%
where the time goes in v1:
time: 126 us; the launch traced here: 125 us
  waiting for transfers between devices  59.9 us (48%)
  Pallas kernels  34.2 us (27%)
  starting transfers between devices  27.2 us (22%)
  matrix products  2.74 us (2%)
    ppermute x32, waiting for transfers between devices, swap(): return lax.ppermute(value, axis, [(i, i ^ bit) for i in range(count)])  59.9 us
    pallas_call x11, Pallas kernels, call(): pl.pallas_call(kernel, out_shape=outs, in_specs=specs, out_specs=[in_vmem...  34.2 us
    ppermute x32, starting transfers between devices, swap(): return lax.ppermute(value, axis, [(i, i ^ bit) for i in range(count)])  27.2 us
    dot_general x3, matrix products, f32_dot(): return jnp.dot(a, b, preferred_element_type=jnp.float32)  2.74 us
  transfers between devices with their start and end apart: 32, of which 13 were waited for; matrix products, arithmetic and copies ran while one was open for 3% of the time, Pallas kernels for 14%

profile of v1, /device:TPU:0, one launch (start us, length us, event | category | flops | bytes accessed | tf_op | source)
XLA Modules:
  0.0 125.3 jit_solution(8998665455446150774)
XLA Ops:
  0.0 3.0 %collective-permute-start.1 = (bf16[96,4096]{1,0:T(8,128)(2,1)}, bf16[96,4096]{1,0:T(8,128)(2,1)S(1)}, u32[]{:S(2)}, u32[]{:S(2)}) collective-permute-start(bf16[96,4096]{1,0:T(8,128)(2,1)} %refs_8_.1), channel_id=1, source_target_pairs={{0,2},{1,3},{2,0},{3,1},{4,6},{5,7},{6,4},{7,5},{8,10},{9,11},{10,... | collective-permute-start | bytes 2359304 | tf_op jit(solution)/shard_map/ppermute | solution.py:39
  4.3 16.5 %collective-permute-done.1.refs_2_ = bf16[96,4096]{1,0:T(8,128)(2,1)S(1)} collective-permute-done((bf16[96,4096]{1,0:T(8,128)(2,1)}, bf16[96,4096]{1,0:T(8,128)(2,1)S(1)}, u32[]{:S(2)}, u32[]{:S(2)}) %collective-permute-start.1) | collective-permute-done | bytes 786464 | tf_op jit(solution)/shard_map/ppermute | solution.py:39
  21.1 2.0 %fusion.4 = f32[2,1024]{1,0:T(2,128)S(1)} fusion(bf16[2,1024]{1,0:T(2,128)(2,1)S(1)} %fusion, bf16[1024,1024]{1,0:T(8,128)(2,1)} %param.20), kind=kOutput, calls=%fused_computation.8 | convolution fusion | flops 4194304 | bytes 2109440 | tf_op jit(solution)/shard_map/dot_general | solution.py:34
  23.1 1.9 %collective-permute-start.3 = (f32[5,1024]{1,0:T(8,128)S(1)}, f32[5,1024]{1,0:T(8,128)S(1)}, u32[]{:S(2)}, u32[]{:S(2)}) collective-permute-start(f32[5,1024]{1,0:T(8,128)S(1)} %pad_maximum_fusion), channel_id=1, source_target_pairs={{0,4},{4,0},{8,12},{12,8},{1,5},{5,1},{9,13},{13,9},{2,6},{6,2},{1... | collective-permute-start | bytes 61448 | tf_op jit(solution)/shard_map/ppermute | solution.py:39
  25.0 2.1 %collective-permute-done.3 = f32[5,1024]{1,0:T(8,128)S(1)} collective-permute-done((f32[5,1024]{1,0:T(8,128)S(1)}, f32[5,1024]{1,0:T(8,128)S(1)}, u32[]{:S(2)}, u32[]{:S(2)}) %collective-permute-start.3) | collective-permute-done | bytes 20512 | tf_op jit(solution)/shard_map/ppermute | solution.py:39
  27.1 2.9 %collective-permute-start.4 = (f32[5,1024]{1,0:T(8,128)S(1)}, f32[5,1024]{1,0:T(8,128)S(1)}, u32[]{:S(2)}, u32[]{:S(2)}) collective-permute-start(f32[5,1024]{1,0:T(8,128)S(1)} %fusion.2), channel_id=1, source_target_pairs={{0,8},{4,12},{8,0},{12,4},{1,9},{5,13},{9,1},{13,5},{2,10},{6,14},... | collective-permute-start | bytes 61448 | tf_op jit(solution)/shard_map/ppermute | solution.py:39
  30.0 2.0 %collective-permute-done.4 = f32[5,1024]{1,0:T(8,128)S(1)} collective-permute-done((f32[5,1024]{1,0:T(8,128)S(1)}, f32[5,1024]{1,0:T(8,128)S(1)}, u32[]{:S(2)}, u32[]{:S(2)}) %collective-permute-start.4) | collective-permute-done | bytes 20512 | tf_op jit(solution)/shard_map/ppermute | solution.py:39
  32.0 1.7 %collective-permute-start.6 = (f32[5,1024]{1,0:T(8,128)S(1)}, f32[5,1024]{1,0:T(8,128)S(1)}, u32[]{:S(2)}, u32[]{:S(2)}) collective-permute-start(f32[5,1024]{1,0:T(8,128)S(1)} %add.18.refs_4_), channel_id=1, source_target_pairs={{0,2},{1,3},{2,0},{3,1},{4,6},{5,7},{6,4},{7,5},{8,10},{9,11},{10,... | collective-permute-start | bytes 61448 | tf_op jit(solution)/shard_map/ppermute | solution.py:39
  33.7 2.2 %collective-permute-done.6.refs_6_ = f32[5,1024]{1,0:T(8,128)S(1)} collective-permute-done((f32[5,1024]{1,0:T(8,128)S(1)}, f32[5,1024]{1,0:T(8,128)S(1)}, u32[]{:S(2)}, u32[]{:S(2)}) %collective-permute-start.6) | collective-permute-done | bytes 20512 | tf_op jit(solution)/shard_map/ppermute | solution.py:39
  38.4 2.7 %shard_map.154 = (f32[96,4096]{1,0:T(8,128)S(1)}, f32[96,4096]{1,0:T(8,128)S(1)}, f32[128,4096]{1,0:T(8,128)S(1)}) custom-call(bf16[96,4096]{1,0:T(8,128)(2,1)S(1)} %copy-done.2, bf16[96,4096]{1,0:T(8,128)(2,1)} %collective-permute-done.refs_1_, bf16[128,4096]{1,0:T(8,128)(2,1)S(1)} %copy-done.6), custom_call_target="tpu_custom_call" | custom-call | tf_op jit(solution)/shard_map/pallas_call | solution.py:440
  41.1 4.3 %shard_map.157 = (bf16[384,256]{1,0:T(8,128)(2,1)S(1)}, bf16[544,128]{1,0:T(8,128)(2,1)S(1)}, bf16[16,128]{1,0:T(8,128)(2,1)}) custom-call(s32[5]{0:T(128)S(1)} %compare_select_fusion.info, f32[96,4096]{1,0:T(8,128)S(1)} %get-tuple-element.32.refs_0_, f32[96,4096]{1,0:T(8,128)S(1)} %get-tuple-element.33.refs_1_, ...), custom_call_target="tpu_custom_call" | custom-call | tf_op jit(solution)/shard_map/pallas_call | solution.py:440
  45.4 1.7 %collective-permute-start.24 = (bf16[544,128]{1,0:T(8,128)(2,1)S(1)}, bf16[544,128]{1,0:T(8,128)(2,1)S(1)}, u32[]{:S(2)}, u32[]{:S(2)}) collective-permute-start(bf16[544,128]{1,0:T(8,128)(2,1)S(1)} %get-tuple-element.45.refs_5_), channel_id=1, source_target_pairs={{0,2},{1,3},{2,0},{3,1},{4,6},{5,7},{6,4},{7,5},{8,10},{9,11},{10,... | collective-permute-start | bytes 417800 | tf_op jit(solution)/shard_map/ppermute | solution.py:39
  49.5 2.0 %collective-permute-done.24.refs_7_ = bf16[544,128]{1,0:T(8,128)(2,1)S(1)} collective-permute-done((bf16[544,128]{1,0:T(8,128)(2,1)S(1)}, bf16[544,128]{1,0:T(8,128)(2,1)S(1)}, u32[]{:S(2)}, u32[]{:S(2)}) %collective-permute-start.24) | collective-permute-done | bytes 139296 | tf_op jit(solution)/shard_map/ppermute | solution.py:39
  51.5 2.9 %collective-permute-start.11 = (bf16[544,128]{1,0:T(8,128)(2,1)S(1)}, bf16[544,128]{1,0:T(8,128)(2,1)S(1)}, u32[]{:S(2)}, u32[]{:S(2)}) collective-permute-start(bf16[544,128]{1,0:T(8,128)(2,1)S(1)} %get-tuple-element.45.refs_5_), channel_id=1, source_target_pairs={{0,8},{4,12},{8,0},{12,4},{1,9},{5,13},{9,1},{13,5},{2,10},{6,14},... | collective-permute-start | bytes 417800 | tf_op jit(solution)/shard_map/ppermute | solution.py:39
  54.3 1.8 %collective-permute-start.15 = (bf16[544,128]{1,0:T(8,128)(2,1)S(1)}, bf16[544,128]{1,0:T(8,128)(2,1)S(1)}, u32[]{:S(2)}, u32[]{:S(2)}) collective-permute-start(bf16[544,128]{1,0:T(8,128)(2,1)S(1)} %get-tuple-element.45.refs_5_), channel_id=1, source_target_pairs={{0,12},{4,8},{8,4},{12,0},{1,13},{5,9},{9,5},{13,1},{2,14},{6,10},... | collective-permute-start | bytes 417800 | tf_op jit(solution)/shard_map/ppermute | solution.py:39
  56.7 8.2 %collective-permute-done.11.refs_5_ = bf16[544,128]{1,0:T(8,128)(2,1)S(1)} collective-permute-done((bf16[544,128]{1,0:T(8,128)(2,1)S(1)}, bf16[544,128]{1,0:T(8,128)(2,1)S(1)}, u32[]{:S(2)}, u32[]{:S(2)}) %collective-permute-start.11) | collective-permute-done | bytes 139296 | tf_op jit(solution)/shard_map/ppermute | solution.py:39
  64.9 1.7 %collective-permute-start.21 = (bf16[544,128]{1,0:T(8,128)(2,1)S(1)}, bf16[544,128]{1,0:T(8,128)(2,1)S(1)}, u32[]{:S(2)}, u32[]{:S(2)}) collective-permute-start(bf16[544,128]{1,0:T(8,128)(2,1)S(1)} %collective-permute-done.19.refs_5_), channel_id=1, source_target_pairs={{0,2},{1,3},{2,0},{3,1},{4,6},{5,7},{6,4},{7,5},{8,10},{9,11},{10,... | collective-permute-start | bytes 417800 | tf_op jit(solution)/shard_map/ppermute | solution.py:39
  67.0 1.7 %collective-permute-start.17 = (bf16[544,128]{1,0:T(8,128)(2,1)S(1)}, bf16[544,128]{1,0:T(8,128)(2,1)S(1)}, u32[]{:S(2)}, u32[]{:S(2)}) collective-permute-start(bf16[544,128]{1,0:T(8,128)(2,1)S(1)} %collective-permute-done.15.refs_9_), channel_id=1, source_target_pairs={{0,2},{1,3},{2,0},{3,1},{4,6},{5,7},{6,4},{7,5},{8,10},{9,11},{10,... | collective-permute-start | bytes 417800 | tf_op jit(solution)/shard_map/ppermute | solution.py:39
  68.7 2.0 %collective-permute-done.21.refs_7_ = bf16[544,128]{1,0:T(8,128)(2,1)S(1)} collective-permute-done((bf16[544,128]{1,0:T(8,128)(2,1)S(1)}, bf16[544,128]{1,0:T(8,128)(2,1)S(1)}, u32[]{:S(2)}, u32[]{:S(2)}) %collective-permute-start.21) | collective-permute-done | bytes 139296 | tf_op jit(solution)/shard_map/ppermute | solution.py:39
  71.2 2.4 %collective-permute-done.13.refs_7_ = bf16[544,128]{1,0:T(8,128)(2,1)S(1)} collective-permute-done((bf16[544,128]{1,0:T(8,128)(2,1)S(1)}, bf16[544,128]{1,0:T(8,128)(2,1)S(1)}, u32[]{:S(2)}, u32[]{:S(2)}) %collective-permute-start.13) | collective-permute-done | bytes 139296 | tf_op jit(solution)/shard_map/ppermute | solution.py:39
  73.5 2.4 %collective-permute-done.17.refs_11_ = bf16[544,128]{1,0:T(8,128)(2,1)S(1)} collective-permute-done((bf16[544,128]{1,0:T(8,128)(2,1)S(1)}, bf16[544,128]{1,0:T(8,128)(2,1)S(1)}, u32[]{:S(2)}, u32[]{:S(2)}) %collective-permute-start.17) | collective-permute-done | bytes 139296 | tf_op jit(solution)/shard_map/ppermute | solution.py:39
  77.6 2.1 %shard_map.159.refs_1_ = bf16[4,256,768]{2,1,0:T(8,128)(2,1)S(1)} custom-call(s32[5]{0:T(128)S(1)} %compare_select_fusion.info, bf16[384,256]{1,0:T(8,128)(2,1)S(1)} %get-tuple-element.40.refs_0_, bf16[384,256]{1,0:T(8,128)(2,1)S(1)} %collective-permute-done.8.refs_1_, bf16[384,256]{1,0:T(8,128)(2,1)S(1)} %collective-permute-done.9.refs_2_, ...), custom_call_target="tpu_custom_call" | custom-call | tf_op jit(solution)/shard_map/pallas_call | solution.py:440
  79.8 4.3 %shard_map.160 = (f32[4,8,768]{2,1,0:T(8,128)S(1)}, f32[4,8,768]{2,1,0:T(8,128)S(1)}, f32[4,128,384]{2,1,0:T(8,128)S(1)}) custom-call(s32[5]{0:T(128)S(1)} %compare_select_fusion.info, f32[8]{0:T(128)S(1)} %copy-done.11, bf16[4,256,768]{2,1,0:T(8,128)(2,1)S(1)} %shard_map.159.refs_1_, f32[1,512]{1,0:T(1,128)S(1)} %bitcast.13, ...), custom_call_target="tpu_custom_call" | custom-call | tf_op jit(solution)/shard_map/pallas_call | solution.py:440
  84.1 4.8 %shard_map.161 = (f32[4,8,768]{2,1,0:T(8,128)S(1)}, f32[4,8,768]{2,1,0:T(8,128)S(1)}, f32[4,128,384]{2,1,0:T(8,128)S(1)}) custom-call(s32[5]{0:T(128)S(1)} %compare_select_fusion.info, f32[8]{0:T(128)S(1)} %copy-done.11, bf16[4,256,768]{2,1,0:T(8,128)(2,1)S(1)} %shard_map.159.refs_1_, f32[1,512]{1,0:T(1,128)S(1)} %bitcast.14, ...), custom_call_target="tpu_custom_call" | custom-call | tf_op jit(solution)/shard_map/pallas_call | solution.py:440
  88.9 8.4 %shard_map.162.refs_0_ = bf16[384,512]{1,0:T(8,128)(2,1)S(1)} custom-call(s32[5]{0:T(128)S(1)} %compare_select_fusion.info, f32[8]{0:T(128)S(1)} %copy-done.11, bf16[4,256,768]{2,1,0:T(8,128)(2,1)S(1)} %shard_map.159.refs_1_, f32[1,512]{1,0:T(1,128)S(1)} %bitcast.15, bf16[512,512]{1,0:T(8,128)(2,1)S(1)} %get-tuple-element.43.refs_3_, ...), custom_call_target="tpu_custom_call" | custom-call | tf_op jit(solution)/shard_map/pallas_call | solution.py:440
  97.4 1.7 %collective-permute-start.27 = (bf16[384,512]{1,0:T(8,128)(2,1)S(1)}, bf16[384,512]{1,0:T(8,128)(2,1)S(1)}, u32[]{:S(2)}, u32[]{:S(2)}) collective-permute-start(bf16[384,512]{1,0:T(8,128)(2,1)S(1)} %shard_map.162.refs_0_), channel_id=1, source_target_pairs={{0,2},{1,3},{2,0},{3,1},{4,6},{5,7},{6,4},{7,5},{8,10},{9,11},{10,... | collective-permute-start | bytes 1179656 | tf_op jit(solution)/shard_map/ppermute | solution.py:39
  99.0 9.5 %collective-permute-done.27.refs_2_ = bf16[384,512]{1,0:T(8,128)(2,1)S(1)} collective-permute-done((bf16[384,512]{1,0:T(8,128)(2,1)S(1)}, bf16[384,512]{1,0:T(8,128)(2,1)S(1)}, u32[]{:S(2)}, u32[]{:S(2)}) %collective-permute-start.27) | collective-permute-done | bytes 393248 | tf_op jit(solution)/shard_map/ppermute | solution.py:39
  108.5 1.7 %collective-permute-done.28.refs_3_ = bf16[384,512]{1,0:T(8,128)(2,1)S(1)} collective-permute-done((bf16[384,512]{1,0:T(8,128)(2,1)S(1)}, bf16[384,512]{1,0:T(8,128)(2,1)S(1)}, u32[]{:S(2)}, u32[]{:S(2)}) %collective-permute-start.28) | collective-permute-done | bytes 393248 | tf_op jit(solution)/shard_map/ppermute | solution.py:39
  110.2 2.4 %shard_map.163 = (bf16[96,1024]{1,0:T(8,128)(2,1)S(1)}, bf16[96,1024]{1,0:T(8,128)(2,1)S(1)}, bf16[96,1024]{1,0:T(8,128)(2,1)S(1)}, bf16[96,1024]{1,0:T(8,128)(2,1)S(1)}) custom-call(s32[5]{0:T(128)S(1)} %compare_select_fusion.info, bf16[384,512]{1,0:T(8,128)(2,1)S(1)} %shard_map.162.refs_0_, bf16[384,512]{1,0:T(8,128)(2,1)S(1)} %collective-permute-done.26.refs_1_, ...), custom_call_target="tpu_custom_call" | custom-call | tf_op jit(solution)/shard_map/pallas_call | solution.py:440
  114.6 6.0 %collective-permute-done.30.refs_2_ = bf16[96,1024]{1,0:T(8,128)(2,1)S(1)} collective-permute-done((bf16[96,1024]{1,0:T(8,128)(2,1)S(1)}, bf16[96,1024]{1,0:T(8,128)(2,1)S(1)}, u32[]{:S(2)}, u32[]{:S(2)}) %collective-permute-start.30) | collective-permute-done | bytes 196640 | tf_op jit(solution)/shard_map/ppermute | solution.py:39
  120.6 3.0 %collective-permute-done.31.refs_3_ = bf16[96,1024]{1,0:T(8,128)(2,1)S(1)} collective-permute-done((bf16[96,1024]{1,0:T(8,128)(2,1)S(1)}, bf16[96,1024]{1,0:T(8,128)(2,1)S(1)}, u32[]{:S(2)}, u32[]{:S(2)}) %collective-permute-start.31) | collective-permute-done | bytes 196640 | tf_op jit(solution)/shard_map/ppermute | solution.py:39
  123.6 1.7 %shard_map.164 = bf16[96,4096]{1,0:T(8,128)(2,1)} custom-call(s32[5]{0:T(128)S(1)} %compare_select_fusion.info, bf16[96,1024]{1,0:T(8,128)(2,1)S(1)} %get-tuple-element.53.refs_0_, bf16[96,1024]{1,0:T(8,128)(2,1)S(1)} %collective-permute-done.29.refs_1_, bf16[96,1024]{1,0:T(8,128)(2,1)S(1)} %collective-permute-done.30.refs_2_, ...), custom_call_target="tpu_custom_call" | custom-call | tf_op jit(solution)/shard_map/pallas_call | solution.py:440
  (79 shorter events, 11.5 us)
Async XLA Ops:
  0.0 20.7 %collective-permute-start.1 = (bf16[96,4096]{1,0:T(8,128)(2,1)}, bf16[96,4096]{1,0:T(8,128)(2,1)S(1)}, u32[]{:S(2)}, u32[]{:S(2)}) collective-permute-start(bf16[96,4096]{1,0:T(8,128)(2,1)} %refs_8_.1), channel_id=1, source_target_pairs={{0,2},{1,3},{2,0},{3,1},{4,6},{5,7},{6,4},{7,5},{8,10},{9,11},{10,... | collective-permute-start | bytes 2359304 | tf_op jit(solution)/shard_map/ppermute | solution.py:39
  3.0 35.4 %collective-permute-start = (bf16[96,4096]{1,0:T(8,128)(2,1)}, bf16[96,4096]{1,0:T(8,128)(2,1)}, u32[]{:S(2)}, u32[]{:S(2)}) collective-permute-start(bf16[96,4096]{1,0:T(8,128)(2,1)} %refs_8_.1), channel_id=1, source_target_pairs={{0,1},{1,0},{2,3},{3,2},{4,5},{5,4},{6,7},{7,6},{8,9},{9,8},{10,11... | collective-permute-start | bytes 2359304 | tf_op jit(solution)/shard_map/ppermute | solution.py:39
  20.7 20.4 %collective-permute-start.2 = (bf16[96,4096]{1,0:T(8,128)(2,1)S(1)}, bf16[96,4096]{1,0:T(8,128)(2,1)S(1)}, u32[]{:S(2)}, u32[]{:S(2)}) collective-permute-start(bf16[96,4096]{1,0:T(8,128)(2,1)S(1)} %collective-permute-done.1.refs_2_), channel_id=1, source_target_pairs={{0,1},{1,0},{2,3},{3,2},{4,5},{5,4},{6,7},{7,6},{8,9},{9,8},{10,11... | collective-permute-start | bytes 2359304 | tf_op jit(solution)/shard_map/ppermute | solution.py:39
  23.1 4.0 %collective-permute-start.3 = (f32[5,1024]{1,0:T(8,128)S(1)}, f32[5,1024]{1,0:T(8,128)S(1)}, u32[]{:S(2)}, u32[]{:S(2)}) collective-permute-start(f32[5,1024]{1,0:T(8,128)S(1)} %pad_maximum_fusion), channel_id=1, source_target_pairs={{0,4},{4,0},{8,12},{12,8},{1,5},{5,1},{9,13},{13,9},{2,6},{6,2},{1... | collective-permute-start | bytes 61448 | tf_op jit(solution)/shard_map/ppermute | solution.py:39
  27.1 4.9 %collective-permute-start.4 = (f32[5,1024]{1,0:T(8,128)S(1)}, f32[5,1024]{1,0:T(8,128)S(1)}, u32[]{:S(2)}, u32[]{:S(2)}) collective-permute-start(f32[5,1024]{1,0:T(8,128)S(1)} %fusion.2), channel_id=1, source_target_pairs={{0,8},{4,12},{8,0},{12,4},{1,9},{5,13},{9,1},{13,5},{2,10},{6,14},... | collective-permute-start | bytes 61448 | tf_op jit(solution)/shard_map/ppermute | solution.py:39
  32.0 3.9 %collective-permute-start.6 = (f32[5,1024]{1,0:T(8,128)S(1)}, f32[5,1024]{1,0:T(8,128)S(1)}, u32[]{:S(2)}, u32[]{:S(2)}) collective-permute-start(f32[5,1024]{1,0:T(8,128)S(1)} %add.18.refs_4_), channel_id=1, source_target_pairs={{0,2},{1,3},{2,0},{3,1},{4,6},{5,7},{6,4},{7,5},{8,10},{9,11},{10,... | collective-permute-start | bytes 61448 | tf_op jit(solution)/shard_map/ppermute | solution.py:39
  33.7 7.3 %collective-permute-start.5 = (f32[5,1024]{1,0:T(8,128)S(1)}, f32[5,1024]{1,0:T(8,128)S(1)}, u32[]{:S(2)}, u32[]{:S(2)}) collective-permute-start(f32[5,1024]{1,0:T(8,128)S(1)} %add.18.refs_4_), channel_id=1, source_target_pairs={{0,1},{1,0},{2,3},{3,2},{4,5},{5,4},{6,7},{7,6},{8,9},{9,8},{10,11... | collective-permute-start | bytes 61448 | tf_op jit(solution)/shard_map/ppermute | solution.py:39
  35.9 5.1 %collective-permute-start.7 = (f32[5,1024]{1,0:T(8,128)S(1)}, f32[5,1024]{1,0:T(8,128)S(1)}, u32[]{:S(2)}, u32[]{:S(2)}) collective-permute-start(f32[5,1024]{1,0:T(8,128)S(1)} %collective-permute-done.6.refs_6_), channel_id=1, source_target_pairs={{0,1},{1,0},{2,3},{3,2},{4,5},{5,4},{6,7},{7,6},{8,9},{9,8},{10,11... | collective-permute-start | bytes 61448 | tf_op jit(solution)/shard_map/ppermute | solution.py:39
  45.4 6.1 %collective-permute-start.24 = (bf16[544,128]{1,0:T(8,128)(2,1)S(1)}, bf16[544,128]{1,0:T(8,128)(2,1)S(1)}, u32[]{:S(2)}, u32[]{:S(2)}) collective-permute-start(bf16[544,128]{1,0:T(8,128)(2,1)S(1)} %get-tuple-element.45.refs_5_), channel_id=1, source_target_pairs={{0,2},{1,3},{2,0},{3,1},{4,6},{5,7},{6,4},{7,5},{8,10},{9,11},{10,... | collective-permute-start | bytes 417800 | tf_op jit(solution)/shard_map/ppermute | solution.py:39
  47.1 7.2 %collective-permute-start.23 = (bf16[544,128]{1,0:T(8,128)(2,1)S(1)}, bf16[544,128]{1,0:T(8,128)(2,1)S(1)}, u32[]{:S(2)}, u32[]{:S(2)}) collective-permute-start(bf16[544,128]{1,0:T(8,128)(2,1)S(1)} %get-tuple-element.45.refs_5_), channel_id=1, source_target_pairs={{0,1},{1,0},{2,3},{3,2},{4,5},{5,4},{6,7},{7,6},{8,9},{9,8},{10,11... | collective-permute-start | bytes 417800 | tf_op jit(solution)/shard_map/ppermute | solution.py:39
  47.4 8.8 %collective-permute-start.19 = (bf16[544,128]{1,0:T(8,128)(2,1)S(1)}, bf16[544,128]{1,0:T(8,128)(2,1)S(1)}, u32[]{:S(2)}, u32[]{:S(2)}) collective-permute-start(bf16[544,128]{1,0:T(8,128)(2,1)S(1)} %get-tuple-element.45.refs_5_), channel_id=1, source_target_pairs={{0,4},{4,0},{8,12},{12,8},{1,5},{5,1},{9,13},{13,9},{2,6},{6,2},{1... | collective-permute-start | bytes 417800 | tf_op jit(solution)/shard_map/ppermute | solution.py:39
  48.9 7.2 %collective-permute-start.9 = (bf16[384,256]{1,0:T(8,128)(2,1)S(1)}, bf16[384,256]{1,0:T(8,128)(2,1)S(1)}, u32[]{:S(2)}, u32[]{:S(2)}) collective-permute-start(bf16[384,256]{1,0:T(8,128)(2,1)S(1)} %get-tuple-element.40.refs_0_), channel_id=1, source_target_pairs={{0,2},{1,3},{2,0},{3,1},{4,6},{5,7},{6,4},{7,5},{8,10},{9,11},{10,... | collective-permute-start | bytes 589832 | tf_op jit(solution)/shard_map/ppermute | solution.py:39
  49.5 17.1 %collective-permute-start.8 = (bf16[384,256]{1,0:T(8,128)(2,1)S(1)}, bf16[384,256]{1,0:T(8,128)(2,1)S(1)}, u32[]{:S(2)}, u32[]{:S(2)}) collective-permute-start(bf16[384,256]{1,0:T(8,128)(2,1)S(1)} %get-tuple-element.40.refs_0_), channel_id=1, source_target_pairs={{0,1},{1,0},{2,3},{3,2},{4,5},{5,4},{6,7},{7,6},{8,9},{9,8},{10,11... | collective-permute-start | bytes 589832 | tf_op jit(solution)/shard_map/ppermute | solution.py:39
  51.5 13.4 %collective-permute-start.11 = (bf16[544,128]{1,0:T(8,128)(2,1)S(1)}, bf16[544,128]{1,0:T(8,128)(2,1)S(1)}, u32[]{:S(2)}, u32[]{:S(2)}) collective-permute-start(bf16[544,128]{1,0:T(8,128)(2,1)S(1)} %get-tuple-element.45.refs_5_), channel_id=1, source_target_pairs={{0,8},{4,12},{8,0},{12,4},{1,9},{5,13},{9,1},{13,5},{2,10},{6,14},... | collective-permute-start | bytes 417800 | tf_op jit(solution)/shard_map/ppermute | solution.py:39
  54.3 12.3 %collective-permute-start.15 = (bf16[544,128]{1,0:T(8,128)(2,1)S(1)}, bf16[544,128]{1,0:T(8,128)(2,1)S(1)}, u32[]{:S(2)}, u32[]{:S(2)}) collective-permute-start(bf16[544,128]{1,0:T(8,128)(2,1)S(1)} %get-tuple-element.45.refs_5_), channel_id=1, source_target_pairs={{0,12},{4,8},{8,4},{12,0},{1,13},{5,9},{9,5},{13,1},{2,14},{6,10},... | collective-permute-start | bytes 417800 | tf_op jit(solution)/shard_map/ppermute | solution.py:39
  56.1 10.9 %collective-permute-start.25 = (bf16[544,128]{1,0:T(8,128)(2,1)S(1)}, bf16[544,128]{1,0:T(8,128)(2,1)S(1)}, u32[]{:S(2)}, u32[]{:S(2)}) collective-permute-start(bf16[544,128]{1,0:T(8,128)(2,1)S(1)} %collective-permute-done.24.refs_7_), channel_id=1, source_target_pairs={{0,1},{1,0},{2,3},{3,2},{4,5},{5,4},{6,7},{7,6},{8,9},{9,8},{10,11... | collective-permute-start | bytes 417800 | tf_op jit(solution)/shard_map/ppermute | solution.py:39
  56.1 19.8 %collective-permute-start.10 = (bf16[384,256]{1,0:T(8,128)(2,1)S(1)}, bf16[384,256]{1,0:T(8,128)(2,1)S(1)}, u32[]{:S(2)}, u32[]{:S(2)}) collective-permute-start(bf16[384,256]{1,0:T(8,128)(2,1)S(1)} %collective-permute-done.9.refs_2_), channel_id=1, source_target_pairs={{0,1},{1,0},{2,3},{3,2},{4,5},{5,4},{6,7},{7,6},{8,9},{9,8},{10,11... | collective-permute-start | bytes 589832 | tf_op jit(solution)/shard_map/ppermute | solution.py:39
  64.9 5.8 %collective-permute-start.21 = (bf16[544,128]{1,0:T(8,128)(2,1)S(1)}, bf16[544,128]{1,0:T(8,128)(2,1)S(1)}, u32[]{:S(2)}, u32[]{:S(2)}) collective-permute-start(bf16[544,128]{1,0:T(8,128)(2,1)S(1)} %collective-permute-done.19.refs_5_), channel_id=1, source_target_pairs={{0,2},{1,3},{2,0},{3,1},{4,6},{5,7},{6,4},{7,5},{8,10},{9,11},{10,... | collective-permute-start | bytes 417800 | tf_op jit(solution)/shard_map/ppermute | solution.py:39
  66.6 4.1 %collective-permute-start.20 = (bf16[544,128]{1,0:T(8,128)(2,1)S(1)}, bf16[544,128]{1,0:T(8,128)(2,1)S(1)}, u32[]{:S(2)}, u32[]{:S(2)}) collective-permute-start(bf16[544,128]{1,0:T(8,128)(2,1)S(1)} %collective-permute-done.19.refs_5_), channel_id=1, source_target_pairs={{0,1},{1,0},{2,3},{3,2},{4,5},{5,4},{6,7},{7,6},{8,9},{9,8},{10,11... | collective-permute-start | bytes 417800 | tf_op jit(solution)/shard_map/ppermute | solution.py:39
  66.6 6.9 %collective-permute-start.13 = (bf16[544,128]{1,0:T(8,128)(2,1)S(1)}, bf16[544,128]{1,0:T(8,128)(2,1)S(1)}, u32[]{:S(2)}, u32[]{:S(2)}) collective-permute-start(bf16[544,128]{1,0:T(8,128)(2,1)S(1)} %collective-permute-done.11.refs_5_), channel_id=1, source_target_pairs={{0,2},{1,3},{2,0},{3,1},{4,6},{5,7},{6,4},{7,5},{8,10},{9,11},{10,... | collective-permute-start | bytes 417800 | tf_op jit(solution)/shard_map/ppermute | solution.py:39
  67.0 8.9 %collective-permute-start.17 = (bf16[544,128]{1,0:T(8,128)(2,1)S(1)}, bf16[544,128]{1,0:T(8,128)(2,1)S(1)}, u32[]{:S(2)}, u32[]{:S(2)}) collective-permute-start(bf16[544,128]{1,0:T(8,128)(2,1)S(1)} %collective-permute-done.15.refs_9_), channel_id=1, source_target_pairs={{0,2},{1,3},{2,0},{3,1},{4,6},{5,7},{6,4},{7,5},{8,10},{9,11},{10,... | collective-permute-start | bytes 417800 | tf_op jit(solution)/shard_map/ppermute | solution.py:39
  70.7 13.4 %collective-permute-start.22 = (bf16[544,128]{1,0:T(8,128)(2,1)S(1)}, bf16[544,128]{1,0:T(8,128)(2,1)S(1)}, u32[]{:S(2)}, u32[]{:S(2)}) collective-permute-start(bf16[544,128]{1,0:T(8,128)(2,1)S(1)} %collective-permute-done.21.refs_7_), channel_id=1, source_target_pairs={{0,1},{1,0},{2,3},{3,2},{4,5},{5,4},{6,7},{7,6},{8,9},{9,8},{10,11... | collective-permute-start | bytes 417800 | tf_op jit(solution)/shard_map/ppermute | solution.py:39
  70.7 18.2 %collective-permute-start.12 = (bf16[544,128]{1,0:T(8,128)(2,1)S(1)}, bf16[544,128]{1,0:T(8,128)(2,1)S(1)}, u32[]{:S(2)}, u32[]{:S(2)}) collective-permute-start(bf16[544,128]{1,0:T(8,128)(2,1)S(1)} %collective-permute-done.11.refs_5_), channel_id=1, source_target_pairs={{0,1},{1,0},{2,3},{3,2},{4,5},{5,4},{6,7},{7,6},{8,9},{9,8},{10,11... | collective-permute-start | bytes 417800 | tf_op jit(solution)/shard_map/ppermute | solution.py:39
  73.5 15.4 %collective-permute-start.16 = (bf16[544,128]{1,0:T(8,128)(2,1)S(1)}, bf16[544,128]{1,0:T(8,128)(2,1)S(1)}, u32[]{:S(2)}, u32[]{:S(2)}) collective-permute-start(bf16[544,128]{1,0:T(8,128)(2,1)S(1)} %collective-permute-done.15.refs_9_), channel_id=1, source_target_pairs={{0,1},{1,0},{2,3},{3,2},{4,5},{5,4},{6,7},{7,6},{8,9},{9,8},{10,11... | collective-permute-start | bytes 417800 | tf_op jit(solution)/shard_map/ppermute | solution.py:39
  75.9 13.0 %collective-permute-start.14 = (bf16[544,128]{1,0:T(8,128)(2,1)S(1)}, bf16[544,128]{1,0:T(8,128)(2,1)S(1)}, u32[]{:S(2)}, u32[]{:S(2)}) collective-permute-start(bf16[544,128]{1,0:T(8,128)(2,1)S(1)} %collective-permute-done.13.refs_7_), channel_id=1, source_target_pairs={{0,1},{1,0},{2,3},{3,2},{4,5},{5,4},{6,7},{7,6},{8,9},{9,8},{10,11... | collective-permute-start | bytes 417800 | tf_op jit(solution)/shard_map/ppermute | solution.py:39
  75.9 13.0 %collective-permute-start.18 = (bf16[544,128]{1,0:T(8,128)(2,1)S(1)}, bf16[544,128]{1,0:T(8,128)(2,1)S(1)}, u32[]{:S(2)}, u32[]{:S(2)}) collective-permute-start(bf16[544,128]{1,0:T(8,128)(2,1)S(1)} %collective-permute-done.17.refs_11_), channel_id=1, source_target_pairs={{0,1},{1,0},{2,3},{3,2},{4,5},{5,4},{6,7},{7,6},{8,9},{9,8},{10,11... | collective-permute-start | bytes 417800 | tf_op jit(solution)/shard_map/ppermute | solution.py:39
  97.4 11.1 %collective-permute-start.27 = (bf16[384,512]{1,0:T(8,128)(2,1)S(1)}, bf16[384,512]{1,0:T(8,128)(2,1)S(1)}, u32[]{:S(2)}, u32[]{:S(2)}) collective-permute-start(bf16[384,512]{1,0:T(8,128)(2,1)S(1)} %shard_map.162.refs_0_), channel_id=1, source_target_pairs={{0,2},{1,3},{2,0},{3,1},{4,6},{5,7},{6,4},{7,5},{8,10},{9,11},{10,... | collective-permute-start | bytes 1179656 | tf_op jit(solution)/shard_map/ppermute | solution.py:39
  99.0 9.5 %collective-permute-start.26 = (bf16[384,512]{1,0:T(8,128)(2,1)S(1)}, bf16[384,512]{1,0:T(8,128)(2,1)S(1)}, u32[]{:S(2)}, u32[]{:S(2)}) collective-permute-start(bf16[384,512]{1,0:T(8,128)(2,1)S(1)} %shard_map.162.refs_0_), channel_id=1, source_target_pairs={{0,1},{1,0},{2,3},{3,2},{4,5},{5,4},{6,7},{7,6},{8,9},{9,8},{10,11... | collective-permute-start | bytes 1179656 | tf_op jit(solution)/shard_map/ppermute | solution.py:39
  108.5 1.7 %collective-permute-start.28 = (bf16[384,512]{1,0:T(8,128)(2,1)S(1)}, bf16[384,512]{1,0:T(8,128)(2,1)S(1)}, u32[]{:S(2)}, u32[]{:S(2)}) collective-permute-start(bf16[384,512]{1,0:T(8,128)(2,1)S(1)} %collective-permute-done.27.refs_2_), channel_id=1, source_target_pairs={{0,1},{1,0},{2,3},{3,2},{4,5},{5,4},{6,7},{7,6},{8,9},{9,8},{10,11... | collective-permute-start | bytes 1179656 | tf_op jit(solution)/shard_map/ppermute | solution.py:39
  112.6 1.9 %collective-permute-start.29 = (bf16[96,1024]{1,0:T(8,128)(2,1)S(1)}, bf16[96,1024]{1,0:T(8,128)(2,1)S(1)}, u32[]{:S(2)}, u32[]{:S(2)}) collective-permute-start(bf16[96,1024]{1,0:T(8,128)(2,1)S(1)} %get-tuple-element.54), channel_id=1, source_target_pairs={{0,1},{1,0},{2,3},{3,2},{4,5},{5,4},{6,7},{7,6},{8,9},{9,8},{10,11... | collective-permute-start | bytes 589832 | tf_op jit(solution)/shard_map/ppermute | solution.py:39
  112.8 7.8 %collective-permute-start.30 = (bf16[96,1024]{1,0:T(8,128)(2,1)S(1)}, bf16[96,1024]{1,0:T(8,128)(2,1)S(1)}, u32[]{:S(2)}, u32[]{:S(2)}) collective-permute-start(bf16[96,1024]{1,0:T(8,128)(2,1)S(1)} %get-tuple-element.55), channel_id=1, source_target_pairs={{0,2},{1,3},{2,0},{3,1},{4,6},{5,7},{6,4},{7,5},{8,10},{9,11},{10,... | collective-permute-start | bytes 589832 | tf_op jit(solution)/shard_map/ppermute | solution.py:39
  114.4 9.2 %collective-permute-start.31 = (bf16[96,1024]{1,0:T(8,128)(2,1)S(1)}, bf16[96,1024]{1,0:T(8,128)(2,1)S(1)}, u32[]{:S(2)}, u32[]{:S(2)}) collective-permute-start(bf16[96,1024]{1,0:T(8,128)(2,1)S(1)} %get-tuple-element.56), channel_id=1, source_target_pairs={{0,3},{1,2},{2,1},{3,0},{4,7},{5,6},{6,5},{7,4},{8,11},{9,10},{10,... | collective-permute-start | bytes 589832 | tf_op jit(solution)/shard_map/ppermute | solution.py:39
  (14 other events, 326.3 us)

commit v2 on v1

--- a/solution.py
+++ b/solution.py
@@ -346,6 +346,15 @@
             r_ref[base : base + seg, :] = block[-1][...]
     score_scale = (PLAIN_QK_DIM + ROTARY_DIM) ** (-0.5) * LOG2E
     lane = lax.broadcasted_iota(jnp.int32, (1, lanes), 1)
+
+    def score(pair, number):
+        base = number * seg
+        span = slice(pair * LANES, (pair + 1) * LANES)
+        key = jnp.concatenate([k_ref[base : base + seg, span], r_ref[base : base + seg, :]], axis=1)
+        return f32_dot(key, q_ref[pair])
+
+    steps = [(pair, number) for pair in range(pairs) for number in range(len(blocks))]
+    ahead = score(*steps[0])
     for pair in range(pairs):
         span = slice(pair * LANES, (pair + 1) * LANES)
         bias = jnp.where(lane < rows, bias_ref[2 * pair], bias_ref[2 * pair + 1]) * LOG2E
@@ -354,11 +363,10 @@
             top = state_in[0][pair, :1, :]
             total, acc = state_in[1][pair], state_in[2][pair]
         for number in range(len(blocks)):
-            base = number * seg
-            key = jnp.concatenate(
-                [k_ref[base : base + seg, span], r_ref[base : base + seg, :]], axis=1
-            )
-            scores = f32_dot(key, q_ref[pair])
+            scores = ahead
+            after = pair * len(blocks) + number + 1
+            if after < len(steps):
+                ahead = score(*steps[after])
             lat, ctx = scores[:tok_keys], scores[tok_keys:]
             peak = jnp.maximum(
                 jnp.max(lat, axis=0, keepdims=True) * score_scale,

time: 126 us -> 123 us (0.976)
  Pallas kernels: 34.2 us -> 31.6 us
    pallas_call x11, Pallas kernels: 34.2 us -> 31.6 us  [call(): pl.pallas_call(kernel, out_shape=outs, in_specs=specs, out_specs=[in_vmem...]
  transfers between devices with their start and end apart: 32 -> 32, of which waited for: 13 -> 13; matrix products, arithmetic and copies ran while one was open for 3% -> 3% of each run, Pallas kernels for 14% -> 13%
where the time goes in v2:
time: 123 us
  waiting for transfers between devices  60 us (49%)
  Pallas kernels  31.6 us (26%)
  starting transfers between devices  27.1 us (22%)
  matrix products  2.74 us (2%)
    ppermute x32, waiting for transfers between devices, swap(): return lax.ppermute(value, axis, [(i, i ^ bit) for i in range(count)])  60 us
    pallas_call x11, Pallas kernels, call(): pl.pallas_call(kernel, out_shape=outs, in_specs=specs, out_specs=[in_vmem...  31.6 us
    ppermute x32, starting transfers between devices, swap(): return lax.ppermute(value, axis, [(i, i ^ bit) for i in range(count)])  27.1 us
    dot_general x3, matrix products, f32_dot(): return jnp.dot(a, b, preferred_element_type=jnp.float32)  2.74 us
  transfers between devices with their start and end apart: 32, of which 13 were waited for; matrix products, arithmetic and copies ran while one was open for 3% of the time, Pallas kernels for 13%

profile of v2, /device:TPU:0, one launch (start us, length us, event | category | flops | bytes accessed | tf_op | source)
XLA Modules:
  0.0 122.8 jit_solution(12156536464698261859)
XLA Ops:
  0.0 3.0 %collective-permute-start.1 = (bf16[96,4096]{1,0:T(8,128)(2,1)}, bf16[96,4096]{1,0:T(8,128)(2,1)S(1)}, u32[]{:S(2)}, u32[]{:S(2)}) collective-permute-start(bf16[96,4096]{1,0:T(8,128)(2,1)} %refs_8_.1), channel_id=1, source_target_pairs={{0,2},{1,3},{2,0},{3,1},{4,6},{5,7},{6,4},{7,5},{8,10},{9,11},{10,... | collective-permute-start | bytes 2359304 | tf_op jit(solution)/shard_map/ppermute | solution.py:39
  4.3 16.5 %collective-permute-done.1.refs_2_ = bf16[96,4096]{1,0:T(8,128)(2,1)S(1)} collective-permute-done((bf16[96,4096]{1,0:T(8,128)(2,1)}, bf16[96,4096]{1,0:T(8,128)(2,1)S(1)}, u32[]{:S(2)}, u32[]{:S(2)}) %collective-permute-start.1) | collective-permute-done | bytes 786464 | tf_op jit(solution)/shard_map/ppermute | solution.py:39
  21.1 2.0 %fusion.4 = f32[2,1024]{1,0:T(2,128)S(1)} fusion(bf16[2,1024]{1,0:T(2,128)(2,1)S(1)} %fusion, bf16[1024,1024]{1,0:T(8,128)(2,1)} %param.20), kind=kOutput, calls=%fused_computation.8 | convolution fusion | flops 4194304 | bytes 2109440 | tf_op jit(solution)/shard_map/dot_general | solution.py:34
  23.1 1.9 %collective-permute-start.3 = (f32[5,1024]{1,0:T(8,128)S(1)}, f32[5,1024]{1,0:T(8,128)S(1)}, u32[]{:S(2)}, u32[]{:S(2)}) collective-permute-start(f32[5,1024]{1,0:T(8,128)S(1)} %pad_maximum_fusion), channel_id=1, source_target_pairs={{0,4},{4,0},{8,12},{12,8},{1,5},{5,1},{9,13},{13,9},{2,6},{6,2},{1... | collective-permute-start | bytes 61448 | tf_op jit(solution)/shard_map/ppermute | solution.py:39
  25.0 2.1 %collective-permute-done.3 = f32[5,1024]{1,0:T(8,128)S(1)} collective-permute-done((f32[5,1024]{1,0:T(8,128)S(1)}, f32[5,1024]{1,0:T(8,128)S(1)}, u32[]{:S(2)}, u32[]{:S(2)}) %collective-permute-start.3) | collective-permute-done | bytes 20512 | tf_op jit(solution)/shard_map/ppermute | solution.py:39
  27.1 2.9 %collective-permute-start.4 = (f32[5,1024]{1,0:T(8,128)S(1)}, f32[5,1024]{1,0:T(8,128)S(1)}, u32[]{:S(2)}, u32[]{:S(2)}) collective-permute-start(f32[5,1024]{1,0:T(8,128)S(1)} %fusion.2), channel_id=1, source_target_pairs={{0,8},{4,12},{8,0},{12,4},{1,9},{5,13},{9,1},{13,5},{2,10},{6,14},... | collective-permute-start | bytes 61448 | tf_op jit(solution)/shard_map/ppermute | solution.py:39
  30.0 2.0 %collective-permute-done.4 = f32[5,1024]{1,0:T(8,128)S(1)} collective-permute-done((f32[5,1024]{1,0:T(8,128)S(1)}, f32[5,1024]{1,0:T(8,128)S(1)}, u32[]{:S(2)}, u32[]{:S(2)}) %collective-permute-start.4) | collective-permute-done | bytes 20512 | tf_op jit(solution)/shard_map/ppermute | solution.py:39
  32.0 1.7 %collective-permute-start.6 = (f32[5,1024]{1,0:T(8,128)S(1)}, f32[5,1024]{1,0:T(8,128)S(1)}, u32[]{:S(2)}, u32[]{:S(2)}) collective-permute-start(f32[5,1024]{1,0:T(8,128)S(1)} %add.18.refs_4_), channel_id=1, source_target_pairs={{0,2},{1,3},{2,0},{3,1},{4,6},{5,7},{6,4},{7,5},{8,10},{9,11},{10,... | collective-permute-start | bytes 61448 | tf_op jit(solution)/shard_map/ppermute | solution.py:39
  33.7 2.2 %collective-permute-done.6.refs_6_ = f32[5,1024]{1,0:T(8,128)S(1)} collective-permute-done((f32[5,1024]{1,0:T(8,128)S(1)}, f32[5,1024]{1,0:T(8,128)S(1)}, u32[]{:S(2)}, u32[]{:S(2)}) %collective-permute-start.6) | collective-permute-done | bytes 20512 | tf_op jit(solution)/shard_map/ppermute | solution.py:39
  38.4 2.7 %shard_map.154 = (f32[96,4096]{1,0:T(8,128)S(1)}, f32[96,4096]{1,0:T(8,128)S(1)}, f32[128,4096]{1,0:T(8,128)S(1)}) custom-call(bf16[96,4096]{1,0:T(8,128)(2,1)S(1)} %copy-done.2, bf16[96,4096]{1,0:T(8,128)(2,1)} %collective-permute-done.refs_1_, bf16[128,4096]{1,0:T(8,128)(2,1)S(1)} %copy-done.6), custom_call_target="tpu_custom_call" | custom-call | tf_op jit(solution)/shard_map/pallas_call | solution.py:448
  41.1 4.3 %shard_map.157 = (bf16[384,256]{1,0:T(8,128)(2,1)S(1)}, bf16[544,128]{1,0:T(8,128)(2,1)S(1)}, bf16[16,128]{1,0:T(8,128)(2,1)}) custom-call(s32[5]{0:T(128)S(1)} %compare_select_fusion.info, f32[96,4096]{1,0:T(8,128)S(1)} %get-tuple-element.32.refs_0_, f32[96,4096]{1,0:T(8,128)S(1)} %get-tuple-element.33.refs_1_, ...), custom_call_target="tpu_custom_call" | custom-call | tf_op jit(solution)/shard_map/pallas_call | solution.py:448
  45.4 1.7 %collective-permute-start.24 = (bf16[544,128]{1,0:T(8,128)(2,1)S(1)}, bf16[544,128]{1,0:T(8,128)(2,1)S(1)}, u32[]{:S(2)}, u32[]{:S(2)}) collective-permute-start(bf16[544,128]{1,0:T(8,128)(2,1)S(1)} %get-tuple-element.45.refs_5_), channel_id=1, source_target_pairs={{0,2},{1,3},{2,0},{3,1},{4,6},{5,7},{6,4},{7,5},{8,10},{9,11},{10,... | collective-permute-start | bytes 417800 | tf_op jit(solution)/shard_map/ppermute | solution.py:39
  49.5 2.0 %collective-permute-done.24.refs_7_ = bf16[544,128]{1,0:T(8,128)(2,1)S(1)} collective-permute-done((bf16[544,128]{1,0:T(8,128)(2,1)S(1)}, bf16[544,128]{1,0:T(8,128)(2,1)S(1)}, u32[]{:S(2)}, u32[]{:S(2)}) %collective-permute-start.24) | collective-permute-done | bytes 139296 | tf_op jit(solution)/shard_map/ppermute | solution.py:39
  51.5 2.9 %collective-permute-start.11 = (bf16[544,128]{1,0:T(8,128)(2,1)S(1)}, bf16[544,128]{1,0:T(8,128)(2,1)S(1)}, u32[]{:S(2)}, u32[]{:S(2)}) collective-permute-start(bf16[544,128]{1,0:T(8,128)(2,1)S(1)} %get-tuple-element.45.refs_5_), channel_id=1, source_target_pairs={{0,8},{4,12},{8,0},{12,4},{1,9},{5,13},{9,1},{13,5},{2,10},{6,14},... | collective-permute-start | bytes 417800 | tf_op jit(solution)/shard_map/ppermute | solution.py:39
  54.3 1.8 %collective-permute-start.15 = (bf16[544,128]{1,0:T(8,128)(2,1)S(1)}, bf16[544,128]{1,0:T(8,128)(2,1)S(1)}, u32[]{:S(2)}, u32[]{:S(2)}) collective-permute-start(bf16[544,128]{1,0:T(8,128)(2,1)S(1)} %get-tuple-element.45.refs_5_), channel_id=1, source_target_pairs={{0,12},{4,8},{8,4},{12,0},{1,13},{5,9},{9,5},{13,1},{2,14},{6,10},... | collective-permute-start | bytes 417800 | tf_op jit(solution)/shard_map/ppermute | solution.py:39
  56.7 8.2 %collective-permute-done.11.refs_5_ = bf16[544,128]{1,0:T(8,128)(2,1)S(1)} collective-permute-done((bf16[544,128]{1,0:T(8,128)(2,1)S(1)}, bf16[544,128]{1,0:T(8,128)(2,1)S(1)}, u32[]{:S(2)}, u32[]{:S(2)}) %collective-permute-start.11) | collective-permute-done | bytes 139296 | tf_op jit(solution)/shard_map/ppermute | solution.py:39
  64.9 1.7 %collective-permute-start.21 = (bf16[544,128]{1,0:T(8,128)(2,1)S(1)}, bf16[544,128]{1,0:T(8,128)(2,1)S(1)}, u32[]{:S(2)}, u32[]{:S(2)}) collective-permute-start(bf16[544,128]{1,0:T(8,128)(2,1)S(1)} %collective-permute-done.19.refs_5_), channel_id=1, source_target_pairs={{0,2},{1,3},{2,0},{3,1},{4,6},{5,7},{6,4},{7,5},{8,10},{9,11},{10,... | collective-permute-start | bytes 417800 | tf_op jit(solution)/shard_map/ppermute | solution.py:39
  67.0 1.7 %collective-permute-start.17 = (bf16[544,128]{1,0:T(8,128)(2,1)S(1)}, bf16[544,128]{1,0:T(8,128)(2,1)S(1)}, u32[]{:S(2)}, u32[]{:S(2)}) collective-permute-start(bf16[544,128]{1,0:T(8,128)(2,1)S(1)} %collective-permute-done.15.refs_9_), channel_id=1, source_target_pairs={{0,2},{1,3},{2,0},{3,1},{4,6},{5,7},{6,4},{7,5},{8,10},{9,11},{10,... | collective-permute-start | bytes 417800 | tf_op jit(solution)/shard_map/ppermute | solution.py:39
  68.7 2.0 %collective-permute-done.21.refs_7_ = bf16[544,128]{1,0:T(8,128)(2,1)S(1)} collective-permute-done((bf16[544,128]{1,0:T(8,128)(2,1)S(1)}, bf16[544,128]{1,0:T(8,128)(2,1)S(1)}, u32[]{:S(2)}, u32[]{:S(2)}) %collective-permute-start.21) | collective-permute-done | bytes 139296 | tf_op jit(solution)/shard_map/ppermute | solution.py:39
  71.2 2.4 %collective-permute-done.13.refs_7_ = bf16[544,128]{1,0:T(8,128)(2,1)S(1)} collective-permute-done((bf16[544,128]{1,0:T(8,128)(2,1)S(1)}, bf16[544,128]{1,0:T(8,128)(2,1)S(1)}, u32[]{:S(2)}, u32[]{:S(2)}) %collective-permute-start.13) | collective-permute-done | bytes 139296 | tf_op jit(solution)/shard_map/ppermute | solution.py:39
  73.5 2.4 %collective-permute-done.17.refs_11_ = bf16[544,128]{1,0:T(8,128)(2,1)S(1)} collective-permute-done((bf16[544,128]{1,0:T(8,128)(2,1)S(1)}, bf16[544,128]{1,0:T(8,128)(2,1)S(1)}, u32[]{:S(2)}, u32[]{:S(2)}) %collective-permute-start.17) | collective-permute-done | bytes 139296 | tf_op jit(solution)/shard_map/ppermute | solution.py:39
  77.6 2.1 %shard_map.159.refs_1_ = bf16[4,256,768]{2,1,0:T(8,128)(2,1)S(1)} custom-call(s32[5]{0:T(128)S(1)} %compare_select_fusion.info, bf16[384,256]{1,0:T(8,128)(2,1)S(1)} %get-tuple-element.40.refs_0_, bf16[384,256]{1,0:T(8,128)(2,1)S(1)} %collective-permute-done.8.refs_1_, bf16[384,256]{1,0:T(8,128)(2,1)S(1)} %collective-permute-done.9.refs_2_, ...), custom_call_target="tpu_custom_call" | custom-call | tf_op jit(solution)/shard_map/pallas_call | solution.py:448
  79.8 3.9 %shard_map.160 = (f32[4,8,768]{2,1,0:T(8,128)S(1)}, f32[4,8,768]{2,1,0:T(8,128)S(1)}, f32[4,128,384]{2,1,0:T(8,128)S(1)}) custom-call(s32[5]{0:T(128)S(1)} %compare_select_fusion.info, f32[8]{0:T(128)S(1)} %copy-done.11, bf16[4,256,768]{2,1,0:T(8,128)(2,1)S(1)} %shard_map.159.refs_1_, f32[1,512]{1,0:T(1,128)S(1)} %bitcast.13, ...), custom_call_target="tpu_custom_call" | custom-call | tf_op jit(solution)/shard_map/pallas_call | solution.py:448
  83.7 4.0 %shard_map.161 = (f32[4,8,768]{2,1,0:T(8,128)S(1)}, f32[4,8,768]{2,1,0:T(8,128)S(1)}, f32[4,128,384]{2,1,0:T(8,128)S(1)}) custom-call(s32[5]{0:T(128)S(1)} %compare_select_fusion.info, f32[8]{0:T(128)S(1)} %copy-done.11, bf16[4,256,768]{2,1,0:T(8,128)(2,1)S(1)} %shard_map.159.refs_1_, f32[1,512]{1,0:T(1,128)S(1)} %bitcast.14, ...), custom_call_target="tpu_custom_call" | custom-call | tf_op jit(solution)/shard_map/pallas_call | solution.py:448
  87.8 7.0 %shard_map.162.refs_0_ = bf16[384,512]{1,0:T(8,128)(2,1)S(1)} custom-call(s32[5]{0:T(128)S(1)} %compare_select_fusion.info, f32[8]{0:T(128)S(1)} %copy-done.11, bf16[4,256,768]{2,1,0:T(8,128)(2,1)S(1)} %shard_map.159.refs_1_, f32[1,512]{1,0:T(1,128)S(1)} %bitcast.15, bf16[512,512]{1,0:T(8,128)(2,1)S(1)} %get-tuple-element.43.refs_3_, ...), custom_call_target="tpu_custom_call" | custom-call | tf_op jit(solution)/shard_map/pallas_call | solution.py:448
  94.8 1.6 %collective-permute-start.27 = (bf16[384,512]{1,0:T(8,128)(2,1)S(1)}, bf16[384,512]{1,0:T(8,128)(2,1)S(1)}, u32[]{:S(2)}, u32[]{:S(2)}) collective-permute-start(bf16[384,512]{1,0:T(8,128)(2,1)S(1)} %shard_map.162.refs_0_), channel_id=1, source_target_pairs={{0,2},{1,3},{2,0},{3,1},{4,6},{5,7},{6,4},{7,5},{8,10},{9,11},{10,... | collective-permute-start | bytes 1179656 | tf_op jit(solution)/shard_map/ppermute | solution.py:39
  96.5 9.5 %collective-permute-done.27.refs_2_ = bf16[384,512]{1,0:T(8,128)(2,1)S(1)} collective-permute-done((bf16[384,512]{1,0:T(8,128)(2,1)S(1)}, bf16[384,512]{1,0:T(8,128)(2,1)S(1)}, u32[]{:S(2)}, u32[]{:S(2)}) %collective-permute-start.27) | collective-permute-done | bytes 393248 | tf_op jit(solution)/shard_map/ppermute | solution.py:39
  105.9 1.7 %collective-permute-done.28.refs_3_ = bf16[384,512]{1,0:T(8,128)(2,1)S(1)} collective-permute-done((bf16[384,512]{1,0:T(8,128)(2,1)S(1)}, bf16[384,512]{1,0:T(8,128)(2,1)S(1)}, u32[]{:S(2)}, u32[]{:S(2)}) %collective-permute-start.28) | collective-permute-done | bytes 393248 | tf_op jit(solution)/shard_map/ppermute | solution.py:39
  107.7 2.4 %shard_map.163 = (bf16[96,1024]{1,0:T(8,128)(2,1)S(1)}, bf16[96,1024]{1,0:T(8,128)(2,1)S(1)}, bf16[96,1024]{1,0:T(8,128)(2,1)S(1)}, bf16[96,1024]{1,0:T(8,128)(2,1)S(1)}) custom-call(s32[5]{0:T(128)S(1)} %compare_select_fusion.info, bf16[384,512]{1,0:T(8,128)(2,1)S(1)} %shard_map.162.refs_0_, bf16[384,512]{1,0:T(8,128)(2,1)S(1)} %collective-permute-done.26.refs_1_, ...), custom_call_target="tpu_custom_call" | custom-call | tf_op jit(solution)/shard_map/pallas_call | solution.py:448
  112.0 6.0 %collective-permute-done.30.refs_2_ = bf16[96,1024]{1,0:T(8,128)(2,1)S(1)} collective-permute-done((bf16[96,1024]{1,0:T(8,128)(2,1)S(1)}, bf16[96,1024]{1,0:T(8,128)(2,1)S(1)}, u32[]{:S(2)}, u32[]{:S(2)}) %collective-permute-start.30) | collective-permute-done | bytes 196640 | tf_op jit(solution)/shard_map/ppermute | solution.py:39
  118.1 3.0 %collective-permute-done.31.refs_3_ = bf16[96,1024]{1,0:T(8,128)(2,1)S(1)} collective-permute-done((bf16[96,1024]{1,0:T(8,128)(2,1)S(1)}, bf16[96,1024]{1,0:T(8,128)(2,1)S(1)}, u32[]{:S(2)}, u32[]{:S(2)}) %collective-permute-start.31) | collective-permute-done | bytes 196640 | tf_op jit(solution)/shard_map/ppermute | solution.py:39
  121.1 1.7 %shard_map.164 = bf16[96,4096]{1,0:T(8,128)(2,1)} custom-call(s32[5]{0:T(128)S(1)} %compare_select_fusion.info, bf16[96,1024]{1,0:T(8,128)(2,1)S(1)} %get-tuple-element.53.refs_0_, bf16[96,1024]{1,0:T(8,128)(2,1)S(1)} %collective-permute-done.29.refs_1_, bf16[96,1024]{1,0:T(8,128)(2,1)S(1)} %collective-permute-done.30.refs_2_, ...), custom_call_target="tpu_custom_call" | custom-call | tf_op jit(solution)/shard_map/pallas_call | solution.py:448
  (79 shorter events, 11.5 us)
Async XLA Ops:
  0.0 20.7 %collective-permute-start.1 = (bf16[96,4096]{1,0:T(8,128)(2,1)}, bf16[96,4096]{1,0:T(8,128)(2,1)S(1)}, u32[]{:S(2)}, u32[]{:S(2)}) collective-permute-start(bf16[96,4096]{1,0:T(8,128)(2,1)} %refs_8_.1), channel_id=1, source_target_pairs={{0,2},{1,3},{2,0},{3,1},{4,6},{5,7},{6,4},{7,5},{8,10},{9,11},{10,... | collective-permute-start | bytes 2359304 | tf_op jit(solution)/shard_map/ppermute | solution.py:39
  3.0 35.4 %collective-permute-start = (bf16[96,4096]{1,0:T(8,128)(2,1)}, bf16[96,4096]{1,0:T(8,128)(2,1)}, u32[]{:S(2)}, u32[]{:S(2)}) collective-permute-start(bf16[96,4096]{1,0:T(8,128)(2,1)} %refs_8_.1), channel_id=1, source_target_pairs={{0,1},{1,0},{2,3},{3,2},{4,5},{5,4},{6,7},{7,6},{8,9},{9,8},{10,11... | collective-permute-start | bytes 2359304 | tf_op jit(solution)/shard_map/ppermute | solution.py:39
  20.7 20.4 %collective-permute-start.2 = (bf16[96,4096]{1,0:T(8,128)(2,1)S(1)}, bf16[96,4096]{1,0:T(8,128)(2,1)S(1)}, u32[]{:S(2)}, u32[]{:S(2)}) collective-permute-start(bf16[96,4096]{1,0:T(8,128)(2,1)S(1)} %collective-permute-done.1.refs_2_), channel_id=1, source_target_pairs={{0,1},{1,0},{2,3},{3,2},{4,5},{5,4},{6,7},{7,6},{8,9},{9,8},{10,11... | collective-permute-start | bytes 2359304 | tf_op jit(solution)/shard_map/ppermute | solution.py:39
  23.1 4.0 %collective-permute-start.3 = (f32[5,1024]{1,0:T(8,128)S(1)}, f32[5,1024]{1,0:T(8,128)S(1)}, u32[]{:S(2)}, u32[]{:S(2)}) collective-permute-start(f32[5,1024]{1,0:T(8,128)S(1)} %pad_maximum_fusion), channel_id=1, source_target_pairs={{0,4},{4,0},{8,12},{12,8},{1,5},{5,1},{9,13},{13,9},{2,6},{6,2},{1... | collective-permute-start | bytes 61448 | tf_op jit(solution)/shard_map/ppermute | solution.py:39
  27.1 4.9 %collective-permute-start.4 = (f32[5,1024]{1,0:T(8,128)S(1)}, f32[5,1024]{1,0:T(8,128)S(1)}, u32[]{:S(2)}, u32[]{:S(2)}) collective-permute-start(f32[5,1024]{1,0:T(8,128)S(1)} %fusion.2), channel_id=1, source_target_pairs={{0,8},{4,12},{8,0},{12,4},{1,9},{5,13},{9,1},{13,5},{2,10},{6,14},... | collective-permute-start | bytes 61448 | tf_op jit(solution)/shard_map/ppermute | solution.py:39
  32.0 3.9 %collective-permute-start.6 = (f32[5,1024]{1,0:T(8,128)S(1)}, f32[5,1024]{1,0:T(8,128)S(1)}, u32[]{:S(2)}, u32[]{:S(2)}) collective-permute-start(f32[5,1024]{1,0:T(8,128)S(1)} %add.18.refs_4_), channel_id=1, source_target_pairs={{0,2},{1,3},{2,0},{3,1},{4,6},{5,7},{6,4},{7,5},{8,10},{9,11},{10,... | collective-permute-start | bytes 61448 | tf_op jit(solution)/shard_map/ppermute | solution.py:39
  33.7 7.3 %collective-permute-start.5 = (f32[5,1024]{1,0:T(8,128)S(1)}, f32[5,1024]{1,0:T(8,128)S(1)}, u32[]{:S(2)}, u32[]{:S(2)}) collective-permute-start(f32[5,1024]{1,0:T(8,128)S(1)} %add.18.refs_4_), channel_id=1, source_target_pairs={{0,1},{1,0},{2,3},{3,2},{4,5},{5,4},{6,7},{7,6},{8,9},{9,8},{10,11... | collective-permute-start | bytes 61448 | tf_op jit(solution)/shard_map/ppermute | solution.py:39
  35.9 5.1 %collective-permute-start.7 = (f32[5,1024]{1,0:T(8,128)S(1)}, f32[5,1024]{1,0:T(8,128)S(1)}, u32[]{:S(2)}, u32[]{:S(2)}) collective-permute-start(f32[5,1024]{1,0:T(8,128)S(1)} %collective-permute-done.6.refs_6_), channel_id=1, source_target_pairs={{0,1},{1,0},{2,3},{3,2},{4,5},{5,4},{6,7},{7,6},{8,9},{9,8},{10,11... | collective-permute-start | bytes 61448 | tf_op jit(solution)/shard_map/ppermute | solution.py:39
  45.4 6.1 %collective-permute-start.24 = (bf16[544,128]{1,0:T(8,128)(2,1)S(1)}, bf16[544,128]{1,0:T(8,128)(2,1)S(1)}, u32[]{:S(2)}, u32[]{:S(2)}) collective-permute-start(bf16[544,128]{1,0:T(8,128)(2,1)S(1)} %get-tuple-element.45.refs_5_), channel_id=1, source_target_pairs={{0,2},{1,3},{2,0},{3,1},{4,6},{5,7},{6,4},{7,5},{8,10},{9,11},{10,... | collective-permute-start | bytes 417800 | tf_op jit(solution)/shard_map/ppermute | solution.py:39
  47.1 7.2 %collective-permute-start.23 = (bf16[544,128]{1,0:T(8,128)(2,1)S(1)}, bf16[544,128]{1,0:T(8,128)(2,1)S(1)}, u32[]{:S(2)}, u32[]{:S(2)}) collective-permute-start(bf16[544,128]{1,0:T(8,128)(2,1)S(1)} %get-tuple-element.45.refs_5_), channel_id=1, source_target_pairs={{0,1},{1,0},{2,3},{3,2},{4,5},{5,4},{6,7},{7,6},{8,9},{9,8},{10,11... | collective-permute-start | bytes 417800 | tf_op jit(solution)/shard_map/ppermute | solution.py:39
  47.4 8.8 %collective-permute-start.19 = (bf16[544,128]{1,0:T(8,128)(2,1)S(1)}, bf16[544,128]{1,0:T(8,128)(2,1)S(1)}, u32[]{:S(2)}, u32[]{:S(2)}) collective-permute-start(bf16[544,128]{1,0:T(8,128)(2,1)S(1)} %get-tuple-element.45.refs_5_), channel_id=1, source_target_pairs={{0,4},{4,0},{8,12},{12,8},{1,5},{5,1},{9,13},{13,9},{2,6},{6,2},{1... | collective-permute-start | bytes 417800 | tf_op jit(solution)/shard_map/ppermute | solution.py:39
  48.9 7.2 %collective-permute-start.9 = (bf16[384,256]{1,0:T(8,128)(2,1)S(1)}, bf16[384,256]{1,0:T(8,128)(2,1)S(1)}, u32[]{:S(2)}, u32[]{:S(2)}) collective-permute-start(bf16[384,256]{1,0:T(8,128)(2,1)S(1)} %get-tuple-element.40.refs_0_), channel_id=1, source_target_pairs={{0,2},{1,3},{2,0},{3,1},{4,6},{5,7},{6,4},{7,5},{8,10},{9,11},{10,... | collective-permute-start | bytes 589832 | tf_op jit(solution)/shard_map/ppermute | solution.py:39
  49.5 17.1 %collective-permute-start.8 = (bf16[384,256]{1,0:T(8,128)(2,1)S(1)}, bf16[384,256]{1,0:T(8,128)(2,1)S(1)}, u32[]{:S(2)}, u32[]{:S(2)}) collective-permute-start(bf16[384,256]{1,0:T(8,128)(2,1)S(1)} %get-tuple-element.40.refs_0_), channel_id=1, source_target_pairs={{0,1},{1,0},{2,3},{3,2},{4,5},{5,4},{6,7},{7,6},{8,9},{9,8},{10,11... | collective-permute-start | bytes 589832 | tf_op jit(solution)/shard_map/ppermute | solution.py:39
  51.5 13.4 %collective-permute-start.11 = (bf16[544,128]{1,0:T(8,128)(2,1)S(1)}, bf16[544,128]{1,0:T(8,128)(2,1)S(1)}, u32[]{:S(2)}, u32[]{:S(2)}) collective-permute-start(bf16[544,128]{1,0:T(8,128)(2,1)S(1)} %get-tuple-element.45.refs_5_), channel_id=1, source_target_pairs={{0,8},{4,12},{8,0},{12,4},{1,9},{5,13},{9,1},{13,5},{2,10},{6,14},... | collective-permute-start | bytes 417800 | tf_op jit(solution)/shard_map/ppermute | solution.py:39
  54.3 12.3 %collective-permute-start.15 = (bf16[544,128]{1,0:T(8,128)(2,1)S(1)}, bf16[544,128]{1,0:T(8,128)(2,1)S(1)}, u32[]{:S(2)}, u32[]{:S(2)}) collective-permute-start(bf16[544,128]{1,0:T(8,128)(2,1)S(1)} %get-tuple-element.45.refs_5_), channel_id=1, source_target_pairs={{0,12},{4,8},{8,4},{12,0},{1,13},{5,9},{9,5},{13,1},{2,14},{6,10},... | collective-permute-start | bytes 417800 | tf_op jit(solution)/shard_map/ppermute | solution.py:39
  56.1 10.9 %collective-permute-start.25 = (bf16[544,128]{1,0:T(8,128)(2,1)S(1)}, bf16[544,128]{1,0:T(8,128)(2,1)S(1)}, u32[]{:S(2)}, u32[]{:S(2)}) collective-permute-start(bf16[544,128]{1,0:T(8,128)(2,1)S(1)} %collective-permute-done.24.refs_7_), channel_id=1, source_target_pairs={{0,1},{1,0},{2,3},{3,2},{4,5},{5,4},{6,7},{7,6},{8,9},{9,8},{10,11... | collective-permute-start | bytes 417800 | tf_op jit(solution)/shard_map/ppermute | solution.py:39
  56.1 19.8 %collective-permute-start.10 = (bf16[384,256]{1,0:T(8,128)(2,1)S(1)}, bf16[384,256]{1,0:T(8,128)(2,1)S(1)}, u32[]{:S(2)}, u32[]{:S(2)}) collective-permute-start(bf16[384,256]{1,0:T(8,128)(2,1)S(1)} %collective-permute-done.9.refs_2_), channel_id=1, source_target_pairs={{0,1},{1,0},{2,3},{3,2},{4,5},{5,4},{6,7},{7,6},{8,9},{9,8},{10,11... | collective-permute-start | bytes 589832 | tf_op jit(solution)/shard_map/ppermute | solution.py:39
  64.9 5.8 %collective-permute-start.21 = (bf16[544,128]{1,0:T(8,128)(2,1)S(1)}, bf16[544,128]{1,0:T(8,128)(2,1)S(1)}, u32[]{:S(2)}, u32[]{:S(2)}) collective-permute-start(bf16[544,128]{1,0:T(8,128)(2,1)S(1)} %collective-permute-done.19.refs_5_), channel_id=1, source_target_pairs={{0,2},{1,3},{2,0},{3,1},{4,6},{5,7},{6,4},{7,5},{8,10},{9,11},{10,... | collective-permute-start | bytes 417800 | tf_op jit(solution)/shard_map/ppermute | solution.py:39
  66.6 4.1 %collective-permute-start.20 = (bf16[544,128]{1,0:T(8,128)(2,1)S(1)}, bf16[544,128]{1,0:T(8,128)(2,1)S(1)}, u32[]{:S(2)}, u32[]{:S(2)}) collective-permute-start(bf16[544,128]{1,0:T(8,128)(2,1)S(1)} %collective-permute-done.19.refs_5_), channel_id=1, source_target_pairs={{0,1},{1,0},{2,3},{3,2},{4,5},{5,4},{6,7},{7,6},{8,9},{9,8},{10,11... | collective-permute-start | bytes 417800 | tf_op jit(solution)/shard_map/ppermute | solution.py:39
  66.6 6.9 %collective-permute-start.13 = (bf16[544,128]{1,0:T(8,128)(2,1)S(1)}, bf16[544,128]{1,0:T(8,128)(2,1)S(1)}, u32[]{:S(2)}, u32[]{:S(2)}) collective-permute-start(bf16[544,128]{1,0:T(8,128)(2,1)S(1)} %collective-permute-done.11.refs_5_), channel_id=1, source_target_pairs={{0,2},{1,3},{2,0},{3,1},{4,6},{5,7},{6,4},{7,5},{8,10},{9,11},{10,... | collective-permute-start | bytes 417800 | tf_op jit(solution)/shard_map/ppermute | solution.py:39
  67.0 8.9 %collective-permute-start.17 = (bf16[544,128]{1,0:T(8,128)(2,1)S(1)}, bf16[544,128]{1,0:T(8,128)(2,1)S(1)}, u32[]{:S(2)}, u32[]{:S(2)}) collective-permute-start(bf16[544,128]{1,0:T(8,128)(2,1)S(1)} %collective-permute-done.15.refs_9_), channel_id=1, source_target_pairs={{0,2},{1,3},{2,0},{3,1},{4,6},{5,7},{6,4},{7,5},{8,10},{9,11},{10,... | collective-permute-start | bytes 417800 | tf_op jit(solution)/shard_map/ppermute | solution.py:39
  70.7 13.1 %collective-permute-start.22 = (bf16[544,128]{1,0:T(8,128)(2,1)S(1)}, bf16[544,128]{1,0:T(8,128)(2,1)S(1)}, u32[]{:S(2)}, u32[]{:S(2)}) collective-permute-start(bf16[544,128]{1,0:T(8,128)(2,1)S(1)} %collective-permute-done.21.refs_7_), channel_id=1, source_target_pairs={{0,1},{1,0},{2,3},{3,2},{4,5},{5,4},{6,7},{7,6},{8,9},{9,8},{10,11... | collective-permute-start | bytes 417800 | tf_op jit(solution)/shard_map/ppermute | solution.py:39
  70.7 17.1 %collective-permute-start.12 = (bf16[544,128]{1,0:T(8,128)(2,1)S(1)}, bf16[544,128]{1,0:T(8,128)(2,1)S(1)}, u32[]{:S(2)}, u32[]{:S(2)}) collective-permute-start(bf16[544,128]{1,0:T(8,128)(2,1)S(1)} %collective-permute-done.11.refs_5_), channel_id=1, source_target_pairs={{0,1},{1,0},{2,3},{3,2},{4,5},{5,4},{6,7},{7,6},{8,9},{9,8},{10,11... | collective-permute-start | bytes 417800 | tf_op jit(solution)/shard_map/ppermute | solution.py:39
  73.5 14.3 %collective-permute-start.16 = (bf16[544,128]{1,0:T(8,128)(2,1)S(1)}, bf16[544,128]{1,0:T(8,128)(2,1)S(1)}, u32[]{:S(2)}, u32[]{:S(2)}) collective-permute-start(bf16[544,128]{1,0:T(8,128)(2,1)S(1)} %collective-permute-done.15.refs_9_), channel_id=1, source_target_pairs={{0,1},{1,0},{2,3},{3,2},{4,5},{5,4},{6,7},{7,6},{8,9},{9,8},{10,11... | collective-permute-start | bytes 417800 | tf_op jit(solution)/shard_map/ppermute | solution.py:39
  75.9 11.9 %collective-permute-start.14 = (bf16[544,128]{1,0:T(8,128)(2,1)S(1)}, bf16[544,128]{1,0:T(8,128)(2,1)S(1)}, u32[]{:S(2)}, u32[]{:S(2)}) collective-permute-start(bf16[544,128]{1,0:T(8,128)(2,1)S(1)} %collective-permute-done.13.refs_7_), channel_id=1, source_target_pairs={{0,1},{1,0},{2,3},{3,2},{4,5},{5,4},{6,7},{7,6},{8,9},{9,8},{10,11... | collective-permute-start | bytes 417800 | tf_op jit(solution)/shard_map/ppermute | solution.py:39
  75.9 11.9 %collective-permute-start.18 = (bf16[544,128]{1,0:T(8,128)(2,1)S(1)}, bf16[544,128]{1,0:T(8,128)(2,1)S(1)}, u32[]{:S(2)}, u32[]{:S(2)}) collective-permute-start(bf16[544,128]{1,0:T(8,128)(2,1)S(1)} %collective-permute-done.17.refs_11_), channel_id=1, source_target_pairs={{0,1},{1,0},{2,3},{3,2},{4,5},{5,4},{6,7},{7,6},{8,9},{9,8},{10,11... | collective-permute-start | bytes 417800 | tf_op jit(solution)/shard_map/ppermute | solution.py:39
  94.8 11.1 %collective-permute-start.27 = (bf16[384,512]{1,0:T(8,128)(2,1)S(1)}, bf16[384,512]{1,0:T(8,128)(2,1)S(1)}, u32[]{:S(2)}, u32[]{:S(2)}) collective-permute-start(bf16[384,512]{1,0:T(8,128)(2,1)S(1)} %shard_map.162.refs_0_), channel_id=1, source_target_pairs={{0,2},{1,3},{2,0},{3,1},{4,6},{5,7},{6,4},{7,5},{8,10},{9,11},{10,... | collective-permute-start | bytes 1179656 | tf_op jit(solution)/shard_map/ppermute | solution.py:39
  96.5 9.5 %collective-permute-start.26 = (bf16[384,512]{1,0:T(8,128)(2,1)S(1)}, bf16[384,512]{1,0:T(8,128)(2,1)S(1)}, u32[]{:S(2)}, u32[]{:S(2)}) collective-permute-start(bf16[384,512]{1,0:T(8,128)(2,1)S(1)} %shard_map.162.refs_0_), channel_id=1, source_target_pairs={{0,1},{1,0},{2,3},{3,2},{4,5},{5,4},{6,7},{7,6},{8,9},{9,8},{10,11... | collective-permute-start | bytes 1179656 | tf_op jit(solution)/shard_map/ppermute | solution.py:39
  105.9 1.7 %collective-permute-start.28 = (bf16[384,512]{1,0:T(8,128)(2,1)S(1)}, bf16[384,512]{1,0:T(8,128)(2,1)S(1)}, u32[]{:S(2)}, u32[]{:S(2)}) collective-permute-start(bf16[384,512]{1,0:T(8,128)(2,1)S(1)} %collective-permute-done.27.refs_2_), channel_id=1, source_target_pairs={{0,1},{1,0},{2,3},{3,2},{4,5},{5,4},{6,7},{7,6},{8,9},{9,8},{10,11... | collective-permute-start | bytes 1179656 | tf_op jit(solution)/shard_map/ppermute | solution.py:39
  110.1 1.9 %collective-permute-start.29 = (bf16[96,1024]{1,0:T(8,128)(2,1)S(1)}, bf16[96,1024]{1,0:T(8,128)(2,1)S(1)}, u32[]{:S(2)}, u32[]{:S(2)}) collective-permute-start(bf16[96,1024]{1,0:T(8,128)(2,1)S(1)} %get-tuple-element.54), channel_id=1, source_target_pairs={{0,1},{1,0},{2,3},{3,2},{4,5},{5,4},{6,7},{7,6},{8,9},{9,8},{10,11... | collective-permute-start | bytes 589832 | tf_op jit(solution)/shard_map/ppermute | solution.py:39
  110.3 7.8 %collective-permute-start.30 = (bf16[96,1024]{1,0:T(8,128)(2,1)S(1)}, bf16[96,1024]{1,0:T(8,128)(2,1)S(1)}, u32[]{:S(2)}, u32[]{:S(2)}) collective-permute-start(bf16[96,1024]{1,0:T(8,128)(2,1)S(1)} %get-tuple-element.55), channel_id=1, source_target_pairs={{0,2},{1,3},{2,0},{3,1},{4,6},{5,7},{6,4},{7,5},{8,10},{9,11},{10,... | collective-permute-start | bytes 589832 | tf_op jit(solution)/shard_map/ppermute | solution.py:39
  111.9 9.2 %collective-permute-start.31 = (bf16[96,1024]{1,0:T(8,128)(2,1)S(1)}, bf16[96,1024]{1,0:T(8,128)(2,1)S(1)}, u32[]{:S(2)}, u32[]{:S(2)}) collective-permute-start(bf16[96,1024]{1,0:T(8,128)(2,1)S(1)} %get-tuple-element.56), channel_id=1, source_target_pairs={{0,3},{1,2},{2,1},{3,0},{4,7},{5,6},{6,5},{7,4},{8,11},{9,10},{10,... | collective-permute-start | bytes 589832 | tf_op jit(solution)/shard_map/ppermute | solution.py:39
  (14 other events, 326.3 us)

commit v3 on v2

--- a/solution.py
+++ b/solution.py
@@ -307,7 +307,7 @@
     return jnp.sum(values.reshape(-1, 8, values.shape[1]), axis=0)
 
 
-def attend_kernel(counts, tok_keys, seg, merged, first, last, info, *refs):
+def attend_kernel(counts, tok_keys, seg, merged, first, last, chosen, info, *refs):
     ids = member_ids(info, counts[0])
     bias_ref, q_ref, gain_ref, wk_ref, wv_ref = refs[:5]
     refs = refs[5:]
@@ -322,16 +322,17 @@
     else:
         state_out, refs = refs[:3], refs[3:]
     scratch, k_ref, v_ref, r_ref = refs
-    pairs, _, lanes = q_ref.shape
+    lanes = q_ref.shape[2]
     rows = lanes // 2
+    heads_of = slice(chosen[0] * LANES, (chosen[-1] + 1) * LANES)
     for number, block in enumerate(blocks):
         pieces = block if merged else block[:-1]
         base = number * seg
         rows_ref = scratch.at[number]
         normed_into(rows_ref, ids, pieces, gain_ref)
-        k_ref[base : base + seg, :] = f32_dot(rows_ref[...], wk_ref[...]).astype(jnp.bfloat16)
+        k_ref[base : base + seg, :] = f32_dot(rows_ref[...], wk_ref[:, heads_of]).astype(jnp.bfloat16)
         v_ref[number] = lax.dot_general(
-            wv_ref[...], rows_ref[...], (((1,), (1,)), ((), ())), preferred_element_type=jnp.float32
+            wv_ref[heads_of, :], rows_ref[...], (((1,), (1,)), ((), ())), preferred_element_type=jnp.float32
         ).astype(jnp.bfloat16)
         if merged:
             quarter = seg // len(pieces)
@@ -349,14 +350,15 @@
 
     def score(pair, number):
         base = number * seg
-        span = slice(pair * LANES, (pair + 1) * LANES)
+        local = pair - chosen[0]
+        span = slice(local * LANES, (local + 1) * LANES)
         key = jnp.concatenate([k_ref[base : base + seg, span], r_ref[base : base + seg, :]], axis=1)
         return f32_dot(key, q_ref[pair])
 
-    steps = [(pair, number) for pair in range(pairs) for number in range(len(blocks))]
+    steps = [(pair, number) for pair in chosen for number in range(len(blocks))]
     ahead = score(*steps[0])
-    for pair in range(pairs):
-        span = slice(pair * LANES, (pair + 1) * LANES)
+    for local, pair in enumerate(chosen):
+        span = slice(local * LANES, (local + 1) * LANES)
         bias = jnp.where(lane < rows, bias_ref[2 * pair], bias_ref[2 * pair + 1]) * LOG2E
         top = total = acc = None
         if not first:
@@ -364,7 +366,7 @@
             total, acc = state_in[1][pair], state_in[2][pair]
         for number in range(len(blocks)):
             scores = ahead
-            after = pair * len(blocks) + number + 1
+            after = local * len(blocks) + number + 1
             if after < len(steps):
                 ahead = score(*steps[after])
             lat, ctx = scores[:tok_keys], scores[tok_keys:]
@@ -401,21 +403,23 @@
             state_out[2][pair] = acc
 
 
-def out_kernel(count, parts, info, *refs):
+def out_kernel(count, splits, parts, info, *refs):
     ids = member_ids(info, count)
-    pieces = refs[:count]
-    w_ref = refs[count]
-    outs = refs[1 + count : 1 + count + parts]
+    pieces = refs[: count * splits]
+    w_ref = refs[count * splits]
+    refs = refs[1 + count * splits :]
+    outs = refs[:parts]
     depth = pieces[0].shape[1]
     total = None
     for number, piece in enumerate(pieces):
-        rows = pl.ds(aligned(ids[number] * depth, LANES), depth)
-        part = f32_dot(piece[...], w_ref[rows, :])
+        split, member = divmod(number, count)
+        start = aligned((ids[member] * splits + split) * depth, LANES)
+        part = f32_dot(piece[...], w_ref[pl.ds(start, depth), :])
         total = part if total is None else total + part
     if parts == 1:
         outs[0][...] = total.astype(jnp.bfloat16)
         return
-    scratch = refs[1 + count + parts]
+    scratch = refs[parts]
     scratch[...] = total
     rows = outs[0].shape[0]
     for number, out_ref in enumerate(outs):
@@ -614,12 +618,10 @@
         shape_of((pairs, 8, 2 * tok_count), jnp.float32),
         shape_of((pairs, LANES, tok_count), jnp.float32),
     ]
-    state = []
-    begin = 0
-    while begin < sp_count:
-        part = blocks[begin : begin + (1 if begin < 2 else 2)]
-        first, last = begin == 0, begin + len(part) >= sp_count
-        state = call(
+
+    def attend(part, first, last, chosen, state):
+        heads = len(chosen) * LANES
+        return call(
             functools.partial(
                 attend_kernel,
                 [len(block) - (0 if merged else 1) for block in part],
@@ -628,8 +630,9 @@
                 merged,
                 first,
                 last,
+                chosen,
             ),
-            shape_of((tok_count, head_count * VALUE_DIM), bf16) if last else held,
+            shape_of((tok_count, heads), bf16) if last else held,
             [
                 info,
                 context_bias,
@@ -643,20 +646,33 @@
             smem=(0, 1),
             scratch=[
                 VMEM((len(part), seg_rows, latent_norm_gain.shape[0]), bf16),
-                VMEM((len(part) * seg_rows, head_count * PLAIN_QK_DIM), bf16),
-                VMEM((len(part), head_count * VALUE_DIM, seg_rows), bf16),
+                VMEM((len(part) * seg_rows, heads), bf16),
+                VMEM((len(part), heads, seg_rows), bf16),
                 VMEM((len(part) * seg_rows, LANES), bf16),
             ],
             mib=16,
         )
+
+    every = list(range(pairs))
+    state = []
+    begin = 0
+    att_pieces = []
+    while begin < sp_count:
+        part = blocks[begin : begin + (1 if begin < 2 else 2)]
+        first, last = begin == 0, begin + len(part) >= sp_count
+        if not last:
+            state = attend(part, first, False, every, state)
         begin += len(part)
-    att_pieces = spread(state)
+    splits = [every[: pairs // 2], every[pairs // 2 :]] if pairs > 1 else [every]
+    for chosen in splits:
+        done = attend(part, first, True, chosen, state)
+        att_pieces.append(spread(done))
     out_cols = w_out.shape[1]
     parts = tp_count if small and own_rows % 8 == 0 else 1
     proj = call(
-        functools.partial(out_kernel, tp_count, parts),
+        functools.partial(out_kernel, tp_count, len(att_pieces), parts),
         [shape_of((tok_count // parts, out_cols), bf16) for _ in range(parts)],
-        [info, *att_pieces, w_o],
+        [info, *[piece for group in att_pieces for piece in group], w_o],
         smem=(0,),
         scratch=[VMEM((tok_count, out_cols), jnp.float32)] if parts > 1 else [],
     )

time: 123 us -> 122 us (level)
  waiting for transfers between devices: 60 us -> 55.8 us
  Pallas kernels: 31.6 us -> 33.4 us
    ppermute x32 -> x35, waiting for transfers between devices: 60 us -> 55.8 us  [swap(): return lax.ppermute(value, axis, [(i, i ^ bit) for i in range(count)])]
    pallas_call x11 -> x12, Pallas kernels: 31.6 us -> 33.4 us  [call(): pl.pallas_call(kernel, out_shape=outs, in_specs=specs, out_specs=[in_vmem...]
    ppermute x32 -> x35, starting transfers between devices: 27.1 us -> 28.2 us  [swap(): return lax.ppermute(value, axis, [(i, i ^ bit) for i in range(count)])]
  transfers between devices with their start and end apart: 32 -> 35, of which waited for: 13 -> 13; matrix products, arithmetic and copies ran while one was open for 3% -> 3% of each run, Pallas kernels for 13% -> 17%
where the time goes in v3:
time: 122 us; the launch traced here: 121 us
  waiting for transfers between devices  55.8 us (46%)
  Pallas kernels  33.4 us (27%)
  starting transfers between devices  28.2 us (23%)
  matrix products  2.74 us (2%)
    ppermute x35, waiting for transfers between devices, swap(): return lax.ppermute(value, axis, [(i, i ^ bit) for i in range(count)])  55.8 us
    pallas_call x12, Pallas kernels, call(): pl.pallas_call(kernel, out_shape=outs, in_specs=specs, out_specs=[in_vmem...  33.4 us
    ppermute x35, starting transfers between devices, swap(): return lax.ppermute(value, axis, [(i, i ^ bit) for i in range(count)])  28.2 us
    dot_general x3, matrix products, f32_dot(): return jnp.dot(a, b, preferred_element_type=jnp.float32)  2.74 us
  transfers between devices with their start and end apart: 35, of which 13 were waited for; matrix products, arithmetic and copies ran while one was open for 3% of the time, Pallas kernels for 17%

profile of v3, /device:TPU:0, one launch (start us, length us, event | category | flops | bytes accessed | tf_op | source)
XLA Modules:
  0.0 121.4 jit_solution(7512871855662604514)
XLA Ops:
  0.0 3.0 %collective-permute-start.1 = (bf16[96,4096]{1,0:T(8,128)(2,1)}, bf16[96,4096]{1,0:T(8,128)(2,1)S(1)}, u32[]{:S(2)}, u32[]{:S(2)}) collective-permute-start(bf16[96,4096]{1,0:T(8,128)(2,1)} %refs_8_.1), channel_id=1, source_target_pairs={{0,2},{1,3},{2,0},{3,1},{4,6},{5,7},{6,4},{7,5},{8,10},{9,11},{10,... | collective-permute-start | bytes 2359304 | tf_op jit(solution)/shard_map/ppermute | solution.py:39
  4.3 16.5 %collective-permute-done.1.refs_2_ = bf16[96,4096]{1,0:T(8,128)(2,1)S(1)} collective-permute-done((bf16[96,4096]{1,0:T(8,128)(2,1)}, bf16[96,4096]{1,0:T(8,128)(2,1)S(1)}, u32[]{:S(2)}, u32[]{:S(2)}) %collective-permute-start.1) | collective-permute-done | bytes 786464 | tf_op jit(solution)/shard_map/ppermute | solution.py:39
  21.1 2.0 %fusion.4 = f32[2,1024]{1,0:T(2,128)S(1)} fusion(bf16[2,1024]{1,0:T(2,128)(2,1)S(1)} %fusion, bf16[1024,1024]{1,0:T(8,128)(2,1)} %param.20), kind=kOutput, calls=%fused_computation.8 | convolution fusion | flops 4194304 | bytes 2109440 | tf_op jit(solution)/shard_map/dot_general | solution.py:34
  23.1 1.9 %collective-permute-start.3 = (f32[5,1024]{1,0:T(8,128)S(1)}, f32[5,1024]{1,0:T(8,128)S(1)}, u32[]{:S(2)}, u32[]{:S(2)}) collective-permute-start(f32[5,1024]{1,0:T(8,128)S(1)} %pad_maximum_fusion), channel_id=1, source_target_pairs={{0,4},{4,0},{8,12},{12,8},{1,5},{5,1},{9,13},{13,9},{2,6},{6,2},{1... | collective-permute-start | bytes 61448 | tf_op jit(solution)/shard_map/ppermute | solution.py:39
  25.0 2.1 %collective-permute-done.3 = f32[5,1024]{1,0:T(8,128)S(1)} collective-permute-done((f32[5,1024]{1,0:T(8,128)S(1)}, f32[5,1024]{1,0:T(8,128)S(1)}, u32[]{:S(2)}, u32[]{:S(2)}) %collective-permute-start.3) | collective-permute-done | bytes 20512 | tf_op jit(solution)/shard_map/ppermute | solution.py:39
  27.1 2.9 %collective-permute-start.4 = (f32[5,1024]{1,0:T(8,128)S(1)}, f32[5,1024]{1,0:T(8,128)S(1)}, u32[]{:S(2)}, u32[]{:S(2)}) collective-permute-start(f32[5,1024]{1,0:T(8,128)S(1)} %fusion.2), channel_id=1, source_target_pairs={{0,8},{4,12},{8,0},{12,4},{1,9},{5,13},{9,1},{13,5},{2,10},{6,14},... | collective-permute-start | bytes 61448 | tf_op jit(solution)/shard_map/ppermute | solution.py:39
  30.0 2.0 %collective-permute-done.4 = f32[5,1024]{1,0:T(8,128)S(1)} collective-permute-done((f32[5,1024]{1,0:T(8,128)S(1)}, f32[5,1024]{1,0:T(8,128)S(1)}, u32[]{:S(2)}, u32[]{:S(2)}) %collective-permute-start.4) | collective-permute-done | bytes 20512 | tf_op jit(solution)/shard_map/ppermute | solution.py:39
  32.0 1.7 %collective-permute-start.6 = (f32[5,1024]{1,0:T(8,128)S(1)}, f32[5,1024]{1,0:T(8,128)S(1)}, u32[]{:S(2)}, u32[]{:S(2)}) collective-permute-start(f32[5,1024]{1,0:T(8,128)S(1)} %add.18.refs_4_), channel_id=1, source_target_pairs={{0,2},{1,3},{2,0},{3,1},{4,6},{5,7},{6,4},{7,5},{8,10},{9,11},{10,... | collective-permute-start | bytes 61448 | tf_op jit(solution)/shard_map/ppermute | solution.py:39
  33.7 2.2 %collective-permute-done.6.refs_6_ = f32[5,1024]{1,0:T(8,128)S(1)} collective-permute-done((f32[5,1024]{1,0:T(8,128)S(1)}, f32[5,1024]{1,0:T(8,128)S(1)}, u32[]{:S(2)}, u32[]{:S(2)}) %collective-permute-start.6) | collective-permute-done | bytes 20512 | tf_op jit(solution)/shard_map/ppermute | solution.py:39
  38.4 2.7 %shard_map.154 = (f32[96,4096]{1,0:T(8,128)S(1)}, f32[96,4096]{1,0:T(8,128)S(1)}, f32[128,4096]{1,0:T(8,128)S(1)}) custom-call(bf16[96,4096]{1,0:T(8,128)(2,1)S(1)} %copy-done.2, bf16[96,4096]{1,0:T(8,128)(2,1)} %collective-permute-done.refs_1_, bf16[128,4096]{1,0:T(8,128)(2,1)S(1)} %copy-done.6), custom_call_target="tpu_custom_call" | custom-call | tf_op jit(solution)/shard_map/pallas_call | solution.py:452
  41.1 4.3 %shard_map.157 = (bf16[384,256]{1,0:T(8,128)(2,1)S(1)}, bf16[544,128]{1,0:T(8,128)(2,1)S(1)}, bf16[16,128]{1,0:T(8,128)(2,1)}) custom-call(s32[5]{0:T(128)S(1)} %compare_select_fusion.info, f32[96,4096]{1,0:T(8,128)S(1)} %get-tuple-element.32.refs_0_, f32[96,4096]{1,0:T(8,128)S(1)} %get-tuple-element.33.refs_1_, ...), custom_call_target="tpu_custom_call" | custom-call | tf_op jit(solution)/shard_map/pallas_call | solution.py:452
  45.4 1.7 %collective-permute-start.24 = (bf16[544,128]{1,0:T(8,128)(2,1)S(1)}, bf16[544,128]{1,0:T(8,128)(2,1)S(1)}, u32[]{:S(2)}, u32[]{:S(2)}) collective-permute-start(bf16[544,128]{1,0:T(8,128)(2,1)S(1)} %get-tuple-element.45.refs_5_), channel_id=1, source_target_pairs={{0,2},{1,3},{2,0},{3,1},{4,6},{5,7},{6,4},{7,5},{8,10},{9,11},{10,... | collective-permute-start | bytes 417800 | tf_op jit(solution)/shard_map/ppermute | solution.py:39
  49.5 2.0 %collective-permute-done.24.refs_7_ = bf16[544,128]{1,0:T(8,128)(2,1)S(1)} collective-permute-done((bf16[544,128]{1,0:T(8,128)(2,1)S(1)}, bf16[544,128]{1,0:T(8,128)(2,1)S(1)}, u32[]{:S(2)}, u32[]{:S(2)}) %collective-permute-start.24) | collective-permute-done | bytes 139296 | tf_op jit(solution)/shard_map/ppermute | solution.py:39
  51.5 2.9 %collective-permute-start.11 = (bf16[544,128]{1,0:T(8,128)(2,1)S(1)}, bf16[544,128]{1,0:T(8,128)(2,1)S(1)}, u32[]{:S(2)}, u32[]{:S(2)}) collective-permute-start(bf16[544,128]{1,0:T(8,128)(2,1)S(1)} %get-tuple-element.45.refs_5_), channel_id=1, source_target_pairs={{0,8},{4,12},{8,0},{12,4},{1,9},{5,13},{9,1},{13,5},{2,10},{6,14},... | collective-permute-start | bytes 417800 | tf_op jit(solution)/shard_map/ppermute | solution.py:39
  54.3 1.8 %collective-permute-start.15 = (bf16[544,128]{1,0:T(8,128)(2,1)S(1)}, bf16[544,128]{1,0:T(8,128)(2,1)S(1)}, u32[]{:S(2)}, u32[]{:S(2)}) collective-permute-start(bf16[544,128]{1,0:T(8,128)(2,1)S(1)} %get-tuple-element.45.refs_5_), channel_id=1, source_target_pairs={{0,12},{4,8},{8,4},{12,0},{1,13},{5,9},{9,5},{13,1},{2,14},{6,10},... | collective-permute-start | bytes 417800 | tf_op jit(solution)/shard_map/ppermute | solution.py:39
  56.7 8.2 %collective-permute-done.11.refs_5_ = bf16[544,128]{1,0:T(8,128)(2,1)S(1)} collective-permute-done((bf16[544,128]{1,0:T(8,128)(2,1)S(1)}, bf16[544,128]{1,0:T(8,128)(2,1)S(1)}, u32[]{:S(2)}, u32[]{:S(2)}) %collective-permute-start.11) | collective-permute-done | bytes 139296 | tf_op jit(solution)/shard_map/ppermute | solution.py:39
  64.9 1.7 %collective-permute-start.21 = (bf16[544,128]{1,0:T(8,128)(2,1)S(1)}, bf16[544,128]{1,0:T(8,128)(2,1)S(1)}, u32[]{:S(2)}, u32[]{:S(2)}) collective-permute-start(bf16[544,128]{1,0:T(8,128)(2,1)S(1)} %collective-permute-done.19.refs_5_), channel_id=1, source_target_pairs={{0,2},{1,3},{2,0},{3,1},{4,6},{5,7},{6,4},{7,5},{8,10},{9,11},{10,... | collective-permute-start | bytes 417800 | tf_op jit(solution)/shard_map/ppermute | solution.py:39
  67.0 1.7 %collective-permute-start.17 = (bf16[544,128]{1,0:T(8,128)(2,1)S(1)}, bf16[544,128]{1,0:T(8,128)(2,1)S(1)}, u32[]{:S(2)}, u32[]{:S(2)}) collective-permute-start(bf16[544,128]{1,0:T(8,128)(2,1)S(1)} %collective-permute-done.15.refs_9_), channel_id=1, source_target_pairs={{0,2},{1,3},{2,0},{3,1},{4,6},{5,7},{6,4},{7,5},{8,10},{9,11},{10,... | collective-permute-start | bytes 417800 | tf_op jit(solution)/shard_map/ppermute | solution.py:39
  68.7 2.0 %collective-permute-done.21.refs_7_ = bf16[544,128]{1,0:T(8,128)(2,1)S(1)} collective-permute-done((bf16[544,128]{1,0:T(8,128)(2,1)S(1)}, bf16[544,128]{1,0:T(8,128)(2,1)S(1)}, u32[]{:S(2)}, u32[]{:S(2)}) %collective-permute-start.21) | collective-permute-done | bytes 139296 | tf_op jit(solution)/shard_map/ppermute | solution.py:39
  71.2 2.3 %collective-permute-done.13.refs_7_ = bf16[544,128]{1,0:T(8,128)(2,1)S(1)} collective-permute-done((bf16[544,128]{1,0:T(8,128)(2,1)S(1)}, bf16[544,128]{1,0:T(8,128)(2,1)S(1)}, u32[]{:S(2)}, u32[]{:S(2)}) %collective-permute-start.13) | collective-permute-done | bytes 139296 | tf_op jit(solution)/shard_map/ppermute | solution.py:39
  73.5 2.4 %collective-permute-done.17.refs_11_ = bf16[544,128]{1,0:T(8,128)(2,1)S(1)} collective-permute-done((bf16[544,128]{1,0:T(8,128)(2,1)S(1)}, bf16[544,128]{1,0:T(8,128)(2,1)S(1)}, u32[]{:S(2)}, u32[]{:S(2)}) %collective-permute-start.17) | collective-permute-done | bytes 139296 | tf_op jit(solution)/shard_map/ppermute | solution.py:39
  77.6 2.1 %shard_map.159.refs_1_ = bf16[4,256,768]{2,1,0:T(8,128)(2,1)S(1)} custom-call(s32[5]{0:T(128)S(1)} %compare_select_fusion.info, bf16[384,256]{1,0:T(8,128)(2,1)S(1)} %get-tuple-element.40.refs_0_, bf16[384,256]{1,0:T(8,128)(2,1)S(1)} %collective-permute-done.8.refs_1_, bf16[384,256]{1,0:T(8,128)(2,1)S(1)} %collective-permute-done.9.refs_2_, ...), custom_call_target="tpu_custom_call" | custom-call | tf_op jit(solution)/shard_map/pallas_call | solution.py:452
  79.8 3.9 %shard_map.160 = (f32[4,8,768]{2,1,0:T(8,128)S(1)}, f32[4,8,768]{2,1,0:T(8,128)S(1)}, f32[4,128,384]{2,1,0:T(8,128)S(1)}) custom-call(s32[5]{0:T(128)S(1)} %compare_select_fusion.info, f32[8]{0:T(128)S(1)} %copy-done.11, bf16[4,256,768]{2,1,0:T(8,128)(2,1)S(1)} %shard_map.159.refs_1_, f32[1,512]{1,0:T(1,128)S(1)} %bitcast.13, ...), custom_call_target="tpu_custom_call" | custom-call | tf_op jit(solution)/shard_map/pallas_call | solution.py:452
  83.7 4.0 %shard_map.161 = (f32[4,8,768]{2,1,0:T(8,128)S(1)}, f32[4,8,768]{2,1,0:T(8,128)S(1)}, f32[4,128,384]{2,1,0:T(8,128)S(1)}) custom-call(s32[5]{0:T(128)S(1)} %compare_select_fusion.info, f32[8]{0:T(128)S(1)} %copy-done.11, bf16[4,256,768]{2,1,0:T(8,128)(2,1)S(1)} %shard_map.159.refs_1_, f32[1,512]{1,0:T(1,128)S(1)} %bitcast.14, ...), custom_call_target="tpu_custom_call" | custom-call | tf_op jit(solution)/shard_map/pallas_call | solution.py:452
  87.8 4.3 %shard_map.163.refs_4_ = bf16[384,256]{1,0:T(8,128)(2,1)S(1)} custom-call(s32[5]{0:T(128)S(1)} %compare_select_fusion.info, f32[8]{0:T(128)S(1)} %copy-done.11, bf16[4,256,768]{2,1,0:T(8,128)(2,1)S(1)} %shard_map.159.refs_1_, f32[1,512]{1,0:T(1,128)S(1)} %bitcast.15, bf16[512,512]{1,0:T(8,128)(2,1)S(1)} %get-tuple-element.43.refs_3_, ...), custom_call_target="tpu_custom_call" | custom-call | tf_op jit(solution)/shard_map/pallas_call | solution.py:452
  92.1 1.6 %collective-permute-start.30 = (bf16[384,256]{1,0:T(8,128)(2,1)S(1)}, bf16[384,256]{1,0:T(8,128)(2,1)S(1)}, u32[]{:S(2)}, u32[]{:S(2)}) collective-permute-start(bf16[384,256]{1,0:T(8,128)(2,1)S(1)} %shard_map.163.refs_4_), channel_id=1, source_target_pairs={{0,2},{1,3},{2,0},{3,1},{4,6},{5,7},{6,4},{7,5},{8,10},{9,11},{10,... | collective-permute-start | bytes 589832 | tf_op jit(solution)/shard_map/ppermute | solution.py:39
  93.7 4.5 %shard_map.162.refs_0_ = bf16[384,256]{1,0:T(8,128)(2,1)S(1)} custom-call(s32[5]{0:T(128)S(1)} %compare_select_fusion.info, f32[8]{0:T(128)S(1)} %copy-done.11, bf16[4,256,768]{2,1,0:T(8,128)(2,1)S(1)} %shard_map.159.refs_1_, f32[1,512]{1,0:T(1,128)S(1)} %bitcast.16, bf16[512,512]{1,0:T(8,128)(2,1)S(1)} %get-tuple-element.43.refs_3_, ...), custom_call_target="tpu_custom_call" | custom-call | tf_op jit(solution)/shard_map/pallas_call | solution.py:452
  99.3 5.6 %collective-permute-done.27.refs_2_ = bf16[384,256]{1,0:T(8,128)(2,1)S(1)} collective-permute-done((bf16[384,256]{1,0:T(8,128)(2,1)S(1)}, bf16[384,256]{1,0:T(8,128)(2,1)S(1)}, u32[]{:S(2)}, u32[]{:S(2)}) %collective-permute-start.27) | collective-permute-done | bytes 196640 | tf_op jit(solution)/shard_map/ppermute | solution.py:39
  106.3 2.4 %shard_map.164 = (bf16[96,1024]{1,0:T(8,128)(2,1)S(1)}, bf16[96,1024]{1,0:T(8,128)(2,1)S(1)}, bf16[96,1024]{1,0:T(8,128)(2,1)S(1)}, bf16[96,1024]{1,0:T(8,128)(2,1)S(1)}) custom-call(s32[5]{0:T(128)S(1)} %compare_select_fusion.info, bf16[384,256]{1,0:T(8,128)(2,1)S(1)} %shard_map.162.refs_0_, bf16[384,256]{1,0:T(8,128)(2,1)S(1)} %collective-permute-done.26.refs_1_, ...), custom_call_target="tpu_custom_call" | custom-call | tf_op jit(solution)/shard_map/pallas_call | solution.py:452
  110.6 6.0 %collective-permute-done.33.refs_2_ = bf16[96,1024]{1,0:T(8,128)(2,1)S(1)} collective-permute-done((bf16[96,1024]{1,0:T(8,128)(2,1)S(1)}, bf16[96,1024]{1,0:T(8,128)(2,1)S(1)}, u32[]{:S(2)}, u32[]{:S(2)}) %collective-permute-start.33) | collective-permute-done | bytes 196640 | tf_op jit(solution)/shard_map/ppermute | solution.py:39
  116.7 3.0 %collective-permute-done.34.refs_3_ = bf16[96,1024]{1,0:T(8,128)(2,1)S(1)} collective-permute-done((bf16[96,1024]{1,0:T(8,128)(2,1)S(1)}, bf16[96,1024]{1,0:T(8,128)(2,1)S(1)}, u32[]{:S(2)}, u32[]{:S(2)}) %collective-permute-start.34) | collective-permute-done | bytes 196640 | tf_op jit(solution)/shard_map/ppermute | solution.py:39
  119.7 1.7 %shard_map.165 = bf16[96,4096]{1,0:T(8,128)(2,1)} custom-call(s32[5]{0:T(128)S(1)} %compare_select_fusion.info, bf16[96,1024]{1,0:T(8,128)(2,1)S(1)} %get-tuple-element.53.refs_0_, bf16[96,1024]{1,0:T(8,128)(2,1)S(1)} %collective-permute-done.32.refs_1_, bf16[96,1024]{1,0:T(8,128)(2,1)S(1)} %collective-permute-done.33.refs_2_, ...), custom_call_target="tpu_custom_call" | custom-call | tf_op jit(solution)/shard_map/pallas_call | solution.py:452
  (86 shorter events, 14.0 us)
Async XLA Ops:
  0.0 20.7 %collective-permute-start.1 = (bf16[96,4096]{1,0:T(8,128)(2,1)}, bf16[96,4096]{1,0:T(8,128)(2,1)S(1)}, u32[]{:S(2)}, u32[]{:S(2)}) collective-permute-start(bf16[96,4096]{1,0:T(8,128)(2,1)} %refs_8_.1), channel_id=1, source_target_pairs={{0,2},{1,3},{2,0},{3,1},{4,6},{5,7},{6,4},{7,5},{8,10},{9,11},{10,... | collective-permute-start | bytes 2359304 | tf_op jit(solution)/shard_map/ppermute | solution.py:39
  3.0 35.4 %collective-permute-start = (bf16[96,4096]{1,0:T(8,128)(2,1)}, bf16[96,4096]{1,0:T(8,128)(2,1)}, u32[]{:S(2)}, u32[]{:S(2)}) collective-permute-start(bf16[96,4096]{1,0:T(8,128)(2,1)} %refs_8_.1), channel_id=1, source_target_pairs={{0,1},{1,0},{2,3},{3,2},{4,5},{5,4},{6,7},{7,6},{8,9},{9,8},{10,11... | collective-permute-start | bytes 2359304 | tf_op jit(solution)/shard_map/ppermute | solution.py:39
  20.7 20.4 %collective-permute-start.2 = (bf16[96,4096]{1,0:T(8,128)(2,1)S(1)}, bf16[96,4096]{1,0:T(8,128)(2,1)S(1)}, u32[]{:S(2)}, u32[]{:S(2)}) collective-permute-start(bf16[96,4096]{1,0:T(8,128)(2,1)S(1)} %collective-permute-done.1.refs_2_), channel_id=1, source_target_pairs={{0,1},{1,0},{2,3},{3,2},{4,5},{5,4},{6,7},{7,6},{8,9},{9,8},{10,11... | collective-permute-start | bytes 2359304 | tf_op jit(solution)/shard_map/ppermute | solution.py:39
  23.1 4.0 %collective-permute-start.3 = (f32[5,1024]{1,0:T(8,128)S(1)}, f32[5,1024]{1,0:T(8,128)S(1)}, u32[]{:S(2)}, u32[]{:S(2)}) collective-permute-start(f32[5,1024]{1,0:T(8,128)S(1)} %pad_maximum_fusion), channel_id=1, source_target_pairs={{0,4},{4,0},{8,12},{12,8},{1,5},{5,1},{9,13},{13,9},{2,6},{6,2},{1... | collective-permute-start | bytes 61448 | tf_op jit(solution)/shard_map/ppermute | solution.py:39
  27.1 4.9 %collective-permute-start.4 = (f32[5,1024]{1,0:T(8,128)S(1)}, f32[5,1024]{1,0:T(8,128)S(1)}, u32[]{:S(2)}, u32[]{:S(2)}) collective-permute-start(f32[5,1024]{1,0:T(8,128)S(1)} %fusion.2), channel_id=1, source_target_pairs={{0,8},{4,12},{8,0},{12,4},{1,9},{5,13},{9,1},{13,5},{2,10},{6,14},... | collective-permute-start | bytes 61448 | tf_op jit(solution)/shard_map/ppermute | solution.py:39
  33.7 7.3 %collective-permute-start.5 = (f32[5,1024]{1,0:T(8,128)S(1)}, f32[5,1024]{1,0:T(8,128)S(1)}, u32[]{:S(2)}, u32[]{:S(2)}) collective-permute-start(f32[5,1024]{1,0:T(8,128)S(1)} %add.18.refs_4_), channel_id=1, source_target_pairs={{0,1},{1,0},{2,3},{3,2},{4,5},{5,4},{6,7},{7,6},{8,9},{9,8},{10,11... | collective-permute-start | bytes 61448 | tf_op jit(solution)/shard_map/ppermute | solution.py:39
  35.9 5.1 %collective-permute-start.7 = (f32[5,1024]{1,0:T(8,128)S(1)}, f32[5,1024]{1,0:T(8,128)S(1)}, u32[]{:S(2)}, u32[]{:S(2)}) collective-permute-start(f32[5,1024]{1,0:T(8,128)S(1)} %collective-permute-done.6.refs_6_), channel_id=1, source_target_pairs={{0,1},{1,0},{2,3},{3,2},{4,5},{5,4},{6,7},{7,6},{8,9},{9,8},{10,11... | collective-permute-start | bytes 61448 | tf_op jit(solution)/shard_map/ppermute | solution.py:39
  45.4 6.1 %collective-permute-start.24 = (bf16[544,128]{1,0:T(8,128)(2,1)S(1)}, bf16[544,128]{1,0:T(8,128)(2,1)S(1)}, u32[]{:S(2)}, u32[]{:S(2)}) collective-permute-start(bf16[544,128]{1,0:T(8,128)(2,1)S(1)} %get-tuple-element.45.refs_5_), channel_id=1, source_target_pairs={{0,2},{1,3},{2,0},{3,1},{4,6},{5,7},{6,4},{7,5},{8,10},{9,11},{10,... | collective-permute-start | bytes 417800 | tf_op jit(solution)/shard_map/ppermute | solution.py:39
  47.1 7.2 %collective-permute-start.23 = (bf16[544,128]{1,0:T(8,128)(2,1)S(1)}, bf16[544,128]{1,0:T(8,128)(2,1)S(1)}, u32[]{:S(2)}, u32[]{:S(2)}) collective-permute-start(bf16[544,128]{1,0:T(8,128)(2,1)S(1)} %get-tuple-element.45.refs_5_), channel_id=1, source_target_pairs={{0,1},{1,0},{2,3},{3,2},{4,5},{5,4},{6,7},{7,6},{8,9},{9,8},{10,11... | collective-permute-start | bytes 417800 | tf_op jit(solution)/shard_map/ppermute | solution.py:39
  47.4 8.8 %collective-permute-start.19 = (bf16[544,128]{1,0:T(8,128)(2,1)S(1)}, bf16[544,128]{1,0:T(8,128)(2,1)S(1)}, u32[]{:S(2)}, u32[]{:S(2)}) collective-permute-start(bf16[544,128]{1,0:T(8,128)(2,1)S(1)} %get-tuple-element.45.refs_5_), channel_id=1, source_target_pairs={{0,4},{4,0},{8,12},{12,8},{1,5},{5,1},{9,13},{13,9},{2,6},{6,2},{1... | collective-permute-start | bytes 417800 | tf_op jit(solution)/shard_map/ppermute | solution.py:39
  48.9 7.2 %collective-permute-start.9 = (bf16[384,256]{1,0:T(8,128)(2,1)S(1)}, bf16[384,256]{1,0:T(8,128)(2,1)S(1)}, u32[]{:S(2)}, u32[]{:S(2)}) collective-permute-start(bf16[384,256]{1,0:T(8,128)(2,1)S(1)} %get-tuple-element.40.refs_0_), channel_id=1, source_target_pairs={{0,2},{1,3},{2,0},{3,1},{4,6},{5,7},{6,4},{7,5},{8,10},{9,11},{10,... | collective-permute-start | bytes 589832 | tf_op jit(solution)/shard_map/ppermute | solution.py:39
  49.5 17.1 %collective-permute-start.8 = (bf16[384,256]{1,0:T(8,128)(2,1)S(1)}, bf16[384,256]{1,0:T(8,128)(2,1)S(1)}, u32[]{:S(2)}, u32[]{:S(2)}) collective-permute-start(bf16[384,256]{1,0:T(8,128)(2,1)S(1)} %get-tuple-element.40.refs_0_), channel_id=1, source_target_pairs={{0,1},{1,0},{2,3},{3,2},{4,5},{5,4},{6,7},{7,6},{8,9},{9,8},{10,11... | collective-permute-start | bytes 589832 | tf_op jit(solution)/shard_map/ppermute | solution.py:39
  51.5 13.4 %collective-permute-start.11 = (bf16[544,128]{1,0:T(8,128)(2,1)S(1)}, bf16[544,128]{1,0:T(8,128)(2,1)S(1)}, u32[]{:S(2)}, u32[]{:S(2)}) collective-permute-start(bf16[544,128]{1,0:T(8,128)(2,1)S(1)} %get-tuple-element.45.refs_5_), channel_id=1, source_target_pairs={{0,8},{4,12},{8,0},{12,4},{1,9},{5,13},{9,1},{13,5},{2,10},{6,14},... | collective-permute-start | bytes 417800 | tf_op jit(solution)/shard_map/ppermute | solution.py:39
  54.3 12.2 %collective-permute-start.15 = (bf16[544,128]{1,0:T(8,128)(2,1)S(1)}, bf16[544,128]{1,0:T(8,128)(2,1)S(1)}, u32[]{:S(2)}, u32[]{:S(2)}) collective-permute-start(bf16[544,128]{1,0:T(8,128)(2,1)S(1)} %get-tuple-element.45.refs_5_), channel_id=1, source_target_pairs={{0,12},{4,8},{8,4},{12,0},{1,13},{5,9},{9,5},{13,1},{2,14},{6,10},... | collective-permute-start | bytes 417800 | tf_op jit(solution)/shard_map/ppermute | solution.py:39
  56.1 10.9 %collective-permute-start.25 = (bf16[544,128]{1,0:T(8,128)(2,1)S(1)}, bf16[544,128]{1,0:T(8,128)(2,1)S(1)}, u32[]{:S(2)}, u32[]{:S(2)}) collective-permute-start(bf16[544,128]{1,0:T(8,128)(2,1)S(1)} %collective-permute-done.24.refs_7_), channel_id=1, source_target_pairs={{0,1},{1,0},{2,3},{3,2},{4,5},{5,4},{6,7},{7,6},{8,9},{9,8},{10,11... | collective-permute-start | bytes 417800 | tf_op jit(solution)/shard_map/ppermute | solution.py:39
  56.1 19.8 %collective-permute-start.10 = (bf16[384,256]{1,0:T(8,128)(2,1)S(1)}, bf16[384,256]{1,0:T(8,128)(2,1)S(1)}, u32[]{:S(2)}, u32[]{:S(2)}) collective-permute-start(bf16[384,256]{1,0:T(8,128)(2,1)S(1)} %collective-permute-done.9.refs_2_), channel_id=1, source_target_pairs={{0,1},{1,0},{2,3},{3,2},{4,5},{5,4},{6,7},{7,6},{8,9},{9,8},{10,11... | collective-permute-start | bytes 589832 | tf_op jit(solution)/shard_map/ppermute | solution.py:39
  64.9 5.8 %collective-permute-start.21 = (bf16[544,128]{1,0:T(8,128)(2,1)S(1)}, bf16[544,128]{1,0:T(8,128)(2,1)S(1)}, u32[]{:S(2)}, u32[]{:S(2)}) collective-permute-start(bf16[544,128]{1,0:T(8,128)(2,1)S(1)} %collective-permute-done.19.refs_5_), channel_id=1, source_target_pairs={{0,2},{1,3},{2,0},{3,1},{4,6},{5,7},{6,4},{7,5},{8,10},{9,11},{10,... | collective-permute-start | bytes 417800 | tf_op jit(solution)/shard_map/ppermute | solution.py:39
  66.6 4.1 %collective-permute-start.20 = (bf16[544,128]{1,0:T(8,128)(2,1)S(1)}, bf16[544,128]{1,0:T(8,128)(2,1)S(1)}, u32[]{:S(2)}, u32[]{:S(2)}) collective-permute-start(bf16[544,128]{1,0:T(8,128)(2,1)S(1)} %collective-permute-done.19.refs_5_), channel_id=1, source_target_pairs={{0,1},{1,0},{2,3},{3,2},{4,5},{5,4},{6,7},{7,6},{8,9},{9,8},{10,11... | collective-permute-start | bytes 417800 | tf_op jit(solution)/shard_map/ppermute | solution.py:39
  66.6 6.9 %collective-permute-start.13 = (bf16[544,128]{1,0:T(8,128)(2,1)S(1)}, bf16[544,128]{1,0:T(8,128)(2,1)S(1)}, u32[]{:S(2)}, u32[]{:S(2)}) collective-permute-start(bf16[544,128]{1,0:T(8,128)(2,1)S(1)} %collective-permute-done.11.refs_5_), channel_id=1, source_target_pairs={{0,2},{1,3},{2,0},{3,1},{4,6},{5,7},{6,4},{7,5},{8,10},{9,11},{10,... | collective-permute-start | bytes 417800 | tf_op jit(solution)/shard_map/ppermute | solution.py:39
  67.0 8.9 %collective-permute-start.17 = (bf16[544,128]{1,0:T(8,128)(2,1)S(1)}, bf16[544,128]{1,0:T(8,128)(2,1)S(1)}, u32[]{:S(2)}, u32[]{:S(2)}) collective-permute-start(bf16[544,128]{1,0:T(8,128)(2,1)S(1)} %collective-permute-done.15.refs_9_), channel_id=1, source_target_pairs={{0,2},{1,3},{2,0},{3,1},{4,6},{5,7},{6,4},{7,5},{8,10},{9,11},{10,... | collective-permute-start | bytes 417800 | tf_op jit(solution)/shard_map/ppermute | solution.py:39
  70.7 13.1 %collective-permute-start.22 = (bf16[544,128]{1,0:T(8,128)(2,1)S(1)}, bf16[544,128]{1,0:T(8,128)(2,1)S(1)}, u32[]{:S(2)}, u32[]{:S(2)}) collective-permute-start(bf16[544,128]{1,0:T(8,128)(2,1)S(1)} %collective-permute-done.21.refs_7_), channel_id=1, source_target_pairs={{0,1},{1,0},{2,3},{3,2},{4,5},{5,4},{6,7},{7,6},{8,9},{9,8},{10,11... | collective-permute-start | bytes 417800 | tf_op jit(solution)/shard_map/ppermute | solution.py:39
  70.7 17.1 %collective-permute-start.12 = (bf16[544,128]{1,0:T(8,128)(2,1)S(1)}, bf16[544,128]{1,0:T(8,128)(2,1)S(1)}, u32[]{:S(2)}, u32[]{:S(2)}) collective-permute-start(bf16[544,128]{1,0:T(8,128)(2,1)S(1)} %collective-permute-done.11.refs_5_), channel_id=1, source_target_pairs={{0,1},{1,0},{2,3},{3,2},{4,5},{5,4},{6,7},{7,6},{8,9},{9,8},{10,11... | collective-permute-start | bytes 417800 | tf_op jit(solution)/shard_map/ppermute | solution.py:39
  73.5 14.3 %collective-permute-start.16 = (bf16[544,128]{1,0:T(8,128)(2,1)S(1)}, bf16[544,128]{1,0:T(8,128)(2,1)S(1)}, u32[]{:S(2)}, u32[]{:S(2)}) collective-permute-start(bf16[544,128]{1,0:T(8,128)(2,1)S(1)} %collective-permute-done.15.refs_9_), channel_id=1, source_target_pairs={{0,1},{1,0},{2,3},{3,2},{4,5},{5,4},{6,7},{7,6},{8,9},{9,8},{10,11... | collective-permute-start | bytes 417800 | tf_op jit(solution)/shard_map/ppermute | solution.py:39
  75.9 11.9 %collective-permute-start.14 = (bf16[544,128]{1,0:T(8,128)(2,1)S(1)}, bf16[544,128]{1,0:T(8,128)(2,1)S(1)}, u32[]{:S(2)}, u32[]{:S(2)}) collective-permute-start(bf16[544,128]{1,0:T(8,128)(2,1)S(1)} %collective-permute-done.13.refs_7_), channel_id=1, source_target_pairs={{0,1},{1,0},{2,3},{3,2},{4,5},{5,4},{6,7},{7,6},{8,9},{9,8},{10,11... | collective-permute-start | bytes 417800 | tf_op jit(solution)/shard_map/ppermute | solution.py:39
  75.9 11.9 %collective-permute-start.18 = (bf16[544,128]{1,0:T(8,128)(2,1)S(1)}, bf16[544,128]{1,0:T(8,128)(2,1)S(1)}, u32[]{:S(2)}, u32[]{:S(2)}) collective-permute-start(bf16[544,128]{1,0:T(8,128)(2,1)S(1)} %collective-permute-done.17.refs_11_), channel_id=1, source_target_pairs={{0,1},{1,0},{2,3},{3,2},{4,5},{5,4},{6,7},{7,6},{8,9},{9,8},{10,11... | collective-permute-start | bytes 417800 | tf_op jit(solution)/shard_map/ppermute | solution.py:39
  92.1 7.2 %collective-permute-start.30 = (bf16[384,256]{1,0:T(8,128)(2,1)S(1)}, bf16[384,256]{1,0:T(8,128)(2,1)S(1)}, u32[]{:S(2)}, u32[]{:S(2)}) collective-permute-start(bf16[384,256]{1,0:T(8,128)(2,1)S(1)} %shard_map.163.refs_4_), channel_id=1, source_target_pairs={{0,2},{1,3},{2,0},{3,1},{4,6},{5,7},{6,4},{7,5},{8,10},{9,11},{10,... | collective-permute-start | bytes 589832 | tf_op jit(solution)/shard_map/ppermute | solution.py:39
  98.2 6.6 %collective-permute-start.27 = (bf16[384,256]{1,0:T(8,128)(2,1)S(1)}, bf16[384,256]{1,0:T(8,128)(2,1)S(1)}, u32[]{:S(2)}, u32[]{:S(2)}) collective-permute-start(bf16[384,256]{1,0:T(8,128)(2,1)S(1)} %shard_map.162.refs_0_), channel_id=1, source_target_pairs={{0,2},{1,3},{2,0},{3,1},{4,6},{5,7},{6,4},{7,5},{8,10},{9,11},{10,... | collective-permute-start | bytes 589832 | tf_op jit(solution)/shard_map/ppermute | solution.py:39
  98.7 6.1 %collective-permute-start.29 = (bf16[384,256]{1,0:T(8,128)(2,1)S(1)}, bf16[384,256]{1,0:T(8,128)(2,1)S(1)}, u32[]{:S(2)}, u32[]{:S(2)}) collective-permute-start(bf16[384,256]{1,0:T(8,128)(2,1)S(1)} %shard_map.163.refs_4_), channel_id=1, source_target_pairs={{0,1},{1,0},{2,3},{3,2},{4,5},{5,4},{6,7},{7,6},{8,9},{9,8},{10,11... | collective-permute-start | bytes 589832 | tf_op jit(solution)/shard_map/ppermute | solution.py:39
  98.8 6.1 %collective-permute-start.26 = (bf16[384,256]{1,0:T(8,128)(2,1)S(1)}, bf16[384,256]{1,0:T(8,128)(2,1)S(1)}, u32[]{:S(2)}, u32[]{:S(2)}) collective-permute-start(bf16[384,256]{1,0:T(8,128)(2,1)S(1)} %shard_map.162.refs_0_), channel_id=1, source_target_pairs={{0,1},{1,0},{2,3},{3,2},{4,5},{5,4},{6,7},{7,6},{8,9},{9,8},{10,11... | collective-permute-start | bytes 589832 | tf_op jit(solution)/shard_map/ppermute | solution.py:39
  99.3 5.6 %collective-permute-start.31 = (bf16[384,256]{1,0:T(8,128)(2,1)S(1)}, bf16[384,256]{1,0:T(8,128)(2,1)S(1)}, u32[]{:S(2)}, u32[]{:S(2)}) collective-permute-start(bf16[384,256]{1,0:T(8,128)(2,1)S(1)} %collective-permute-done.30.refs_6_), channel_id=1, source_target_pairs={{0,1},{1,0},{2,3},{3,2},{4,5},{5,4},{6,7},{7,6},{8,9},{9,8},{10,11... | collective-permute-start | bytes 589832 | tf_op jit(solution)/shard_map/ppermute | solution.py:39
  108.9 7.8 %collective-permute-start.33 = (bf16[96,1024]{1,0:T(8,128)(2,1)S(1)}, bf16[96,1024]{1,0:T(8,128)(2,1)S(1)}, u32[]{:S(2)}, u32[]{:S(2)}) collective-permute-start(bf16[96,1024]{1,0:T(8,128)(2,1)S(1)} %get-tuple-element.55), channel_id=1, source_target_pairs={{0,2},{1,3},{2,0},{3,1},{4,6},{5,7},{6,4},{7,5},{8,10},{9,11},{10,... | collective-permute-start | bytes 589832 | tf_op jit(solution)/shard_map/ppermute | solution.py:39
  109.4 10.3 %collective-permute-start.34 = (bf16[96,1024]{1,0:T(8,128)(2,1)S(1)}, bf16[96,1024]{1,0:T(8,128)(2,1)S(1)}, u32[]{:S(2)}, u32[]{:S(2)}) collective-permute-start(bf16[96,1024]{1,0:T(8,128)(2,1)S(1)} %get-tuple-element.56), channel_id=1, source_target_pairs={{0,3},{1,2},{2,1},{3,0},{4,7},{5,6},{6,5},{7,4},{8,11},{9,10},{10,... | collective-permute-start | bytes 589832 | tf_op jit(solution)/shard_map/ppermute | solution.py:39
  (17 other events, 333.6 us)

commit v4 on v3

--- a/solution.py
+++ b/solution.py
@@ -403,28 +403,32 @@
             state_out[2][pair] = acc
 
 
-def out_kernel(count, splits, parts, info, *refs):
+def out_kernel(count, splits, parts, wanted, info, *refs):
     ids = member_ids(info, count)
     pieces = refs[: count * splits]
     w_ref = refs[count * splits]
-    refs = refs[1 + count * splits :]
-    outs = refs[:parts]
+    outs = refs[1 + count * splits :]
     depth = pieces[0].shape[1]
-    total = None
-    for number, piece in enumerate(pieces):
-        split, member = divmod(number, count)
-        start = aligned((ids[member] * splits + split) * depth, LANES)
-        part = f32_dot(piece[...], w_ref[pl.ds(start, depth), :])
-        total = part if total is None else total + part
-    if parts == 1:
-        outs[0][...] = total.astype(jnp.bfloat16)
-        return
-    scratch = refs[parts]
-    scratch[...] = total
     rows = outs[0].shape[0]
-    for number, out_ref in enumerate(outs):
-        start = aligned(ids[number] * rows, 8)
-        out_ref[...] = scratch[pl.ds(start, rows), :].astype(jnp.bfloat16)
+    for place_of in range(0, len(wanted), 2):
+        group = wanted[place_of : place_of + 2]
+        total = None
+        for number, piece in enumerate(pieces):
+            split, member = divmod(number, count)
+            start = aligned((ids[member] * splits + split) * depth, LANES)
+            if parts == 1:
+                left = piece[...]
+            else:
+                left = jnp.concatenate(
+                    [piece[pl.ds(aligned(ids[owner] * rows, 16), rows), :] for owner in group],
+                    axis=0,
+                )
+            part = f32_dot(left, w_ref[pl.ds(start, depth), :])
+            total = part if total is None else total + part
+        for number in range(len(group)):
+            outs[place_of + number][...] = total[number * rows : (number + 1) * rows].astype(
+                jnp.bfloat16
+            )
 
 
 def final_kernel(count, mod_count, info, *refs):
@@ -668,18 +672,24 @@
         done = attend(part, first, True, chosen, state)
         att_pieces.append(spread(done))
     out_cols = w_out.shape[1]
-    parts = tp_count if small and own_rows % 8 == 0 else 1
-    proj = call(
-        functools.partial(out_kernel, tp_count, len(att_pieces), parts),
-        [shape_of((tok_count // parts, out_cols), bf16) for _ in range(parts)],
-        [info, *[piece for group in att_pieces for piece in group], w_o],
-        smem=(0,),
-        scratch=[VMEM((tok_count, out_cols), jnp.float32)] if parts > 1 else [],
-    )
+    parts = tp_count if small and own_rows % 16 == 0 else 1
+    if parts > 2:
+        turns = [list(range(2, parts)), [0, 1]]
+    else:
+        turns = [list(range(parts))]
+    proj = {}
+    for wanted in turns:
+        emitted = call(
+            functools.partial(out_kernel, tp_count, len(att_pieces), parts, wanted),
+            [shape_of((tok_count // parts, out_cols), bf16) for _ in wanted],
+            [info, *[piece for group in att_pieces for piece in group], w_o],
+            smem=(0,),
+        )
+        proj.update(zip(wanted, emitted))
     if parts > 1:
         proj_pieces = [
             swap(value, "tp", member) if member else value
-            for member, value in enumerate(proj)
+            for member, value in sorted(proj.items())
         ]
     else:
         by_owner = proj[0].reshape(tp_count, own_rows, out_cols)

time: 122 us -> 120 us (0.984)
  waiting for transfers between devices: 55.8 us -> 53.3 us
    ppermute x35, waiting for transfers between devices: 55.8 us -> 53.3 us  [swap(): return lax.ppermute(value, axis, [(i, i ^ bit) for i in range(count)])]
    pallas_call x12 -> x13, Pallas kernels: 33.4 us -> 34.1 us  [call(): pl.pallas_call(kernel, out_shape=outs, in_specs=specs, out_specs=[in_vmem...]
  transfers between devices with their start and end apart: 35 -> 35, of which waited for: 13 -> 13; matrix products, arithmetic and copies ran while one was open for 3% -> 3% of each run, Pallas kernels for 17% -> 19%
where the time goes in v4:
time: 120 us
  waiting for transfers between devices  53.3 us (44%)
  Pallas kernels  34.1 us (28%)
  starting transfers between devices  28.5 us (24%)
  matrix products  2.74 us (2%)
    ppermute x35, waiting for transfers between devices, swap(): return lax.ppermute(value, axis, [(i, i ^ bit) for i in range(count)])  53.3 us
    pallas_call x13, Pallas kernels, call(): pl.pallas_call(kernel, out_shape=outs, in_specs=specs, out_specs=[in_vmem...  34.1 us
    ppermute x35, starting transfers between devices, swap(): return lax.ppermute(value, axis, [(i, i ^ bit) for i in range(count)])  28.5 us
    dot_general x3, matrix products, f32_dot(): return jnp.dot(a, b, preferred_element_type=jnp.float32)  2.74 us
  transfers between devices with their start and end apart: 35, of which 13 were waited for; matrix products, arithmetic and copies ran while one was open for 3% of the time, Pallas kernels for 19%

profile of v4, /device:TPU:0, one launch (start us, length us, event | category | flops | bytes accessed | tf_op | source)
XLA Modules:
  0.0 119.9 jit_solution(4803802911122848111)
XLA Ops:
  0.0 3.0 %collective-permute-start.1 = (bf16[96,4096]{1,0:T(8,128)(2,1)}, bf16[96,4096]{1,0:T(8,128)(2,1)S(1)}, u32[]{:S(2)}, u32[]{:S(2)}) collective-permute-start(bf16[96,4096]{1,0:T(8,128)(2,1)} %refs_8_.1), channel_id=1, source_target_pairs={{0,2},{1,3},{2,0},{3,1},{4,6},{5,7},{6,4},{7,5},{8,10},{9,11},{10,... | collective-permute-start | bytes 2359304 | tf_op jit(solution)/shard_map/ppermute | solution.py:39
  4.3 16.5 %collective-permute-done.1.refs_2_ = bf16[96,4096]{1,0:T(8,128)(2,1)S(1)} collective-permute-done((bf16[96,4096]{1,0:T(8,128)(2,1)}, bf16[96,4096]{1,0:T(8,128)(2,1)S(1)}, u32[]{:S(2)}, u32[]{:S(2)}) %collective-permute-start.1) | collective-permute-done | bytes 786464 | tf_op jit(solution)/shard_map/ppermute | solution.py:39
  21.1 2.0 %fusion.4 = f32[2,1024]{1,0:T(2,128)S(1)} fusion(bf16[2,1024]{1,0:T(2,128)(2,1)S(1)} %fusion, bf16[1024,1024]{1,0:T(8,128)(2,1)} %param.20), kind=kOutput, calls=%fused_computation.8 | convolution fusion | flops 4194304 | bytes 2109440 | tf_op jit(solution)/shard_map/dot_general | solution.py:34
  23.1 1.9 %collective-permute-start.3 = (f32[5,1024]{1,0:T(8,128)S(1)}, f32[5,1024]{1,0:T(8,128)S(1)}, u32[]{:S(2)}, u32[]{:S(2)}) collective-permute-start(f32[5,1024]{1,0:T(8,128)S(1)} %pad_maximum_fusion), channel_id=1, source_target_pairs={{0,4},{4,0},{8,12},{12,8},{1,5},{5,1},{9,13},{13,9},{2,6},{6,2},{1... | collective-permute-start | bytes 61448 | tf_op jit(solution)/shard_map/ppermute | solution.py:39
  25.0 2.1 %collective-permute-done.3 = f32[5,1024]{1,0:T(8,128)S(1)} collective-permute-done((f32[5,1024]{1,0:T(8,128)S(1)}, f32[5,1024]{1,0:T(8,128)S(1)}, u32[]{:S(2)}, u32[]{:S(2)}) %collective-permute-start.3) | collective-permute-done | bytes 20512 | tf_op jit(solution)/shard_map/ppermute | solution.py:39
  27.1 2.9 %collective-permute-start.4 = (f32[5,1024]{1,0:T(8,128)S(1)}, f32[5,1024]{1,0:T(8,128)S(1)}, u32[]{:S(2)}, u32[]{:S(2)}) collective-permute-start(f32[5,1024]{1,0:T(8,128)S(1)} %fusion.2), channel_id=1, source_target_pairs={{0,8},{4,12},{8,0},{12,4},{1,9},{5,13},{9,1},{13,5},{2,10},{6,14},... | collective-permute-start | bytes 61448 | tf_op jit(solution)/shard_map/ppermute | solution.py:39
  30.0 2.0 %collective-permute-done.4 = f32[5,1024]{1,0:T(8,128)S(1)} collective-permute-done((f32[5,1024]{1,0:T(8,128)S(1)}, f32[5,1024]{1,0:T(8,128)S(1)}, u32[]{:S(2)}, u32[]{:S(2)}) %collective-permute-start.4) | collective-permute-done | bytes 20512 | tf_op jit(solution)/shard_map/ppermute | solution.py:39
  32.0 1.7 %collective-permute-start.6 = (f32[5,1024]{1,0:T(8,128)S(1)}, f32[5,1024]{1,0:T(8,128)S(1)}, u32[]{:S(2)}, u32[]{:S(2)}) collective-permute-start(f32[5,1024]{1,0:T(8,128)S(1)} %add.18.refs_4_), channel_id=1, source_target_pairs={{0,2},{1,3},{2,0},{3,1},{4,6},{5,7},{6,4},{7,5},{8,10},{9,11},{10,... | collective-permute-start | bytes 61448 | tf_op jit(solution)/shard_map/ppermute | solution.py:39
  33.7 2.2 %collective-permute-done.6.refs_6_ = f32[5,1024]{1,0:T(8,128)S(1)} collective-permute-done((f32[5,1024]{1,0:T(8,128)S(1)}, f32[5,1024]{1,0:T(8,128)S(1)}, u32[]{:S(2)}, u32[]{:S(2)}) %collective-permute-start.6) | collective-permute-done | bytes 20512 | tf_op jit(solution)/shard_map/ppermute | solution.py:39
  35.9 1.6 %shard_map.156 = (f32[512,128]{1,0:T(8,128)S(1)}, f32[512,128]{1,0:T(8,128)S(1)}, f32[32,384]{1,0:T(8,128)S(1)}) custom-call(s32[5]{0:T(128)S(1)} %compare_select_fusion.info), custom_call_target="tpu_custom_call" | custom-call | tf_op jit(solution)/shard_map/pallas_call | solution.py:456
  38.4 2.7 %shard_map.154 = (f32[96,4096]{1,0:T(8,128)S(1)}, f32[96,4096]{1,0:T(8,128)S(1)}, f32[128,4096]{1,0:T(8,128)S(1)}) custom-call(bf16[96,4096]{1,0:T(8,128)(2,1)S(1)} %copy-done.2, bf16[96,4096]{1,0:T(8,128)(2,1)} %collective-permute-done.refs_1_, bf16[128,4096]{1,0:T(8,128)(2,1)S(1)} %copy-done.6), custom_call_target="tpu_custom_call" | custom-call | tf_op jit(solution)/shard_map/pallas_call | solution.py:456
  41.1 4.3 %shard_map.157 = (bf16[384,256]{1,0:T(8,128)(2,1)S(1)}, bf16[544,128]{1,0:T(8,128)(2,1)S(1)}, bf16[16,128]{1,0:T(8,128)(2,1)}) custom-call(s32[5]{0:T(128)S(1)} %compare_select_fusion.info, f32[96,4096]{1,0:T(8,128)S(1)} %get-tuple-element.32.refs_0_, f32[96,4096]{1,0:T(8,128)S(1)} %get-tuple-element.33.refs_1_, ...), custom_call_target="tpu_custom_call" | custom-call | tf_op jit(solution)/shard_map/pallas_call | solution.py:456
  45.4 1.7 %collective-permute-start.24 = (bf16[544,128]{1,0:T(8,128)(2,1)S(1)}, bf16[544,128]{1,0:T(8,128)(2,1)S(1)}, u32[]{:S(2)}, u32[]{:S(2)}) collective-permute-start(bf16[544,128]{1,0:T(8,128)(2,1)S(1)} %get-tuple-element.45.refs_5_), channel_id=1, source_target_pairs={{0,2},{1,3},{2,0},{3,1},{4,6},{5,7},{6,4},{7,5},{8,10},{9,11},{10,... | collective-permute-start | bytes 417800 | tf_op jit(solution)/shard_map/ppermute | solution.py:39
  49.5 2.0 %collective-permute-done.24.refs_7_ = bf16[544,128]{1,0:T(8,128)(2,1)S(1)} collective-permute-done((bf16[544,128]{1,0:T(8,128)(2,1)S(1)}, bf16[544,128]{1,0:T(8,128)(2,1)S(1)}, u32[]{:S(2)}, u32[]{:S(2)}) %collective-permute-start.24) | collective-permute-done | bytes 139296 | tf_op jit(solution)/shard_map/ppermute | solution.py:39
  51.5 2.9 %collective-permute-start.11 = (bf16[544,128]{1,0:T(8,128)(2,1)S(1)}, bf16[544,128]{1,0:T(8,128)(2,1)S(1)}, u32[]{:S(2)}, u32[]{:S(2)}) collective-permute-start(bf16[544,128]{1,0:T(8,128)(2,1)S(1)} %get-tuple-element.45.refs_5_), channel_id=1, source_target_pairs={{0,8},{4,12},{8,0},{12,4},{1,9},{5,13},{9,1},{13,5},{2,10},{6,14},... | collective-permute-start | bytes 417800 | tf_op jit(solution)/shard_map/ppermute | solution.py:39
  54.3 1.8 %collective-permute-start.15 = (bf16[544,128]{1,0:T(8,128)(2,1)S(1)}, bf16[544,128]{1,0:T(8,128)(2,1)S(1)}, u32[]{:S(2)}, u32[]{:S(2)}) collective-permute-start(bf16[544,128]{1,0:T(8,128)(2,1)S(1)} %get-tuple-element.45.refs_5_), channel_id=1, source_target_pairs={{0,12},{4,8},{8,4},{12,0},{1,13},{5,9},{9,5},{13,1},{2,14},{6,10},... | collective-permute-start | bytes 417800 | tf_op jit(solution)/shard_map/ppermute | solution.py:39
  56.7 8.2 %collective-permute-done.11.refs_5_ = bf16[544,128]{1,0:T(8,128)(2,1)S(1)} collective-permute-done((bf16[544,128]{1,0:T(8,128)(2,1)S(1)}, bf16[544,128]{1,0:T(8,128)(2,1)S(1)}, u32[]{:S(2)}, u32[]{:S(2)}) %collective-permute-start.11) | collective-permute-done | bytes 139296 | tf_op jit(solution)/shard_map/ppermute | solution.py:39
  64.9 1.7 %collective-permute-start.21 = (bf16[544,128]{1,0:T(8,128)(2,1)S(1)}, bf16[544,128]{1,0:T(8,128)(2,1)S(1)}, u32[]{:S(2)}, u32[]{:S(2)}) collective-permute-start(bf16[544,128]{1,0:T(8,128)(2,1)S(1)} %collective-permute-done.19.refs_5_), channel_id=1, source_target_pairs={{0,2},{1,3},{2,0},{3,1},{4,6},{5,7},{6,4},{7,5},{8,10},{9,11},{10,... | collective-permute-start | bytes 417800 | tf_op jit(solution)/shard_map/ppermute | solution.py:39
  67.0 1.7 %collective-permute-start.17 = (bf16[544,128]{1,0:T(8,128)(2,1)S(1)}, bf16[544,128]{1,0:T(8,128)(2,1)S(1)}, u32[]{:S(2)}, u32[]{:S(2)}) collective-permute-start(bf16[544,128]{1,0:T(8,128)(2,1)S(1)} %collective-permute-done.15.refs_9_), channel_id=1, source_target_pairs={{0,2},{1,3},{2,0},{3,1},{4,6},{5,7},{6,4},{7,5},{8,10},{9,11},{10,... | collective-permute-start | bytes 417800 | tf_op jit(solution)/shard_map/ppermute | solution.py:39
  68.7 2.0 %collective-permute-done.21.refs_7_ = bf16[544,128]{1,0:T(8,128)(2,1)S(1)} collective-permute-done((bf16[544,128]{1,0:T(8,128)(2,1)S(1)}, bf16[544,128]{1,0:T(8,128)(2,1)S(1)}, u32[]{:S(2)}, u32[]{:S(2)}) %collective-permute-start.21) | collective-permute-done | bytes 139296 | tf_op jit(solution)/shard_map/ppermute | solution.py:39
  71.2 2.3 %collective-permute-done.13.refs_7_ = bf16[544,128]{1,0:T(8,128)(2,1)S(1)} collective-permute-done((bf16[544,128]{1,0:T(8,128)(2,1)S(1)}, bf16[544,128]{1,0:T(8,128)(2,1)S(1)}, u32[]{:S(2)}, u32[]{:S(2)}) %collective-permute-start.13) | collective-permute-done | bytes 139296 | tf_op jit(solution)/shard_map/ppermute | solution.py:39
  73.5 2.4 %collective-permute-done.17.refs_11_ = bf16[544,128]{1,0:T(8,128)(2,1)S(1)} collective-permute-done((bf16[544,128]{1,0:T(8,128)(2,1)S(1)}, bf16[544,128]{1,0:T(8,128)(2,1)S(1)}, u32[]{:S(2)}, u32[]{:S(2)}) %collective-permute-start.17) | collective-permute-done | bytes 139296 | tf_op jit(solution)/shard_map/ppermute | solution.py:39
  77.6 2.1 %shard_map.159.refs_1_ = bf16[4,256,768]{2,1,0:T(8,128)(2,1)S(1)} custom-call(s32[5]{0:T(128)S(1)} %compare_select_fusion.info, bf16[384,256]{1,0:T(8,128)(2,1)S(1)} %get-tuple-element.40.refs_0_, bf16[384,256]{1,0:T(8,128)(2,1)S(1)} %collective-permute-done.8.refs_1_, bf16[384,256]{1,0:T(8,128)(2,1)S(1)} %collective-permute-done.9.refs_2_, ...), custom_call_target="tpu_custom_call" | custom-call | tf_op jit(solution)/shard_map/pallas_call | solution.py:456
  79.8 3.9 %shard_map.160 = (f32[4,8,768]{2,1,0:T(8,128)S(1)}, f32[4,8,768]{2,1,0:T(8,128)S(1)}, f32[4,128,384]{2,1,0:T(8,128)S(1)}) custom-call(s32[5]{0:T(128)S(1)} %compare_select_fusion.info, f32[8]{0:T(128)S(1)} %copy-done.11, bf16[4,256,768]{2,1,0:T(8,128)(2,1)S(1)} %shard_map.159.refs_1_, f32[1,512]{1,0:T(1,128)S(1)} %bitcast.13, ...), custom_call_target="tpu_custom_call" | custom-call | tf_op jit(solution)/shard_map/pallas_call | solution.py:456
  83.7 4.0 %shard_map.161 = (f32[4,8,768]{2,1,0:T(8,128)S(1)}, f32[4,8,768]{2,1,0:T(8,128)S(1)}, f32[4,128,384]{2,1,0:T(8,128)S(1)}) custom-call(s32[5]{0:T(128)S(1)} %compare_select_fusion.info, f32[8]{0:T(128)S(1)} %copy-done.11, bf16[4,256,768]{2,1,0:T(8,128)(2,1)S(1)} %shard_map.159.refs_1_, f32[1,512]{1,0:T(1,128)S(1)} %bitcast.14, ...), custom_call_target="tpu_custom_call" | custom-call | tf_op jit(solution)/shard_map/pallas_call | solution.py:456
  87.8 4.3 %shard_map.163.refs_4_ = bf16[384,256]{1,0:T(8,128)(2,1)S(1)} custom-call(s32[5]{0:T(128)S(1)} %compare_select_fusion.info, f32[8]{0:T(128)S(1)} %copy-done.11, bf16[4,256,768]{2,1,0:T(8,128)(2,1)S(1)} %shard_map.159.refs_1_, f32[1,512]{1,0:T(1,128)S(1)} %bitcast.15, bf16[512,512]{1,0:T(8,128)(2,1)S(1)} %get-tuple-element.43.refs_3_, ...), custom_call_target="tpu_custom_call" | custom-call | tf_op jit(solution)/shard_map/pallas_call | solution.py:456
  92.1 1.6 %collective-permute-start.30 = (bf16[384,256]{1,0:T(8,128)(2,1)S(1)}, bf16[384,256]{1,0:T(8,128)(2,1)S(1)}, u32[]{:S(2)}, u32[]{:S(2)}) collective-permute-start(bf16[384,256]{1,0:T(8,128)(2,1)S(1)} %shard_map.163.refs_4_), channel_id=1, source_target_pairs={{0,2},{1,3},{2,0},{3,1},{4,6},{5,7},{6,4},{7,5},{8,10},{9,11},{10,... | collective-permute-start | bytes 589832 | tf_op jit(solution)/shard_map/ppermute | solution.py:39
  93.7 4.5 %shard_map.162.refs_0_ = bf16[384,256]{1,0:T(8,128)(2,1)S(1)} custom-call(s32[5]{0:T(128)S(1)} %compare_select_fusion.info, f32[8]{0:T(128)S(1)} %copy-done.11, bf16[4,256,768]{2,1,0:T(8,128)(2,1)S(1)} %shard_map.159.refs_1_, f32[1,512]{1,0:T(1,128)S(1)} %bitcast.16, bf16[512,512]{1,0:T(8,128)(2,1)S(1)} %get-tuple-element.43.refs_3_, ...), custom_call_target="tpu_custom_call" | custom-call | tf_op jit(solution)/shard_map/pallas_call | solution.py:456
  99.3 5.6 %collective-permute-done.27.refs_2_ = bf16[384,256]{1,0:T(8,128)(2,1)S(1)} collective-permute-done((bf16[384,256]{1,0:T(8,128)(2,1)S(1)}, bf16[384,256]{1,0:T(8,128)(2,1)S(1)}, u32[]{:S(2)}, u32[]{:S(2)}) %collective-permute-start.27) | collective-permute-done | bytes 196640 | tf_op jit(solution)/shard_map/ppermute | solution.py:39
  111.7 4.0 %collective-permute-done.33.refs_2_ = bf16[96,1024]{1,0:T(8,128)(2,1)S(1)} collective-permute-done((bf16[96,1024]{1,0:T(8,128)(2,1)S(1)}, bf16[96,1024]{1,0:T(8,128)(2,1)S(1)}, u32[]{:S(2)}, u32[]{:S(2)}) %collective-permute-start.33) | collective-permute-done | bytes 196640 | tf_op jit(solution)/shard_map/ppermute | solution.py:39
  115.7 2.6 %collective-permute-done.34.refs_3_ = bf16[96,1024]{1,0:T(8,128)(2,1)S(1)} collective-permute-done((bf16[96,1024]{1,0:T(8,128)(2,1)S(1)}, bf16[96,1024]{1,0:T(8,128)(2,1)S(1)}, u32[]{:S(2)}, u32[]{:S(2)}) %collective-permute-start.34) | collective-permute-done | bytes 196640 | tf_op jit(solution)/shard_map/ppermute | solution.py:39
  118.2 1.7 %shard_map.166 = bf16[96,4096]{1,0:T(8,128)(2,1)} custom-call(s32[5]{0:T(128)S(1)} %compare_select_fusion.info, bf16[96,1024]{1,0:T(8,128)(2,1)S(1)} %get-tuple-element.53.refs_0_, bf16[96,1024]{1,0:T(8,128)(2,1)S(1)} %collective-permute-done.32.refs_1_, bf16[96,1024]{1,0:T(8,128)(2,1)S(1)} %collective-permute-done.33.refs_2_, ...), custom_call_target="tpu_custom_call" | custom-call | tf_op jit(solution)/shard_map/pallas_call | solution.py:456
  (87 shorter events, 15.8 us)
Async XLA Ops:
  0.0 20.7 %collective-permute-start.1 = (bf16[96,4096]{1,0:T(8,128)(2,1)}, bf16[96,4096]{1,0:T(8,128)(2,1)S(1)}, u32[]{:S(2)}, u32[]{:S(2)}) collective-permute-start(bf16[96,4096]{1,0:T(8,128)(2,1)} %refs_8_.1), channel_id=1, source_target_pairs={{0,2},{1,3},{2,0},{3,1},{4,6},{5,7},{6,4},{7,5},{8,10},{9,11},{10,... | collective-permute-start | bytes 2359304 | tf_op jit(solution)/shard_map/ppermute | solution.py:39
  3.0 35.4 %collective-permute-start = (bf16[96,4096]{1,0:T(8,128)(2,1)}, bf16[96,4096]{1,0:T(8,128)(2,1)}, u32[]{:S(2)}, u32[]{:S(2)}) collective-permute-start(bf16[96,4096]{1,0:T(8,128)(2,1)} %refs_8_.1), channel_id=1, source_target_pairs={{0,1},{1,0},{2,3},{3,2},{4,5},{5,4},{6,7},{7,6},{8,9},{9,8},{10,11... | collective-permute-start | bytes 2359304 | tf_op jit(solution)/shard_map/ppermute | solution.py:39
  20.7 20.4 %collective-permute-start.2 = (bf16[96,4096]{1,0:T(8,128)(2,1)S(1)}, bf16[96,4096]{1,0:T(8,128)(2,1)S(1)}, u32[]{:S(2)}, u32[]{:S(2)}) collective-permute-start(bf16[96,4096]{1,0:T(8,128)(2,1)S(1)} %collective-permute-done.1.refs_2_), channel_id=1, source_target_pairs={{0,1},{1,0},{2,3},{3,2},{4,5},{5,4},{6,7},{7,6},{8,9},{9,8},{10,11... | collective-permute-start | bytes 2359304 | tf_op jit(solution)/shard_map/ppermute | solution.py:39
  27.1 4.9 %collective-permute-start.4 = (f32[5,1024]{1,0:T(8,128)S(1)}, f32[5,1024]{1,0:T(8,128)S(1)}, u32[]{:S(2)}, u32[]{:S(2)}) collective-permute-start(f32[5,1024]{1,0:T(8,128)S(1)} %fusion.2), channel_id=1, source_target_pairs={{0,8},{4,12},{8,0},{12,4},{1,9},{5,13},{9,1},{13,5},{2,10},{6,14},... | collective-permute-start | bytes 61448 | tf_op jit(solution)/shard_map/ppermute | solution.py:39
  33.7 7.3 %collective-permute-start.5 = (f32[5,1024]{1,0:T(8,128)S(1)}, f32[5,1024]{1,0:T(8,128)S(1)}, u32[]{:S(2)}, u32[]{:S(2)}) collective-permute-start(f32[5,1024]{1,0:T(8,128)S(1)} %add.18.refs_4_), channel_id=1, source_target_pairs={{0,1},{1,0},{2,3},{3,2},{4,5},{5,4},{6,7},{7,6},{8,9},{9,8},{10,11... | collective-permute-start | bytes 61448 | tf_op jit(solution)/shard_map/ppermute | solution.py:39
  35.9 5.1 %collective-permute-start.7 = (f32[5,1024]{1,0:T(8,128)S(1)}, f32[5,1024]{1,0:T(8,128)S(1)}, u32[]{:S(2)}, u32[]{:S(2)}) collective-permute-start(f32[5,1024]{1,0:T(8,128)S(1)} %collective-permute-done.6.refs_6_), channel_id=1, source_target_pairs={{0,1},{1,0},{2,3},{3,2},{4,5},{5,4},{6,7},{7,6},{8,9},{9,8},{10,11... | collective-permute-start | bytes 61448 | tf_op jit(solution)/shard_map/ppermute | solution.py:39
  45.4 6.1 %collective-permute-start.24 = (bf16[544,128]{1,0:T(8,128)(2,1)S(1)}, bf16[544,128]{1,0:T(8,128)(2,1)S(1)}, u32[]{:S(2)}, u32[]{:S(2)}) collective-permute-start(bf16[544,128]{1,0:T(8,128)(2,1)S(1)} %get-tuple-element.45.refs_5_), channel_id=1, source_target_pairs={{0,2},{1,3},{2,0},{3,1},{4,6},{5,7},{6,4},{7,5},{8,10},{9,11},{10,... | collective-permute-start | bytes 417800 | tf_op jit(solution)/shard_map/ppermute | solution.py:39
  47.1 7.2 %collective-permute-start.23 = (bf16[544,128]{1,0:T(8,128)(2,1)S(1)}, bf16[544,128]{1,0:T(8,128)(2,1)S(1)}, u32[]{:S(2)}, u32[]{:S(2)}) collective-permute-start(bf16[544,128]{1,0:T(8,128)(2,1)S(1)} %get-tuple-element.45.refs_5_), channel_id=1, source_target_pairs={{0,1},{1,0},{2,3},{3,2},{4,5},{5,4},{6,7},{7,6},{8,9},{9,8},{10,11... | collective-permute-start | bytes 417800 | tf_op jit(solution)/shard_map/ppermute | solution.py:39
  47.4 8.8 %collective-permute-start.19 = (bf16[544,128]{1,0:T(8,128)(2,1)S(1)}, bf16[544,128]{1,0:T(8,128)(2,1)S(1)}, u32[]{:S(2)}, u32[]{:S(2)}) collective-permute-start(bf16[544,128]{1,0:T(8,128)(2,1)S(1)} %get-tuple-element.45.refs_5_), channel_id=1, source_target_pairs={{0,4},{4,0},{8,12},{12,8},{1,5},{5,1},{9,13},{13,9},{2,6},{6,2},{1... | collective-permute-start | bytes 417800 | tf_op jit(solution)/shard_map/ppermute | solution.py:39
  48.9 7.2 %collective-permute-start.9 = (bf16[384,256]{1,0:T(8,128)(2,1)S(1)}, bf16[384,256]{1,0:T(8,128)(2,1)S(1)}, u32[]{:S(2)}, u32[]{:S(2)}) collective-permute-start(bf16[384,256]{1,0:T(8,128)(2,1)S(1)} %get-tuple-element.40.refs_0_), channel_id=1, source_target_pairs={{0,2},{1,3},{2,0},{3,1},{4,6},{5,7},{6,4},{7,5},{8,10},{9,11},{10,... | collective-permute-start | bytes 589832 | tf_op jit(solution)/shard_map/ppermute | solution.py:39
  49.5 17.1 %collective-permute-start.8 = (bf16[384,256]{1,0:T(8,128)(2,1)S(1)}, bf16[384,256]{1,0:T(8,128)(2,1)S(1)}, u32[]{:S(2)}, u32[]{:S(2)}) collective-permute-start(bf16[384,256]{1,0:T(8,128)(2,1)S(1)} %get-tuple-element.40.refs_0_), channel_id=1, source_target_pairs={{0,1},{1,0},{2,3},{3,2},{4,5},{5,4},{6,7},{7,6},{8,9},{9,8},{10,11... | collective-permute-start | bytes 589832 | tf_op jit(solution)/shard_map/ppermute | solution.py:39
  51.5 13.4 %collective-permute-start.11 = (bf16[544,128]{1,0:T(8,128)(2,1)S(1)}, bf16[544,128]{1,0:T(8,128)(2,1)S(1)}, u32[]{:S(2)}, u32[]{:S(2)}) collective-permute-start(bf16[544,128]{1,0:T(8,128)(2,1)S(1)} %get-tuple-element.45.refs_5_), channel_id=1, source_target_pairs={{0,8},{4,12},{8,0},{12,4},{1,9},{5,13},{9,1},{13,5},{2,10},{6,14},... | collective-permute-start | bytes 417800 | tf_op jit(solution)/shard_map/ppermute | solution.py:39
  54.3 12.2 %collective-permute-start.15 = (bf16[544,128]{1,0:T(8,128)(2,1)S(1)}, bf16[544,128]{1,0:T(8,128)(2,1)S(1)}, u32[]{:S(2)}, u32[]{:S(2)}) collective-permute-start(bf16[544,128]{1,0:T(8,128)(2,1)S(1)} %get-tuple-element.45.refs_5_), channel_id=1, source_target_pairs={{0,12},{4,8},{8,4},{12,0},{1,13},{5,9},{9,5},{13,1},{2,14},{6,10},... | collective-permute-start | bytes 417800 | tf_op jit(solution)/shard_map/ppermute | solution.py:39
  56.1 10.9 %collective-permute-start.25 = (bf16[544,128]{1,0:T(8,128)(2,1)S(1)}, bf16[544,128]{1,0:T(8,128)(2,1)S(1)}, u32[]{:S(2)}, u32[]{:S(2)}) collective-permute-start(bf16[544,128]{1,0:T(8,128)(2,1)S(1)} %collective-permute-done.24.refs_7_), channel_id=1, source_target_pairs={{0,1},{1,0},{2,3},{3,2},{4,5},{5,4},{6,7},{7,6},{8,9},{9,8},{10,11... | collective-permute-start | bytes 417800 | tf_op jit(solution)/shard_map/ppermute | solution.py:39
  56.1 19.8 %collective-permute-start.10 = (bf16[384,256]{1,0:T(8,128)(2,1)S(1)}, bf16[384,256]{1,0:T(8,128)(2,1)S(1)}, u32[]{:S(2)}, u32[]{:S(2)}) collective-permute-start(bf16[384,256]{1,0:T(8,128)(2,1)S(1)} %collective-permute-done.9.refs_2_), channel_id=1, source_target_pairs={{0,1},{1,0},{2,3},{3,2},{4,5},{5,4},{6,7},{7,6},{8,9},{9,8},{10,11... | collective-permute-start | bytes 589832 | tf_op jit(solution)/shard_map/ppermute | solution.py:39
  64.9 5.8 %collective-permute-start.21 = (bf16[544,128]{1,0:T(8,128)(2,1)S(1)}, bf16[544,128]{1,0:T(8,128)(2,1)S(1)}, u32[]{:S(2)}, u32[]{:S(2)}) collective-permute-start(bf16[544,128]{1,0:T(8,128)(2,1)S(1)} %collective-permute-done.19.refs_5_), channel_id=1, source_target_pairs={{0,2},{1,3},{2,0},{3,1},{4,6},{5,7},{6,4},{7,5},{8,10},{9,11},{10,... | collective-permute-start | bytes 417800 | tf_op jit(solution)/shard_map/ppermute | solution.py:39
  66.6 4.1 %collective-permute-start.20 = (bf16[544,128]{1,0:T(8,128)(2,1)S(1)}, bf16[544,128]{1,0:T(8,128)(2,1)S(1)}, u32[]{:S(2)}, u32[]{:S(2)}) collective-permute-start(bf16[544,128]{1,0:T(8,128)(2,1)S(1)} %collective-permute-done.19.refs_5_), channel_id=1, source_target_pairs={{0,1},{1,0},{2,3},{3,2},{4,5},{5,4},{6,7},{7,6},{8,9},{9,8},{10,11... | collective-permute-start | bytes 417800 | tf_op jit(solution)/shard_map/ppermute | solution.py:39
  66.6 6.9 %collective-permute-start.13 = (bf16[544,128]{1,0:T(8,128)(2,1)S(1)}, bf16[544,128]{1,0:T(8,128)(2,1)S(1)}, u32[]{:S(2)}, u32[]{:S(2)}) collective-permute-start(bf16[544,128]{1,0:T(8,128)(2,1)S(1)} %collective-permute-done.11.refs_5_), channel_id=1, source_target_pairs={{0,2},{1,3},{2,0},{3,1},{4,6},{5,7},{6,4},{7,5},{8,10},{9,11},{10,... | collective-permute-start | bytes 417800 | tf_op jit(solution)/shard_map/ppermute | solution.py:39
  67.0 8.9 %collective-permute-start.17 = (bf16[544,128]{1,0:T(8,128)(2,1)S(1)}, bf16[544,128]{1,0:T(8,128)(2,1)S(1)}, u32[]{:S(2)}, u32[]{:S(2)}) collective-permute-start(bf16[544,128]{1,0:T(8,128)(2,1)S(1)} %collective-permute-done.15.refs_9_), channel_id=1, source_target_pairs={{0,2},{1,3},{2,0},{3,1},{4,6},{5,7},{6,4},{7,5},{8,10},{9,11},{10,... | collective-permute-start | bytes 417800 | tf_op jit(solution)/shard_map/ppermute | solution.py:39
  70.7 13.1 %collective-permute-start.22 = (bf16[544,128]{1,0:T(8,128)(2,1)S(1)}, bf16[544,128]{1,0:T(8,128)(2,1)S(1)}, u32[]{:S(2)}, u32[]{:S(2)}) collective-permute-start(bf16[544,128]{1,0:T(8,128)(2,1)S(1)} %collective-permute-done.21.refs_7_), channel_id=1, source_target_pairs={{0,1},{1,0},{2,3},{3,2},{4,5},{5,4},{6,7},{7,6},{8,9},{9,8},{10,11... | collective-permute-start | bytes 417800 | tf_op jit(solution)/shard_map/ppermute | solution.py:39
  70.7 17.1 %collective-permute-start.12 = (bf16[544,128]{1,0:T(8,128)(2,1)S(1)}, bf16[544,128]{1,0:T(8,128)(2,1)S(1)}, u32[]{:S(2)}, u32[]{:S(2)}) collective-permute-start(bf16[544,128]{1,0:T(8,128)(2,1)S(1)} %collective-permute-done.11.refs_5_), channel_id=1, source_target_pairs={{0,1},{1,0},{2,3},{3,2},{4,5},{5,4},{6,7},{7,6},{8,9},{9,8},{10,11... | collective-permute-start | bytes 417800 | tf_op jit(solution)/shard_map/ppermute | solution.py:39
  73.5 14.3 %collective-permute-start.16 = (bf16[544,128]{1,0:T(8,128)(2,1)S(1)}, bf16[544,128]{1,0:T(8,128)(2,1)S(1)}, u32[]{:S(2)}, u32[]{:S(2)}) collective-permute-start(bf16[544,128]{1,0:T(8,128)(2,1)S(1)} %collective-permute-done.15.refs_9_), channel_id=1, source_target_pairs={{0,1},{1,0},{2,3},{3,2},{4,5},{5,4},{6,7},{7,6},{8,9},{9,8},{10,11... | collective-permute-start | bytes 417800 | tf_op jit(solution)/shard_map/ppermute | solution.py:39
  75.9 11.9 %collective-permute-start.14 = (bf16[544,128]{1,0:T(8,128)(2,1)S(1)}, bf16[544,128]{1,0:T(8,128)(2,1)S(1)}, u32[]{:S(2)}, u32[]{:S(2)}) collective-permute-start(bf16[544,128]{1,0:T(8,128)(2,1)S(1)} %collective-permute-done.13.refs_7_), channel_id=1, source_target_pairs={{0,1},{1,0},{2,3},{3,2},{4,5},{5,4},{6,7},{7,6},{8,9},{9,8},{10,11... | collective-permute-start | bytes 417800 | tf_op jit(solution)/shard_map/ppermute | solution.py:39
  75.9 11.9 %collective-permute-start.18 = (bf16[544,128]{1,0:T(8,128)(2,1)S(1)}, bf16[544,128]{1,0:T(8,128)(2,1)S(1)}, u32[]{:S(2)}, u32[]{:S(2)}) collective-permute-start(bf16[544,128]{1,0:T(8,128)(2,1)S(1)} %collective-permute-done.17.refs_11_), channel_id=1, source_target_pairs={{0,1},{1,0},{2,3},{3,2},{4,5},{5,4},{6,7},{7,6},{8,9},{9,8},{10,11... | collective-permute-start | bytes 417800 | tf_op jit(solution)/shard_map/ppermute | solution.py:39
  92.1 7.2 %collective-permute-start.30 = (bf16[384,256]{1,0:T(8,128)(2,1)S(1)}, bf16[384,256]{1,0:T(8,128)(2,1)S(1)}, u32[]{:S(2)}, u32[]{:S(2)}) collective-permute-start(bf16[384,256]{1,0:T(8,128)(2,1)S(1)} %shard_map.163.refs_4_), channel_id=1, source_target_pairs={{0,2},{1,3},{2,0},{3,1},{4,6},{5,7},{6,4},{7,5},{8,10},{9,11},{10,... | collective-permute-start | bytes 589832 | tf_op jit(solution)/shard_map/ppermute | solution.py:39
  98.2 6.6 %collective-permute-start.27 = (bf16[384,256]{1,0:T(8,128)(2,1)S(1)}, bf16[384,256]{1,0:T(8,128)(2,1)S(1)}, u32[]{:S(2)}, u32[]{:S(2)}) collective-permute-start(bf16[384,256]{1,0:T(8,128)(2,1)S(1)} %shard_map.162.refs_0_), channel_id=1, source_target_pairs={{0,2},{1,3},{2,0},{3,1},{4,6},{5,7},{6,4},{7,5},{8,10},{9,11},{10,... | collective-permute-start | bytes 589832 | tf_op jit(solution)/shard_map/ppermute | solution.py:39
  98.8 6.1 %collective-permute-start.29 = (bf16[384,256]{1,0:T(8,128)(2,1)S(1)}, bf16[384,256]{1,0:T(8,128)(2,1)S(1)}, u32[]{:S(2)}, u32[]{:S(2)}) collective-permute-start(bf16[384,256]{1,0:T(8,128)(2,1)S(1)} %shard_map.163.refs_4_), channel_id=1, source_target_pairs={{0,1},{1,0},{2,3},{3,2},{4,5},{5,4},{6,7},{7,6},{8,9},{9,8},{10,11... | collective-permute-start | bytes 589832 | tf_op jit(solution)/shard_map/ppermute | solution.py:39
  98.8 6.1 %collective-permute-start.26 = (bf16[384,256]{1,0:T(8,128)(2,1)S(1)}, bf16[384,256]{1,0:T(8,128)(2,1)S(1)}, u32[]{:S(2)}, u32[]{:S(2)}) collective-permute-start(bf16[384,256]{1,0:T(8,128)(2,1)S(1)} %shard_map.162.refs_0_), channel_id=1, source_target_pairs={{0,1},{1,0},{2,3},{3,2},{4,5},{5,4},{6,7},{7,6},{8,9},{9,8},{10,11... | collective-permute-start | bytes 589832 | tf_op jit(solution)/shard_map/ppermute | solution.py:39
  99.3 5.6 %collective-permute-start.31 = (bf16[384,256]{1,0:T(8,128)(2,1)S(1)}, bf16[384,256]{1,0:T(8,128)(2,1)S(1)}, u32[]{:S(2)}, u32[]{:S(2)}) collective-permute-start(bf16[384,256]{1,0:T(8,128)(2,1)S(1)} %collective-permute-done.30.refs_6_), channel_id=1, source_target_pairs={{0,1},{1,0},{2,3},{3,2},{4,5},{5,4},{6,7},{7,6},{8,9},{9,8},{10,11... | collective-permute-start | bytes 589832 | tf_op jit(solution)/shard_map/ppermute | solution.py:39
  107.8 7.8 %collective-permute-start.33 = (bf16[96,1024]{1,0:T(8,128)(2,1)S(1)}, bf16[96,1024]{1,0:T(8,128)(2,1)S(1)}, u32[]{:S(2)}, u32[]{:S(2)}) collective-permute-start(bf16[96,1024]{1,0:T(8,128)(2,1)S(1)} %get-tuple-element.55), channel_id=1, source_target_pairs={{0,2},{1,3},{2,0},{3,1},{4,6},{5,7},{6,4},{7,5},{8,10},{9,11},{10,... | collective-permute-start | bytes 589832 | tf_op jit(solution)/shard_map/ppermute | solution.py:39
  108.4 9.9 %collective-permute-start.34 = (bf16[96,1024]{1,0:T(8,128)(2,1)S(1)}, bf16[96,1024]{1,0:T(8,128)(2,1)S(1)}, u32[]{:S(2)}, u32[]{:S(2)}) collective-permute-start(bf16[96,1024]{1,0:T(8,128)(2,1)S(1)} %get-tuple-element.56), channel_id=1, source_target_pairs={{0,3},{1,2},{2,1},{3,0},{4,7},{5,6},{6,5},{7,4},{8,11},{9,10},{10,... | collective-permute-start | bytes 589832 | tf_op jit(solution)/shard_map/ppermute | solution.py:39
  110.9 7.3 %collective-permute-start.32 = (bf16[96,1024]{1,0:T(8,128)(2,1)S(1)}, bf16[96,1024]{1,0:T(8,128)(2,1)S(1)}, u32[]{:S(2)}, u32[]{:S(2)}) collective-permute-start(bf16[96,1024]{1,0:T(8,128)(2,1)S(1)} %get-tuple-element.54), channel_id=1, source_target_pairs={{0,1},{1,0},{2,3},{3,2},{4,5},{5,4},{6,7},{7,6},{8,9},{9,8},{10,11... | collective-permute-start | bytes 589832 | tf_op jit(solution)/shard_map/ppermute | solution.py:39
  (17 other events, 335.7 us)

commit v5 on v4

--- a/solution.py
+++ b/solution.py
@@ -307,33 +307,42 @@
     return jnp.sum(values.reshape(-1, 8, values.shape[1]), axis=0)
 
 
-def attend_kernel(counts, tok_keys, seg, merged, first, last, chosen, info, *refs):
+def attend_kernel(counts, tok_keys, seg, merged, first, last, chosen, reuse, info, *refs):
     ids = member_ids(info, counts[0])
     bias_ref, q_ref, gain_ref, wk_ref, wv_ref = refs[:5]
     refs = refs[5:]
     blocks = []
-    for count in counts:
+    for count in [] if reuse else counts:
         blocks.append(refs[: count + (0 if merged else 1)])
         refs = refs[len(blocks[-1]) :]
     if not first:
         state_in, refs = refs[:3], refs[3:]
+    if reuse:
+        scratch, r_ref, refs = refs[0], refs[1], refs[2:]
     if last:
         out_ref, refs = refs[0], refs[1:]
     else:
         state_out, refs = refs[:3], refs[3:]
-    scratch, k_ref, v_ref, r_ref = refs
+    if reuse:
+        k_ref, v_ref = refs
+    else:
+        scratch, r_ref, k_ref, v_ref = refs
     lanes = q_ref.shape[2]
     rows = lanes // 2
     heads_of = slice(chosen[0] * LANES, (chosen[-1] + 1) * LANES)
-    for number, block in enumerate(blocks):
+    for number in range(len(counts)):
+        block = () if reuse else blocks[number]
         pieces = block if merged else block[:-1]
         base = number * seg
         rows_ref = scratch.at[number]
-        normed_into(rows_ref, ids, pieces, gain_ref)
+        if not reuse:
+            normed_into(rows_ref, ids, pieces, gain_ref)
         k_ref[base : base + seg, :] = f32_dot(rows_ref[...], wk_ref[:, heads_of]).astype(jnp.bfloat16)
         v_ref[number] = lax.dot_general(
             wv_ref[heads_of, :], rows_ref[...], (((1,), (1,)), ((), ())), preferred_element_type=jnp.float32
         ).astype(jnp.bfloat16)
+        if reuse:
+            continue
         if merged:
             quarter = seg // len(pieces)
             sub = quarter // (LANES // ROTARY_DIM)
@@ -355,7 +364,7 @@
         key = jnp.concatenate([k_ref[base : base + seg, span], r_ref[base : base + seg, :]], axis=1)
         return f32_dot(key, q_ref[pair])
 
-    steps = [(pair, number) for pair in chosen for number in range(len(blocks))]
+    steps = [(pair, number) for pair in chosen for number in range(len(counts))]
     ahead = score(*steps[0])
     for local, pair in enumerate(chosen):
         span = slice(local * LANES, (local + 1) * LANES)
@@ -364,9 +373,9 @@
         if not first:
             top = state_in[0][pair, :1, :]
             total, acc = state_in[1][pair], state_in[2][pair]
-        for number in range(len(blocks)):
+        for number in range(len(counts)):
             scores = ahead
-            after = local * len(blocks) + number + 1
+            after = local * len(counts) + number + 1
             if after < len(steps):
                 ahead = score(*steps[after])
             lat, ctx = scores[:tok_keys], scores[tok_keys:]
@@ -408,22 +417,22 @@
     pieces = refs[: count * splits]
     w_ref = refs[count * splits]
     outs = refs[1 + count * splits :]
-    depth = pieces[0].shape[1]
     rows = outs[0].shape[0]
     for place_of in range(0, len(wanted), 2):
         group = wanted[place_of : place_of + 2]
         total = None
-        for number, piece in enumerate(pieces):
-            split, member = divmod(number, count)
-            start = aligned((ids[member] * splits + split) * depth, LANES)
+        for member in range(count):
+            sides = pieces[member::count]
             if parts == 1:
-                left = piece[...]
+                strips = [[side[...]] for side in sides]
             else:
-                left = jnp.concatenate(
-                    [piece[pl.ds(aligned(ids[owner] * rows, 16), rows), :] for owner in group],
-                    axis=0,
-                )
-            part = f32_dot(left, w_ref[pl.ds(start, depth), :])
+                strips = [
+                    [side[pl.ds(aligned(ids[owner] * rows, 16), rows), :] for owner in group]
+                    for side in sides
+                ]
+            left = jnp.concatenate([jnp.concatenate(strip, axis=0) for strip in strips], axis=1)
+            start = aligned(ids[member] * left.shape[1], LANES)
+            part = f32_dot(left, w_ref[pl.ds(start, left.shape[1]), :])
             total = part if total is None else total + part
         for number in range(len(group)):
             outs[place_of + number][...] = total[number * rows : (number + 1) * rows].astype(
@@ -623,8 +632,21 @@
         shape_of((pairs, LANES, tok_count), jnp.float32),
     ]
 
-    def attend(part, first, last, chosen, state):
+    def attend(part, first, last, chosen, state, kept=(), keep=False):
         heads = len(chosen) * LANES
+        outs = [shape_of((tok_count, heads), bf16)] if last else held
+        carried = [
+            ((len(part), seg_rows, latent_norm_gain.shape[0]), bf16),
+            ((len(part) * seg_rows, LANES), bf16),
+        ]
+        scratch = [
+            VMEM((len(part) * seg_rows, heads), bf16),
+            VMEM((len(part), heads, seg_rows), bf16),
+        ]
+        if keep:
+            outs = outs + [shape_of(*one) for one in carried]
+        elif not kept:
+            scratch = [VMEM(*one) for one in carried] + scratch
         return call(
             functools.partial(
                 attend_kernel,
@@ -635,8 +657,9 @@
                 first,
                 last,
                 chosen,
+                bool(kept),
             ),
-            shape_of((tok_count, heads), bf16) if last else held,
+            outs,
             [
                 info,
                 context_bias,
@@ -644,16 +667,12 @@
                 latent_norm_gain[None, :],
                 w_k,
                 w_vt,
-                *[piece for block in part for piece in block],
+                *([] if kept else [piece for block in part for piece in block]),
                 *state,
+                *kept,
             ],
             smem=(0, 1),
-            scratch=[
-                VMEM((len(part), seg_rows, latent_norm_gain.shape[0]), bf16),
-                VMEM((len(part) * seg_rows, heads), bf16),
-                VMEM((len(part), heads, seg_rows), bf16),
-                VMEM((len(part) * seg_rows, LANES), bf16),
-            ],
+            scratch=scratch,
             mib=16,
         )
 
@@ -668,8 +687,11 @@
             state = attend(part, first, False, every, state)
         begin += len(part)
     splits = [every[: pairs // 2], every[pairs // 2 :]] if pairs > 1 else [every]
-    for chosen in splits:
-        done = attend(part, first, True, chosen, state)
+    kept = ()
+    for number, chosen in enumerate(splits):
+        keep = number == 0 and len(splits) > 1
+        done, *more = attend(part, first, True, chosen, state, kept, keep)
+        kept = tuple(more) or kept
         att_pieces.append(spread(done))
     out_cols = w_out.shape[1]
     parts = tp_count if small and own_rows % 16 == 0 else 1

time: 120 us -> 123 us (1.025)
  waiting for transfers between devices: 53.3 us -> 56.2 us
    ppermute x35, waiting for transfers between devices: 53.3 us -> 56.2 us  [swap(): return lax.ppermute(value, axis, [(i, i ^ bit) for i in range(count)])]
  transfers between devices with their start and end apart: 35 -> 35, of which waited for: 13 -> 14; matrix products, arithmetic and copies ran while one was open for 3% -> 3% of each run, Pallas kernels for 19% -> 15%
where the time goes in v5:
time: 123 us; the launch traced here: 122 us
  waiting for transfers between devices  56.2 us (46%)
  Pallas kernels  33.5 us (27%)
  starting transfers between devices  28.4 us (23%)
  matrix products  2.74 us (2%)
    ppermute x35, waiting for transfers between devices, swap(): return lax.ppermute(value, axis, [(i, i ^ bit) for i in range(count)])  56.2 us
    pallas_call x13, Pallas kernels, call(): pl.pallas_call(kernel, out_shape=outs, in_specs=specs, out_specs=[in_vmem...  33.5 us
    ppermute x35, starting transfers between devices, swap(): return lax.ppermute(value, axis, [(i, i ^ bit) for i in range(count)])  28.4 us
    dot_general x3, matrix products, f32_dot(): return jnp.dot(a, b, preferred_element_type=jnp.float32)  2.74 us
  transfers between devices with their start and end apart: 35, of which 14 were waited for; matrix products, arithmetic and copies ran while one was open for 3% of the time, Pallas kernels for 15%

profile of v5, /device:TPU:0, one launch (start us, length us, event | category | flops | bytes accessed | tf_op | source)
XLA Modules:
  0.0 122.2 jit_solution(5893358672890116501)
XLA Ops:
  0.0 3.0 %collective-permute-start.1 = (bf16[96,4096]{1,0:T(8,128)(2,1)}, bf16[96,4096]{1,0:T(8,128)(2,1)S(1)}, u32[]{:S(2)}, u32[]{:S(2)}) collective-permute-start(bf16[96,4096]{1,0:T(8,128)(2,1)} %refs_8_.1), channel_id=1, source_target_pairs={{0,2},{1,3},{2,0},{3,1},{4,6},{5,7},{6,4},{7,5},{8,10},{9,11},{10,... | collective-permute-start | bytes 2359304 | tf_op jit(solution)/shard_map/ppermute | solution.py:39
  4.3 16.5 %collective-permute-done.1.refs_2_ = bf16[96,4096]{1,0:T(8,128)(2,1)S(1)} collective-permute-done((bf16[96,4096]{1,0:T(8,128)(2,1)}, bf16[96,4096]{1,0:T(8,128)(2,1)S(1)}, u32[]{:S(2)}, u32[]{:S(2)}) %collective-permute-start.1) | collective-permute-done | bytes 786464 | tf_op jit(solution)/shard_map/ppermute | solution.py:39
  21.1 2.0 %fusion.4 = f32[2,1024]{1,0:T(2,128)S(1)} fusion(bf16[2,1024]{1,0:T(2,128)(2,1)S(1)} %fusion, bf16[1024,1024]{1,0:T(8,128)(2,1)} %param.20), kind=kOutput, calls=%fused_computation.8 | convolution fusion | flops 4194304 | bytes 2109440 | tf_op jit(solution)/shard_map/dot_general | solution.py:34
  23.1 1.9 %collective-permute-start.3 = (f32[5,1024]{1,0:T(8,128)S(1)}, f32[5,1024]{1,0:T(8,128)S(1)}, u32[]{:S(2)}, u32[]{:S(2)}) collective-permute-start(f32[5,1024]{1,0:T(8,128)S(1)} %pad_maximum_fusion), channel_id=1, source_target_pairs={{0,4},{4,0},{8,12},{12,8},{1,5},{5,1},{9,13},{13,9},{2,6},{6,2},{1... | collective-permute-start | bytes 61448 | tf_op jit(solution)/shard_map/ppermute | solution.py:39
  25.0 2.1 %collective-permute-done.3 = f32[5,1024]{1,0:T(8,128)S(1)} collective-permute-done((f32[5,1024]{1,0:T(8,128)S(1)}, f32[5,1024]{1,0:T(8,128)S(1)}, u32[]{:S(2)}, u32[]{:S(2)}) %collective-permute-start.3) | collective-permute-done | bytes 20512 | tf_op jit(solution)/shard_map/ppermute | solution.py:39
  27.1 2.9 %collective-permute-start.4 = (f32[5,1024]{1,0:T(8,128)S(1)}, f32[5,1024]{1,0:T(8,128)S(1)}, u32[]{:S(2)}, u32[]{:S(2)}) collective-permute-start(f32[5,1024]{1,0:T(8,128)S(1)} %fusion.2), channel_id=1, source_target_pairs={{0,8},{4,12},{8,0},{12,4},{1,9},{5,13},{9,1},{13,5},{2,10},{6,14},... | collective-permute-start | bytes 61448 | tf_op jit(solution)/shard_map/ppermute | solution.py:39
  30.0 2.0 %collective-permute-done.4 = f32[5,1024]{1,0:T(8,128)S(1)} collective-permute-done((f32[5,1024]{1,0:T(8,128)S(1)}, f32[5,1024]{1,0:T(8,128)S(1)}, u32[]{:S(2)}, u32[]{:S(2)}) %collective-permute-start.4) | collective-permute-done | bytes 20512 | tf_op jit(solution)/shard_map/ppermute | solution.py:39
  32.0 1.7 %collective-permute-start.6 = (f32[5,1024]{1,0:T(8,128)S(1)}, f32[5,1024]{1,0:T(8,128)S(1)}, u32[]{:S(2)}, u32[]{:S(2)}) collective-permute-start(f32[5,1024]{1,0:T(8,128)S(1)} %add.18.refs_4_), channel_id=1, source_target_pairs={{0,2},{1,3},{2,0},{3,1},{4,6},{5,7},{6,4},{7,5},{8,10},{9,11},{10,... | collective-permute-start | bytes 61448 | tf_op jit(solution)/shard_map/ppermute | solution.py:39
  33.7 2.2 %collective-permute-done.6.refs_6_ = f32[5,1024]{1,0:T(8,128)S(1)} collective-permute-done((f32[5,1024]{1,0:T(8,128)S(1)}, f32[5,1024]{1,0:T(8,128)S(1)}, u32[]{:S(2)}, u32[]{:S(2)}) %collective-permute-start.6) | collective-permute-done | bytes 20512 | tf_op jit(solution)/shard_map/ppermute | solution.py:39
  38.4 2.7 %shard_map.154 = (f32[96,4096]{1,0:T(8,128)S(1)}, f32[96,4096]{1,0:T(8,128)S(1)}, f32[128,4096]{1,0:T(8,128)S(1)}) custom-call(bf16[96,4096]{1,0:T(8,128)(2,1)S(1)} %copy-done.2, bf16[96,4096]{1,0:T(8,128)(2,1)} %collective-permute-done.refs_1_, bf16[128,4096]{1,0:T(8,128)(2,1)S(1)} %copy-done.6), custom_call_target="tpu_custom_call" | custom-call | tf_op jit(solution)/shard_map/pallas_call | solution.py:465
  41.1 4.3 %shard_map.157 = (bf16[384,256]{1,0:T(8,128)(2,1)S(1)}, bf16[544,128]{1,0:T(8,128)(2,1)S(1)}, bf16[16,128]{1,0:T(8,128)(2,1)}) custom-call(s32[5]{0:T(128)S(1)} %compare_select_fusion.info, f32[96,4096]{1,0:T(8,128)S(1)} %get-tuple-element.35.refs_0_, f32[96,4096]{1,0:T(8,128)S(1)} %get-tuple-element.36.refs_1_, ...), custom_call_target="tpu_custom_call" | custom-call | tf_op jit(solution)/shard_map/pallas_call | solution.py:465
  45.4 1.7 %collective-permute-start.24 = (bf16[544,128]{1,0:T(8,128)(2,1)S(1)}, bf16[544,128]{1,0:T(8,128)(2,1)S(1)}, u32[]{:S(2)}, u32[]{:S(2)}) collective-permute-start(bf16[544,128]{1,0:T(8,128)(2,1)S(1)} %get-tuple-element.48.refs_5_), channel_id=1, source_target_pairs={{0,2},{1,3},{2,0},{3,1},{4,6},{5,7},{6,4},{7,5},{8,10},{9,11},{10,... | collective-permute-start | bytes 417800 | tf_op jit(solution)/shard_map/ppermute | solution.py:39
  49.5 2.0 %collective-permute-done.24.refs_7_ = bf16[544,128]{1,0:T(8,128)(2,1)S(1)} collective-permute-done((bf16[544,128]{1,0:T(8,128)(2,1)S(1)}, bf16[544,128]{1,0:T(8,128)(2,1)S(1)}, u32[]{:S(2)}, u32[]{:S(2)}) %collective-permute-start.24) | collective-permute-done | bytes 139296 | tf_op jit(solution)/shard_map/ppermute | solution.py:39
  51.5 2.9 %collective-permute-start.11 = (bf16[544,128]{1,0:T(8,128)(2,1)S(1)}, bf16[544,128]{1,0:T(8,128)(2,1)S(1)}, u32[]{:S(2)}, u32[]{:S(2)}) collective-permute-start(bf16[544,128]{1,0:T(8,128)(2,1)S(1)} %get-tuple-element.48.refs_5_), channel_id=1, source_target_pairs={{0,8},{4,12},{8,0},{12,4},{1,9},{5,13},{9,1},{13,5},{2,10},{6,14},... | collective-permute-start | bytes 417800 | tf_op jit(solution)/shard_map/ppermute | solution.py:39
  54.3 1.8 %collective-permute-start.15 = (bf16[544,128]{1,0:T(8,128)(2,1)S(1)}, bf16[544,128]{1,0:T(8,128)(2,1)S(1)}, u32[]{:S(2)}, u32[]{:S(2)}) collective-permute-start(bf16[544,128]{1,0:T(8,128)(2,1)S(1)} %get-tuple-element.48.refs_5_), channel_id=1, source_target_pairs={{0,12},{4,8},{8,4},{12,0},{1,13},{5,9},{9,5},{13,1},{2,14},{6,10},... | collective-permute-start | bytes 417800 | tf_op jit(solution)/shard_map/ppermute | solution.py:39
  56.7 8.2 %collective-permute-done.11.refs_5_ = bf16[544,128]{1,0:T(8,128)(2,1)S(1)} collective-permute-done((bf16[544,128]{1,0:T(8,128)(2,1)S(1)}, bf16[544,128]{1,0:T(8,128)(2,1)S(1)}, u32[]{:S(2)}, u32[]{:S(2)}) %collective-permute-start.11) | collective-permute-done | bytes 139296 | tf_op jit(solution)/shard_map/ppermute | solution.py:39
  64.9 1.7 %collective-permute-start.21 = (bf16[544,128]{1,0:T(8,128)(2,1)S(1)}, bf16[544,128]{1,0:T(8,128)(2,1)S(1)}, u32[]{:S(2)}, u32[]{:S(2)}) collective-permute-start(bf16[544,128]{1,0:T(8,128)(2,1)S(1)} %collective-permute-done.19.refs_5_), channel_id=1, source_target_pairs={{0,2},{1,3},{2,0},{3,1},{4,6},{5,7},{6,4},{7,5},{8,10},{9,11},{10,... | collective-permute-start | bytes 417800 | tf_op jit(solution)/shard_map/ppermute | solution.py:39
  67.0 1.7 %collective-permute-start.17 = (bf16[544,128]{1,0:T(8,128)(2,1)S(1)}, bf16[544,128]{1,0:T(8,128)(2,1)S(1)}, u32[]{:S(2)}, u32[]{:S(2)}) collective-permute-start(bf16[544,128]{1,0:T(8,128)(2,1)S(1)} %collective-permute-done.15.refs_9_), channel_id=1, source_target_pairs={{0,2},{1,3},{2,0},{3,1},{4,6},{5,7},{6,4},{7,5},{8,10},{9,11},{10,... | collective-permute-start | bytes 417800 | tf_op jit(solution)/shard_map/ppermute | solution.py:39
  68.7 2.0 %collective-permute-done.21.refs_7_ = bf16[544,128]{1,0:T(8,128)(2,1)S(1)} collective-permute-done((bf16[544,128]{1,0:T(8,128)(2,1)S(1)}, bf16[544,128]{1,0:T(8,128)(2,1)S(1)}, u32[]{:S(2)}, u32[]{:S(2)}) %collective-permute-start.21) | collective-permute-done | bytes 139296 | tf_op jit(solution)/shard_map/ppermute | solution.py:39
  71.2 2.4 %collective-permute-done.13.refs_7_ = bf16[544,128]{1,0:T(8,128)(2,1)S(1)} collective-permute-done((bf16[544,128]{1,0:T(8,128)(2,1)S(1)}, bf16[544,128]{1,0:T(8,128)(2,1)S(1)}, u32[]{:S(2)}, u32[]{:S(2)}) %collective-permute-start.13) | collective-permute-done | bytes 139296 | tf_op jit(solution)/shard_map/ppermute | solution.py:39
  73.5 2.4 %collective-permute-done.17.refs_11_ = bf16[544,128]{1,0:T(8,128)(2,1)S(1)} collective-permute-done((bf16[544,128]{1,0:T(8,128)(2,1)S(1)}, bf16[544,128]{1,0:T(8,128)(2,1)S(1)}, u32[]{:S(2)}, u32[]{:S(2)}) %collective-permute-start.17) | collective-permute-done | bytes 139296 | tf_op jit(solution)/shard_map/ppermute | solution.py:39
  77.6 2.1 %shard_map.159.refs_1_ = bf16[4,256,768]{2,1,0:T(8,128)(2,1)S(1)} custom-call(s32[5]{0:T(128)S(1)} %compare_select_fusion.info, bf16[384,256]{1,0:T(8,128)(2,1)S(1)} %get-tuple-element.43.refs_0_, bf16[384,256]{1,0:T(8,128)(2,1)S(1)} %collective-permute-done.8.refs_1_, bf16[384,256]{1,0:T(8,128)(2,1)S(1)} %collective-permute-done.9.refs_2_, ...), custom_call_target="tpu_custom_call" | custom-call | tf_op jit(solution)/shard_map/pallas_call | solution.py:465
  79.8 3.9 %shard_map.160 = (f32[4,8,768]{2,1,0:T(8,128)S(1)}, f32[4,8,768]{2,1,0:T(8,128)S(1)}, f32[4,128,384]{2,1,0:T(8,128)S(1)}) custom-call(s32[5]{0:T(128)S(1)} %compare_select_fusion.info, f32[8]{0:T(128)S(1)} %copy-done.11, bf16[4,256,768]{2,1,0:T(8,128)(2,1)S(1)} %shard_map.159.refs_1_, f32[1,512]{1,0:T(1,128)S(1)} %bitcast.13, ...), custom_call_target="tpu_custom_call" | custom-call | tf_op jit(solution)/shard_map/pallas_call | solution.py:465
  83.7 4.0 %shard_map.161 = (f32[4,8,768]{2,1,0:T(8,128)S(1)}, f32[4,8,768]{2,1,0:T(8,128)S(1)}, f32[4,128,384]{2,1,0:T(8,128)S(1)}) custom-call(s32[5]{0:T(128)S(1)} %compare_select_fusion.info, f32[8]{0:T(128)S(1)} %copy-done.11, bf16[4,256,768]{2,1,0:T(8,128)(2,1)S(1)} %shard_map.159.refs_1_, f32[1,512]{1,0:T(1,128)S(1)} %bitcast.14, ...), custom_call_target="tpu_custom_call" | custom-call | tf_op jit(solution)/shard_map/pallas_call | solution.py:465
  87.8 4.3 %shard_map.162 = (bf16[384,256]{1,0:T(8,128)(2,1)S(1)}, bf16[2,512,512]{2,1,0:T(8,128)(2,1)S(1)}, bf16[1024,128]{1,0:T(8,128)(2,1)S(1)}) custom-call(s32[5]{0:T(128)S(1)} %compare_select_fusion.info, f32[8]{0:T(128)S(1)} %copy-done.11, bf16[4,256,768]{2,1,0:T(8,128)(2,1)S(1)} %shard_map.159.refs_1_, f32[1,512]{1,0:T(1,128)S(1)} %bitcast.15, ...), custom_call_target="tpu_custom_call" | custom-call | tf_op jit(solution)/shard_map/pallas_call | solution.py:465
  92.1 3.9 %shard_map.163.refs_4_ = bf16[384,256]{1,0:T(8,128)(2,1)S(1)} custom-call(s32[5]{0:T(128)S(1)} %compare_select_fusion.info, f32[8]{0:T(128)S(1)} %copy-done.11, bf16[4,256,768]{2,1,0:T(8,128)(2,1)S(1)} %shard_map.159.refs_1_, f32[1,512]{1,0:T(1,128)S(1)} %bitcast.16, bf16[512,512]{1,0:T(8,128)(2,1)S(1)} %get-tuple-element.46.refs_3_, ...), custom_call_target="tpu_custom_call" | custom-call | tf_op jit(solution)/shard_map/pallas_call | solution.py:465
  98.7 5.2 %collective-permute-done.30.refs_6_ = bf16[384,256]{1,0:T(8,128)(2,1)S(1)} collective-permute-done((bf16[384,256]{1,0:T(8,128)(2,1)S(1)}, bf16[384,256]{1,0:T(8,128)(2,1)S(1)}, u32[]{:S(2)}, u32[]{:S(2)}) %collective-permute-start.30) | collective-permute-done | bytes 196640 | tf_op jit(solution)/shard_map/ppermute | solution.py:39
  103.9 3.3 %collective-permute-done.27.refs_2_ = bf16[384,256]{1,0:T(8,128)(2,1)S(1)} collective-permute-done((bf16[384,256]{1,0:T(8,128)(2,1)S(1)}, bf16[384,256]{1,0:T(8,128)(2,1)S(1)}, u32[]{:S(2)}, u32[]{:S(2)}) %collective-permute-start.27) | collective-permute-done | bytes 196640 | tf_op jit(solution)/shard_map/ppermute | solution.py:39
  110.2 1.6 %collective-permute-start.33 = (bf16[96,1024]{1,0:T(8,128)(2,1)S(1)}, bf16[96,1024]{1,0:T(8,128)(2,1)S(1)}, u32[]{:S(2)}, u32[]{:S(2)}) collective-permute-start(bf16[96,1024]{1,0:T(8,128)(2,1)S(1)} %get-tuple-element.61), channel_id=1, source_target_pairs={{0,2},{1,3},{2,0},{3,1},{4,6},{5,7},{6,4},{7,5},{8,10},{9,11},{10,... | collective-permute-start | bytes 589832 | tf_op jit(solution)/shard_map/ppermute | solution.py:39
  114.0 4.0 %collective-permute-done.33.refs_2_ = bf16[96,1024]{1,0:T(8,128)(2,1)S(1)} collective-permute-done((bf16[96,1024]{1,0:T(8,128)(2,1)S(1)}, bf16[96,1024]{1,0:T(8,128)(2,1)S(1)}, u32[]{:S(2)}, u32[]{:S(2)}) %collective-permute-start.33) | collective-permute-done | bytes 196640 | tf_op jit(solution)/shard_map/ppermute | solution.py:39
  118.0 2.6 %collective-permute-done.34.refs_3_ = bf16[96,1024]{1,0:T(8,128)(2,1)S(1)} collective-permute-done((bf16[96,1024]{1,0:T(8,128)(2,1)S(1)}, bf16[96,1024]{1,0:T(8,128)(2,1)S(1)}, u32[]{:S(2)}, u32[]{:S(2)}) %collective-permute-start.34) | collective-permute-done | bytes 196640 | tf_op jit(solution)/shard_map/ppermute | solution.py:39
  120.6 1.7 %shard_map.166 = bf16[96,4096]{1,0:T(8,128)(2,1)} custom-call(s32[5]{0:T(128)S(1)} %compare_select_fusion.info, bf16[96,1024]{1,0:T(8,128)(2,1)S(1)} %get-tuple-element.59.refs_0_, bf16[96,1024]{1,0:T(8,128)(2,1)S(1)} %collective-permute-done.32.refs_1_, bf16[96,1024]{1,0:T(8,128)(2,1)S(1)} %collective-permute-done.33.refs_2_, ...), custom_call_target="tpu_custom_call" | custom-call | tf_op jit(solution)/shard_map/pallas_call | solution.py:465
  (87 shorter events, 17.3 us)
Async XLA Ops:
  0.0 20.7 %collective-permute-start.1 = (bf16[96,4096]{1,0:T(8,128)(2,1)}, bf16[96,4096]{1,0:T(8,128)(2,1)S(1)}, u32[]{:S(2)}, u32[]{:S(2)}) collective-permute-start(bf16[96,4096]{1,0:T(8,128)(2,1)} %refs_8_.1), channel_id=1, source_target_pairs={{0,2},{1,3},{2,0},{3,1},{4,6},{5,7},{6,4},{7,5},{8,10},{9,11},{10,... | collective-permute-start | bytes 2359304 | tf_op jit(solution)/shard_map/ppermute | solution.py:39
  3.0 35.4 %collective-permute-start = (bf16[96,4096]{1,0:T(8,128)(2,1)}, bf16[96,4096]{1,0:T(8,128)(2,1)}, u32[]{:S(2)}, u32[]{:S(2)}) collective-permute-start(bf16[96,4096]{1,0:T(8,128)(2,1)} %refs_8_.1), channel_id=1, source_target_pairs={{0,1},{1,0},{2,3},{3,2},{4,5},{5,4},{6,7},{7,6},{8,9},{9,8},{10,11... | collective-permute-start | bytes 2359304 | tf_op jit(solution)/shard_map/ppermute | solution.py:39
  20.7 20.4 %collective-permute-start.2 = (bf16[96,4096]{1,0:T(8,128)(2,1)S(1)}, bf16[96,4096]{1,0:T(8,128)(2,1)S(1)}, u32[]{:S(2)}, u32[]{:S(2)}) collective-permute-start(bf16[96,4096]{1,0:T(8,128)(2,1)S(1)} %collective-permute-done.1.refs_2_), channel_id=1, source_target_pairs={{0,1},{1,0},{2,3},{3,2},{4,5},{5,4},{6,7},{7,6},{8,9},{9,8},{10,11... | collective-permute-start | bytes 2359304 | tf_op jit(solution)/shard_map/ppermute | solution.py:39
  23.1 4.0 %collective-permute-start.3 = (f32[5,1024]{1,0:T(8,128)S(1)}, f32[5,1024]{1,0:T(8,128)S(1)}, u32[]{:S(2)}, u32[]{:S(2)}) collective-permute-start(f32[5,1024]{1,0:T(8,128)S(1)} %pad_maximum_fusion), channel_id=1, source_target_pairs={{0,4},{4,0},{8,12},{12,8},{1,5},{5,1},{9,13},{13,9},{2,6},{6,2},{1... | collective-permute-start | bytes 61448 | tf_op jit(solution)/shard_map/ppermute | solution.py:39
  27.1 4.9 %collective-permute-start.4 = (f32[5,1024]{1,0:T(8,128)S(1)}, f32[5,1024]{1,0:T(8,128)S(1)}, u32[]{:S(2)}, u32[]{:S(2)}) collective-permute-start(f32[5,1024]{1,0:T(8,128)S(1)} %fusion.2), channel_id=1, source_target_pairs={{0,8},{4,12},{8,0},{12,4},{1,9},{5,13},{9,1},{13,5},{2,10},{6,14},... | collective-permute-start | bytes 61448 | tf_op jit(solution)/shard_map/ppermute | solution.py:39
  33.7 7.3 %collective-permute-start.5 = (f32[5,1024]{1,0:T(8,128)S(1)}, f32[5,1024]{1,0:T(8,128)S(1)}, u32[]{:S(2)}, u32[]{:S(2)}) collective-permute-start(f32[5,1024]{1,0:T(8,128)S(1)} %add.18.refs_4_), channel_id=1, source_target_pairs={{0,1},{1,0},{2,3},{3,2},{4,5},{5,4},{6,7},{7,6},{8,9},{9,8},{10,11... | collective-permute-start | bytes 61448 | tf_op jit(solution)/shard_map/ppermute | solution.py:39
  35.9 5.1 %collective-permute-start.7 = (f32[5,1024]{1,0:T(8,128)S(1)}, f32[5,1024]{1,0:T(8,128)S(1)}, u32[]{:S(2)}, u32[]{:S(2)}) collective-permute-start(f32[5,1024]{1,0:T(8,128)S(1)} %collective-permute-done.6.refs_6_), channel_id=1, source_target_pairs={{0,1},{1,0},{2,3},{3,2},{4,5},{5,4},{6,7},{7,6},{8,9},{9,8},{10,11... | collective-permute-start | bytes 61448 | tf_op jit(solution)/shard_map/ppermute | solution.py:39
  45.4 6.1 %collective-permute-start.24 = (bf16[544,128]{1,0:T(8,128)(2,1)S(1)}, bf16[544,128]{1,0:T(8,128)(2,1)S(1)}, u32[]{:S(2)}, u32[]{:S(2)}) collective-permute-start(bf16[544,128]{1,0:T(8,128)(2,1)S(1)} %get-tuple-element.48.refs_5_), channel_id=1, source_target_pairs={{0,2},{1,3},{2,0},{3,1},{4,6},{5,7},{6,4},{7,5},{8,10},{9,11},{10,... | collective-permute-start | bytes 417800 | tf_op jit(solution)/shard_map/ppermute | solution.py:39
  47.1 7.2 %collective-permute-start.23 = (bf16[544,128]{1,0:T(8,128)(2,1)S(1)}, bf16[544,128]{1,0:T(8,128)(2,1)S(1)}, u32[]{:S(2)}, u32[]{:S(2)}) collective-permute-start(bf16[544,128]{1,0:T(8,128)(2,1)S(1)} %get-tuple-element.48.refs_5_), channel_id=1, source_target_pairs={{0,1},{1,0},{2,3},{3,2},{4,5},{5,4},{6,7},{7,6},{8,9},{9,8},{10,11... | collective-permute-start | bytes 417800 | tf_op jit(solution)/shard_map/ppermute | solution.py:39
  47.4 8.8 %collective-permute-start.19 = (bf16[544,128]{1,0:T(8,128)(2,1)S(1)}, bf16[544,128]{1,0:T(8,128)(2,1)S(1)}, u32[]{:S(2)}, u32[]{:S(2)}) collective-permute-start(bf16[544,128]{1,0:T(8,128)(2,1)S(1)} %get-tuple-element.48.refs_5_), channel_id=1, source_target_pairs={{0,4},{4,0},{8,12},{12,8},{1,5},{5,1},{9,13},{13,9},{2,6},{6,2},{1... | collective-permute-start | bytes 417800 | tf_op jit(solution)/shard_map/ppermute | solution.py:39
  48.9 7.2 %collective-permute-start.9 = (bf16[384,256]{1,0:T(8,128)(2,1)S(1)}, bf16[384,256]{1,0:T(8,128)(2,1)S(1)}, u32[]{:S(2)}, u32[]{:S(2)}) collective-permute-start(bf16[384,256]{1,0:T(8,128)(2,1)S(1)} %get-tuple-element.43.refs_0_), channel_id=1, source_target_pairs={{0,2},{1,3},{2,0},{3,1},{4,6},{5,7},{6,4},{7,5},{8,10},{9,11},{10,... | collective-permute-start | bytes 589832 | tf_op jit(solution)/shard_map/ppermute | solution.py:39
  49.5 17.1 %collective-permute-start.8 = (bf16[384,256]{1,0:T(8,128)(2,1)S(1)}, bf16[384,256]{1,0:T(8,128)(2,1)S(1)}, u32[]{:S(2)}, u32[]{:S(2)}) collective-permute-start(bf16[384,256]{1,0:T(8,128)(2,1)S(1)} %get-tuple-element.43.refs_0_), channel_id=1, source_target_pairs={{0,1},{1,0},{2,3},{3,2},{4,5},{5,4},{6,7},{7,6},{8,9},{9,8},{10,11... | collective-permute-start | bytes 589832 | tf_op jit(solution)/shard_map/ppermute | solution.py:39
  51.5 13.4 %collective-permute-start.11 = (bf16[544,128]{1,0:T(8,128)(2,1)S(1)}, bf16[544,128]{1,0:T(8,128)(2,1)S(1)}, u32[]{:S(2)}, u32[]{:S(2)}) collective-permute-start(bf16[544,128]{1,0:T(8,128)(2,1)S(1)} %get-tuple-element.48.refs_5_), channel_id=1, source_target_pairs={{0,8},{4,12},{8,0},{12,4},{1,9},{5,13},{9,1},{13,5},{2,10},{6,14},... | collective-permute-start | bytes 417800 | tf_op jit(solution)/shard_map/ppermute | solution.py:39
  54.3 12.2 %collective-permute-start.15 = (bf16[544,128]{1,0:T(8,128)(2,1)S(1)}, bf16[544,128]{1,0:T(8,128)(2,1)S(1)}, u32[]{:S(2)}, u32[]{:S(2)}) collective-permute-start(bf16[544,128]{1,0:T(8,128)(2,1)S(1)} %get-tuple-element.48.refs_5_), channel_id=1, source_target_pairs={{0,12},{4,8},{8,4},{12,0},{1,13},{5,9},{9,5},{13,1},{2,14},{6,10},... | collective-permute-start | bytes 417800 | tf_op jit(solution)/shard_map/ppermute | solution.py:39
  56.1 10.9 %collective-permute-start.25 = (bf16[544,128]{1,0:T(8,128)(2,1)S(1)}, bf16[544,128]{1,0:T(8,128)(2,1)S(1)}, u32[]{:S(2)}, u32[]{:S(2)}) collective-permute-start(bf16[544,128]{1,0:T(8,128)(2,1)S(1)} %collective-permute-done.24.refs_7_), channel_id=1, source_target_pairs={{0,1},{1,0},{2,3},{3,2},{4,5},{5,4},{6,7},{7,6},{8,9},{9,8},{10,11... | collective-permute-start | bytes 417800 | tf_op jit(solution)/shard_map/ppermute | solution.py:39
  56.1 19.8 %collective-permute-start.10 = (bf16[384,256]{1,0:T(8,128)(2,1)S(1)}, bf16[384,256]{1,0:T(8,128)(2,1)S(1)}, u32[]{:S(2)}, u32[]{:S(2)}) collective-permute-start(bf16[384,256]{1,0:T(8,128)(2,1)S(1)} %collective-permute-done.9.refs_2_), channel_id=1, source_target_pairs={{0,1},{1,0},{2,3},{3,2},{4,5},{5,4},{6,7},{7,6},{8,9},{9,8},{10,11... | collective-permute-start | bytes 589832 | tf_op jit(solution)/shard_map/ppermute | solution.py:39
  64.9 5.8 %collective-permute-start.21 = (bf16[544,128]{1,0:T(8,128)(2,1)S(1)}, bf16[544,128]{1,0:T(8,128)(2,1)S(1)}, u32[]{:S(2)}, u32[]{:S(2)}) collective-permute-start(bf16[544,128]{1,0:T(8,128)(2,1)S(1)} %collective-permute-done.19.refs_5_), channel_id=1, source_target_pairs={{0,2},{1,3},{2,0},{3,1},{4,6},{5,7},{6,4},{7,5},{8,10},{9,11},{10,... | collective-permute-start | bytes 417800 | tf_op jit(solution)/shard_map/ppermute | solution.py:39
  66.6 4.1 %collective-permute-start.20 = (bf16[544,128]{1,0:T(8,128)(2,1)S(1)}, bf16[544,128]{1,0:T(8,128)(2,1)S(1)}, u32[]{:S(2)}, u32[]{:S(2)}) collective-permute-start(bf16[544,128]{1,0:T(8,128)(2,1)S(1)} %collective-permute-done.19.refs_5_), channel_id=1, source_target_pairs={{0,1},{1,0},{2,3},{3,2},{4,5},{5,4},{6,7},{7,6},{8,9},{9,8},{10,11... | collective-permute-start | bytes 417800 | tf_op jit(solution)/shard_map/ppermute | solution.py:39
  66.6 6.9 %collective-permute-start.13 = (bf16[544,128]{1,0:T(8,128)(2,1)S(1)}, bf16[544,128]{1,0:T(8,128)(2,1)S(1)}, u32[]{:S(2)}, u32[]{:S(2)}) collective-permute-start(bf16[544,128]{1,0:T(8,128)(2,1)S(1)} %collective-permute-done.11.refs_5_), channel_id=1, source_target_pairs={{0,2},{1,3},{2,0},{3,1},{4,6},{5,7},{6,4},{7,5},{8,10},{9,11},{10,... | collective-permute-start | bytes 417800 | tf_op jit(solution)/shard_map/ppermute | solution.py:39
  67.0 8.9 %collective-permute-start.17 = (bf16[544,128]{1,0:T(8,128)(2,1)S(1)}, bf16[544,128]{1,0:T(8,128)(2,1)S(1)}, u32[]{:S(2)}, u32[]{:S(2)}) collective-permute-start(bf16[544,128]{1,0:T(8,128)(2,1)S(1)} %collective-permute-done.15.refs_9_), channel_id=1, source_target_pairs={{0,2},{1,3},{2,0},{3,1},{4,6},{5,7},{6,4},{7,5},{8,10},{9,11},{10,... | collective-permute-start | bytes 417800 | tf_op jit(solution)/shard_map/ppermute | solution.py:39
  70.6 13.1 %collective-permute-start.22 = (bf16[544,128]{1,0:T(8,128)(2,1)S(1)}, bf16[544,128]{1,0:T(8,128)(2,1)S(1)}, u32[]{:S(2)}, u32[]{:S(2)}) collective-permute-start(bf16[544,128]{1,0:T(8,128)(2,1)S(1)} %collective-permute-done.21.refs_7_), channel_id=1, source_target_pairs={{0,1},{1,0},{2,3},{3,2},{4,5},{5,4},{6,7},{7,6},{8,9},{9,8},{10,11... | collective-permute-start | bytes 417800 | tf_op jit(solution)/shard_map/ppermute | solution.py:39
  70.7 17.1 %collective-permute-start.12 = (bf16[544,128]{1,0:T(8,128)(2,1)S(1)}, bf16[544,128]{1,0:T(8,128)(2,1)S(1)}, u32[]{:S(2)}, u32[]{:S(2)}) collective-permute-start(bf16[544,128]{1,0:T(8,128)(2,1)S(1)} %collective-permute-done.11.refs_5_), channel_id=1, source_target_pairs={{0,1},{1,0},{2,3},{3,2},{4,5},{5,4},{6,7},{7,6},{8,9},{9,8},{10,11... | collective-permute-start | bytes 417800 | tf_op jit(solution)/shard_map/ppermute | solution.py:39
  73.5 14.3 %collective-permute-start.16 = (bf16[544,128]{1,0:T(8,128)(2,1)S(1)}, bf16[544,128]{1,0:T(8,128)(2,1)S(1)}, u32[]{:S(2)}, u32[]{:S(2)}) collective-permute-start(bf16[544,128]{1,0:T(8,128)(2,1)S(1)} %collective-permute-done.15.refs_9_), channel_id=1, source_target_pairs={{0,1},{1,0},{2,3},{3,2},{4,5},{5,4},{6,7},{7,6},{8,9},{9,8},{10,11... | collective-permute-start | bytes 417800 | tf_op jit(solution)/shard_map/ppermute | solution.py:39
  75.9 11.9 %collective-permute-start.14 = (bf16[544,128]{1,0:T(8,128)(2,1)S(1)}, bf16[544,128]{1,0:T(8,128)(2,1)S(1)}, u32[]{:S(2)}, u32[]{:S(2)}) collective-permute-start(bf16[544,128]{1,0:T(8,128)(2,1)S(1)} %collective-permute-done.13.refs_7_), channel_id=1, source_target_pairs={{0,1},{1,0},{2,3},{3,2},{4,5},{5,4},{6,7},{7,6},{8,9},{9,8},{10,11... | collective-permute-start | bytes 417800 | tf_op jit(solution)/shard_map/ppermute | solution.py:39
  75.9 11.9 %collective-permute-start.18 = (bf16[544,128]{1,0:T(8,128)(2,1)S(1)}, bf16[544,128]{1,0:T(8,128)(2,1)S(1)}, u32[]{:S(2)}, u32[]{:S(2)}) collective-permute-start(bf16[544,128]{1,0:T(8,128)(2,1)S(1)} %collective-permute-done.17.refs_11_), channel_id=1, source_target_pairs={{0,1},{1,0},{2,3},{3,2},{4,5},{5,4},{6,7},{7,6},{8,9},{9,8},{10,11... | collective-permute-start | bytes 417800 | tf_op jit(solution)/shard_map/ppermute | solution.py:39
  96.1 7.8 %collective-permute-start.30 = (bf16[384,256]{1,0:T(8,128)(2,1)S(1)}, bf16[384,256]{1,0:T(8,128)(2,1)S(1)}, u32[]{:S(2)}, u32[]{:S(2)}) collective-permute-start(bf16[384,256]{1,0:T(8,128)(2,1)S(1)} %shard_map.163.refs_4_), channel_id=1, source_target_pairs={{0,2},{1,3},{2,0},{3,1},{4,6},{5,7},{6,4},{7,5},{8,10},{9,11},{10,... | collective-permute-start | bytes 589832 | tf_op jit(solution)/shard_map/ppermute | solution.py:39
  97.7 9.5 %collective-permute-start.27 = (bf16[384,256]{1,0:T(8,128)(2,1)S(1)}, bf16[384,256]{1,0:T(8,128)(2,1)S(1)}, u32[]{:S(2)}, u32[]{:S(2)}) collective-permute-start(bf16[384,256]{1,0:T(8,128)(2,1)S(1)} %get-tuple-element.55.refs_0_), channel_id=1, source_target_pairs={{0,2},{1,3},{2,0},{3,1},{4,6},{5,7},{6,4},{7,5},{8,10},{9,11},{10,... | collective-permute-start | bytes 589832 | tf_op jit(solution)/shard_map/ppermute | solution.py:39
  98.1 9.0 %collective-permute-start.29 = (bf16[384,256]{1,0:T(8,128)(2,1)S(1)}, bf16[384,256]{1,0:T(8,128)(2,1)S(1)}, u32[]{:S(2)}, u32[]{:S(2)}) collective-permute-start(bf16[384,256]{1,0:T(8,128)(2,1)S(1)} %shard_map.163.refs_4_), channel_id=1, source_target_pairs={{0,1},{1,0},{2,3},{3,2},{4,5},{5,4},{6,7},{7,6},{8,9},{9,8},{10,11... | collective-permute-start | bytes 589832 | tf_op jit(solution)/shard_map/ppermute | solution.py:39
  98.1 9.0 %collective-permute-start.26 = (bf16[384,256]{1,0:T(8,128)(2,1)S(1)}, bf16[384,256]{1,0:T(8,128)(2,1)S(1)}, u32[]{:S(2)}, u32[]{:S(2)}) collective-permute-start(bf16[384,256]{1,0:T(8,128)(2,1)S(1)} %get-tuple-element.55.refs_0_), channel_id=1, source_target_pairs={{0,1},{1,0},{2,3},{3,2},{4,5},{5,4},{6,7},{7,6},{8,9},{9,8},{10,11... | collective-permute-start | bytes 589832 | tf_op jit(solution)/shard_map/ppermute | solution.py:39
  110.2 7.8 %collective-permute-start.33 = (bf16[96,1024]{1,0:T(8,128)(2,1)S(1)}, bf16[96,1024]{1,0:T(8,128)(2,1)S(1)}, u32[]{:S(2)}, u32[]{:S(2)}) collective-permute-start(bf16[96,1024]{1,0:T(8,128)(2,1)S(1)} %get-tuple-element.61), channel_id=1, source_target_pairs={{0,2},{1,3},{2,0},{3,1},{4,6},{5,7},{6,4},{7,5},{8,10},{9,11},{10,... | collective-permute-start | bytes 589832 | tf_op jit(solution)/shard_map/ppermute | solution.py:39
  111.8 8.8 %collective-permute-start.34 = (bf16[96,1024]{1,0:T(8,128)(2,1)S(1)}, bf16[96,1024]{1,0:T(8,128)(2,1)S(1)}, u32[]{:S(2)}, u32[]{:S(2)}) collective-permute-start(bf16[96,1024]{1,0:T(8,128)(2,1)S(1)} %get-tuple-element.62), channel_id=1, source_target_pairs={{0,3},{1,2},{2,1},{3,0},{4,7},{5,6},{6,5},{7,4},{8,11},{9,10},{10,... | collective-permute-start | bytes 589832 | tf_op jit(solution)/shard_map/ppermute | solution.py:39
  113.4 7.2 %collective-permute-start.32 = (bf16[96,1024]{1,0:T(8,128)(2,1)S(1)}, bf16[96,1024]{1,0:T(8,128)(2,1)S(1)}, u32[]{:S(2)}, u32[]{:S(2)}) collective-permute-start(bf16[96,1024]{1,0:T(8,128)(2,1)S(1)} %get-tuple-element.60), channel_id=1, source_target_pairs={{0,1},{1,0},{2,3},{3,2},{4,5},{5,4},{6,7},{7,6},{8,9},{9,8},{10,11... | collective-permute-start | bytes 589832 | tf_op jit(solution)/shard_map/ppermute | solution.py:39
  (17 other events, 335.0 us)
